TPU v7x, 32 devices: a whole 2x2x4 slice. The times are simulated.
32 devices in a mesh: sp: 4 (over z), dp: 8 (over y, x, core).
Axes of the slice: x: 2, y: 2, z: 4, core: 2. Of those that a mesh axis runs over, the one named last changes fastest.
Arguments:
- hidden: bfloat16 [8, 512, 2048], P('dp', 'sp'), may hold values from -6 to 6
- queries: bfloat16 [8, 512, 1024], P('dp', 'sp'), may hold values from -6 to 6
- values: bfloat16 [8, 512, 2048], P('dp', 'sp'), may hold values from -6 to 6
- key_weight: bfloat16 [2048, 1024], P('dp'), may hold values from -0.125 to 0.125
- decay_down: bfloat16 [2048, 16], replicated, may hold values from -0.125 to 0.125
- decay_up: float32 [16, 1024], replicated, may hold values from -1.5 to 1.5
- decay_bias: float32 [1024], replicated, may hold values from -1 to 8
- span_shift: bfloat16 [8, 512], P('dp', 'sp'), may hold values from -1.5 to 1.5, as said below
- norm_gain: float32 [2048], replicated, may hold values from 0.1 to 1.9
Outputs:
- attended: bfloat16 [8, 512, 2048], P('dp', 'sp')
Inputs may be any that keep to these rules, and one draw needn't show every extreme that they name: `span_shift`: constant over each aligned block of 64 positions.
All inputs are finite; a program needn't handle non-finite values.
Results may differ from a plain program's by a relative error of at most 0.0073.
Values may be sent and summed in bfloat16 or wider, within the bound.
No kernel may reach another device: no remote copies, remote signals or barrier semaphores. Data moves between devices by JAX's collectives and lax.ppermute only.
A program may use at most 64 MiB of HBM per device.

v0:
```python
import jax
import jax.numpy as jnp
from jax import lax
from jax.experimental import pallas as pl
from jax.experimental.pallas import tpu as pltpu

from jax.sharding import PartitionSpec as P

HEADS = 4
DK = 256
DV = 512
BLOCK = 64
KEY = 1024
VAL = 2048


decay_tau = 16.0
norm_eps = 1e-05
highest = lax.Precision.HIGHEST


def mechanism(query, keys_in, value_in, log_decay):
    length, key_width = query.shape
    value_width = value_in.shape[-1]
    blocks = length // BLOCK
    step_decay = log_decay.reshape(blocks, BLOCK, key_width)
    inclusive = jnp.cumsum(step_decay, axis=1)
    exclusive = inclusive - step_decay
    total = inclusive[:, -1, :]
    query3 = query.reshape(blocks, BLOCK, key_width)
    keys3 = keys_in.reshape(blocks, BLOCK, key_width)
    value_tensor3 = value_in.reshape(blocks, BLOCK, value_width)
    query_forward_part = (query3 * jnp.exp(inclusive)).astype(jnp.bfloat16)
    key_fwd = (keys3 * jnp.exp(-inclusive)).astype(jnp.bfloat16)
    query_reverse_part = (query3 * jnp.exp(-exclusive)).astype(jnp.bfloat16)
    key_bwd = (keys3 * jnp.exp(exclusive)).astype(jnp.bfloat16)
    key_end = (keys3 * jnp.exp(total[:, None, :] - inclusive)).astype(jnp.bfloat16)
    fwd_scores = jnp.einsum(
        "nid,njd->nij", query_forward_part, key_fwd, preferred_element_type=jnp.float32
    )
    bwd_scores = jnp.einsum(
        "nid,njd->nij", query_reverse_part, key_bwd, preferred_element_type=jnp.float32
    )
    row_index = lax.broadcasted_iota(jnp.int32, (BLOCK, BLOCK), 0)
    col_index = lax.broadcasted_iota(jnp.int32, (BLOCK, BLOCK), 1)
    attention_scores = jnp.where((col_index <= row_index)[None], fwd_scores, bwd_scores).astype(
        jnp.bfloat16
    )
    inner_block_term = jnp.einsum(
        "ucy,uyh->uch", attention_scores, value_tensor3, preferred_element_type=jnp.float32
    )
    end_terms = jnp.einsum(
        "njd,nje->nde", key_end, value_tensor3, preferred_element_type=jnp.float32
    )
    start_terms = jnp.einsum(
        "njd,nje->nde", key_bwd, value_tensor3, preferred_element_type=jnp.float32
    )
    rates = jnp.exp(total)

    def forward_step(carry_state, inputs):
        rate, term = inputs
        return (rate[:, None] * carry_state + term, carry_state)

    def backward_step(carry_state, inputs):
        rate, term = inputs
        state_here = rate[:, None] * carry_state
        return (state_here + term, state_here)

    empty = jnp.zeros((key_width, value_width), jnp.float32)
    _, forward_scan_states = lax.scan(forward_step, empty, (rates, end_terms))
    _, reverse_scan_states = lax.scan(backward_step, empty, (rates, start_terms), reverse=True)
    produced_rows = jnp.einsum(
        "tzv,tvg->tzg",
        query_forward_part,
        forward_scan_states.astype(jnp.bfloat16),
        preferred_element_type=jnp.float32,
    )
    produced_rows = produced_rows + jnp.einsum(
        "tzv,tvg->tzg",
        query_reverse_part,
        reverse_scan_states.astype(jnp.bfloat16),
        preferred_element_type=jnp.float32,
    )
    return (inner_block_term + produced_rows).reshape(length, value_width).astype(jnp.bfloat16)


def general_body(
    hidden, queries, values, key_weight, decay_down, decay_up, decay_bias, span_shift, norm_gain
):
    seq_count, tok_count, model_width = hidden.shape
    group_size = lax.axis_size("sp")
    value_split = group_size // HEADS
    part_width = DV // value_split
    head_index = lax.axis_index("sp") // value_split
    token_rows = hidden.reshape(tok_count, model_width)

    def per_item(tensor, width):
        by_head = tensor.reshape(tok_count, HEADS, width).transpose(1, 0, 2)
        spread_out = jnp.broadcast_to(by_head[:, None], (HEADS, value_split, tok_count, width))
        return spread_out.reshape(group_size, tok_count, width)

    def every_item(tensor):
        return jnp.broadcast_to(tensor[None], (group_size,) + tensor.shape)

    key_sums = jnp.dot(
        token_rows,
        lax.all_gather(key_weight, "dp", axis=0, tiled=True),
        preferred_element_type=jnp.float32,
    )
    keys = key_sums.astype(jnp.bfloat16)
    head_key = lax.all_to_all(per_item(keys, DK), "sp", split_axis=0, concat_axis=1, tiled=True)[0]
    low = jnp.dot(token_rows, decay_down, preferred_element_type=jnp.float32).astype(jnp.bfloat16)
    value_items = values.reshape(tok_count, group_size, part_width).transpose(1, 0, 2)
    head_query, head_value, head_low, head_shift = (
        lax.all_to_all(
            per_item(queries.reshape(tok_count, KEY), DK),
            "sp",
            split_axis=0,
            concat_axis=1,
            tiled=True,
        ),
        lax.all_to_all(value_items, "sp", split_axis=0, concat_axis=1, tiled=True),
        lax.all_to_all(every_item(low), "sp", split_axis=0, concat_axis=1, tiled=True),
        lax.all_to_all(
            every_item(span_shift.reshape(tok_count, 1)),
            "sp",
            split_axis=0,
            concat_axis=1,
            tiled=True,
        ),
    )
    up_columns = lax.dynamic_slice_in_dim(decay_up, head_index * DK, DK, 1)
    bias_part = lax.dynamic_slice_in_dim(decay_bias, head_index * DK, DK, 0)
    pre = jnp.dot(
        head_low[0].astype(jnp.float32),
        up_columns,
        precision=highest,
        preferred_element_type=jnp.float32,
    )
    pre = pre + bias_part[None, :] + head_shift[0].astype(jnp.float32)
    log_decay = jax.nn.log_sigmoid(pre) / decay_tau
    scaled = head_query[0].astype(jnp.float32) * DK ** (-0.5)
    mixed = mechanism(scaled, head_key.astype(jnp.float32), head_value[0], log_decay)
    returned = lax.all_to_all(mixed[None], "sp", split_axis=1, concat_axis=0, tiled=True)
    grouped = returned.astype(jnp.float32).transpose(1, 0, 2).reshape(tok_count, HEADS, DV)
    normed = grouped * lax.rsqrt(jnp.mean(grouped * grouped, axis=-1, keepdims=True) + norm_eps)
    normed = normed * norm_gain.reshape(HEADS, DV)[None]
    return normed.reshape(seq_count, tok_count, VAL).astype(jnp.bfloat16)


GROUP = 4 * BLOCK
PACK = 8


def room(mebibytes):
    return pltpu.CompilerParams(vmem_limit_bytes=mebibytes * 2**20)


def exchange(tensor, axis, flip):
    size = lax.axis_size(axis)
    return lax.ppermute(tensor, axis, [(i, i ^ flip) for i in range(size)])


def dot_nn(left, right):
    return lax.dot_general(
        left, right, (((1,), (0,)), ((), ())), preferred_element_type=jnp.float32
    )


def dot_nt(left, right):
    return lax.dot_general(
        left, right, (((1,), (1,)), ((), ())), preferred_element_type=jnp.float32
    )


def dot_tn(left, right):
    return lax.dot_general(
        left, right, (((0,), (0,)), ((), ())), preferred_element_type=jnp.float32
    )


def columns_kernel(place_ref, weight_ref, out_ref, sems):
    copies = []
    for half in range(2):
        at = pl.multiple_of((place_ref[0] ^ (2 * half)) * DK, DK)
        copies.append(
            pltpu.make_async_copy(
                weight_ref.at[:, pl.ds(at, DK)],
                out_ref.at[:, pl.ds(half * DK, DK)],
                sems.at[half],
            )
        )
    for copy in copies:
        copy.start()
    for copy in copies:
        copy.wait()


def take_columns(place, weight):
    rows = weight.shape[0]
    return pl.pallas_call(
        columns_kernel,
        in_specs=[pl.BlockSpec(memory_space=pltpu.SMEM), pl.BlockSpec(memory_space=pl.ANY)],
        out_specs=pl.BlockSpec(memory_space=pltpu.VMEM),
        out_shape=jax.ShapeDtypeStruct((rows, 2 * DK), weight.dtype),
        scratch_shapes=[pltpu.SemaphoreType.DMA((2,))],
        compiler_params=room(8),
        name="columns",
    )(place, weight)


def parcels_kernel(place_ref, hidden_ref, down_ref, shift_ref, query_ref, value_ref, *refs):
    out_refs, sems = refs[:HEADS], refs[HEADS]
    tok_count = query_ref.shape[0]
    copies = []
    for flip, out_ref in enumerate(out_refs):
        head = place_ref[0] ^ flip
        for which, (source, width, at) in enumerate(((query_ref, DK, 0), (value_ref, DV, DK))):
            copies.append(
                pltpu.make_async_copy(
                    source.at[:, pl.ds(pl.multiple_of(head * width, width), width)],
                    out_ref.at[pl.ds(0, tok_count), pl.ds(at, width)],
                    sems.at[flip, which],
                )
            )
    for copy in copies:
        copy.start()
    low = dot_nt(down_ref[...], hidden_ref[...]).astype(jnp.bfloat16)
    shift = jnp.broadcast_to(shift_ref[...].astype(jnp.float32), (PACK, tok_count))
    empty = jnp.zeros((PACK, DK + DV - 3 * tok_count), jnp.float32)
    low = low.astype(jnp.float32)
    tail = jnp.concatenate([low[:PACK], low[PACK:], shift, empty], axis=1).astype(jnp.bfloat16)
    for out_ref in out_refs:
        out_ref[tok_count:, :] = tail
    for copy in copies:
        copy.wait()


def make_parcels(place, token_rows, decay_down, queries, values, shift):
    tok_count = token_rows.shape[0]
    shape = jax.ShapeDtypeStruct((tok_count + PACK, DK + DV), jnp.bfloat16)
    return pl.pallas_call(
        parcels_kernel,
        in_specs=[pl.BlockSpec(memory_space=pltpu.SMEM)]
        + [pl.BlockSpec(memory_space=pltpu.VMEM)] * 3
        + [pl.BlockSpec(memory_space=pl.ANY)] * 2,
        out_specs=[pl.BlockSpec(memory_space=pltpu.VMEM)] * HEADS,
        out_shape=[shape] * HEADS,
        scratch_shapes=[pltpu.SemaphoreType.DMA((HEADS, 2))],
        compiler_params=room(8),
        name="parcels",
    )(place, token_rows, decay_down.T, shift, queries, values)


def keys_kernel(rank_ref, hidden_ref, peer_ref, *refs):
    pieces, (own_ref, send_ref) = refs[:-2], refs[-2:]
    tok_count = hidden_ref.shape[0]
    sums = jnp.zeros((2 * tok_count, 2 * DK), jnp.float32)
    for flip, piece in enumerate(pieces):
        rows = piece.shape[0]
        at = pl.multiple_of((rank_ref[0] ^ flip) * rows, rows)
        both = jnp.concatenate([hidden_ref[:, pl.ds(at, rows)], peer_ref[:, pl.ds(at, rows)]], axis=0)
        sums = sums + dot_nn(both, piece[...])
    keys = sums.astype(jnp.bfloat16)
    own_ref[...] = keys[:, :DK]
    send_ref[...] = keys[:, DK:]


def project_keys(rank, token_rows, peer_rows, pieces):
    tok_count = token_rows.shape[0]
    shape = jax.ShapeDtypeStruct((2 * tok_count, DK), jnp.bfloat16)
    return pl.pallas_call(
        keys_kernel,
        in_specs=[pl.BlockSpec(memory_space=pltpu.SMEM)]
        + [pl.BlockSpec(memory_space=pltpu.VMEM)] * (2 + len(pieces)),
        out_shape=[shape, shape],
        compiler_params=room(12),
        name="keys",
    )(rank, token_rows, peer_rows, *pieces)


def split3(tensor):
    first = tensor.astype(jnp.bfloat16)
    rest = tensor - first.astype(jnp.float32)
    second = rest.astype(jnp.bfloat16)
    third = (rest - second.astype(jnp.float32)).astype(jnp.bfloat16)
    return first, second, third


def mechanism_kernel(
    place_ref, up_ref, bias_ref, gain_ref, own_ref, got_ref, p0, p1, p2, p3, *refs
):
    outs, (query_s, value_s, key_s, low_s, mixed_s, fwd_s, bwd_s) = refs[:HEADS], refs[HEADS:]
    place = place_ref[0]
    tok_count = outs[0].shape[0]
    length = query_s.shape[0]
    rank = up_ref.shape[0]
    for flip, parcel in enumerate((p0, p1, p2, p3)):
        at = pl.ds(pl.multiple_of((place ^ flip) * tok_count, tok_count), tok_count)
        query_s[at, :] = parcel[:tok_count, :DK]
        value_s[at, :] = parcel[:tok_count, DK:]
        keys = own_ref if flip < 2 else got_ref
        key_s[at, :] = keys[pl.ds((flip % 2) * tok_count, tok_count), :]
        low = parcel[tok_count:, :tok_count].astype(jnp.float32)
        high = parcel[tok_count:, tok_count : 2 * tok_count].astype(jnp.float32)
        shift = parcel[tok_count:, 2 * tok_count : 3 * tok_count].astype(jnp.float32)
        row = lax.broadcasted_iota(jnp.int32, shift.shape, 0)
        first = jnp.where(row == 0, shift, 0.0)
        stack = jnp.concatenate([low, high] * 3 + [first, jnp.zeros_like(first)], axis=0)
        low_s[:, at] = stack.astype(jnp.bfloat16)
    ones = (lax.broadcasted_iota(jnp.int32, (rank, DK), 0) == 0).astype(jnp.float32)
    up = jnp.concatenate(
        [part.astype(jnp.float32) for part in split3(up_ref[...])] + [ones], axis=0
    ).astype(jnp.bfloat16)
    pre = dot_tn(low_s[...], up) + bias_ref[...]
    log_decay = (jnp.minimum(pre, 0.0) - jnp.log1p(jnp.exp(-jnp.abs(pre)))) * (1.0 / decay_tau)

    row = lax.broadcasted_iota(jnp.int32, (GROUP, GROUP), 0)
    col = lax.broadcasted_iota(jnp.int32, (GROUP, GROUP), 1)
    same = (row // BLOCK) == (col // BLOCK)
    lower = same & (col <= row)
    upper = same & (col > row)
    sum_up_to = jnp.where(lower, 1.0, 0.0).astype(jnp.bfloat16)
    steps = [[] for _ in range(5)]
    rates = []
    for start in range(0, length, GROUP):
        decay = log_decay[start : start + GROUP]
        inclusive = sum(dot_nn(sum_up_to, part) for part in split3(decay))
        exclusive = inclusive - decay
        by_block = inclusive.reshape(GROUP // BLOCK, BLOCK, DK)
        total = by_block[:, BLOCK - 1 :, :]
        scaled = query_s[start : start + GROUP, :].astype(jnp.float32) * DK**-0.5
        keys = key_s[start : start + GROUP, :].astype(jnp.float32)
        query_fwd = (scaled * jnp.exp(inclusive)).astype(jnp.bfloat16)
        key_fwd = (keys * jnp.exp(-inclusive)).astype(jnp.bfloat16)
        query_bwd = (scaled * jnp.exp(-exclusive)).astype(jnp.bfloat16)
        key_bwd = (keys * jnp.exp(exclusive)).astype(jnp.bfloat16)
        key_end = (keys * jnp.exp(total - by_block).reshape(GROUP, DK)).astype(jnp.bfloat16)
        scores = jnp.where(
            lower, dot_nt(query_fwd, key_fwd), jnp.where(upper, dot_nt(query_bwd, key_bwd), 0.0)
        ).astype(jnp.bfloat16)
        mixed_s[start : start + GROUP, :] = dot_nn(scores, value_s[start : start + GROUP, :])
        for block in range(GROUP // BLOCK):
            at = slice(block * BLOCK, (block + 1) * BLOCK)
            for kept, tensor in zip(steps, (query_fwd, query_bwd, key_bwd, key_end)):
                kept.append(tensor[at])
            rates.append(jnp.exp(total[block]))
    query_fwd, query_bwd, key_bwd, key_end = steps[:4]
    blocks = length // BLOCK

    def rows(block):
        return slice(block * BLOCK, (block + 1) * BLOCK)

    for block in range(1, blocks):
        term = dot_tn(value_s[rows(block - 1), :], key_end[block - 1])
        if block > 1:
            term = term + fwd_s[...] * rates[block - 1]
        fwd_s[...] = term
        mixed_s[rows(block), :] += dot_nt(query_fwd[block], term.astype(jnp.bfloat16))
        back = blocks - 1 - block
        term = dot_tn(value_s[rows(back + 1), :], key_bwd[back + 1])
        if block > 1:
            term = term + bwd_s[...]
        term = term * rates[back]
        bwd_s[...] = term
        mixed_s[rows(back), :] += dot_nt(query_bwd[back], term.astype(jnp.bfloat16))

    for flip, out_ref in enumerate(outs):
        at = pl.ds(pl.multiple_of((place ^ flip) * tok_count, tok_count), tok_count)
        mixed = mixed_s[at, :].astype(jnp.bfloat16).astype(jnp.float32)
        mean = jnp.mean(mixed * mixed, axis=-1, keepdims=True)
        out_ref[...] = (mixed * lax.rsqrt(mean + norm_eps) * gain_ref[...]).astype(jnp.bfloat16)


def mix_heads(place, decay_up, decay_bias, norm_gain, own, got, parcels):
    tok_count = parcels[0].shape[0] - PACK
    length = HEADS * tok_count
    rank = decay_up.shape[0]
    whole = lambda a: pl.BlockSpec(a.shape, lambda i, p: (0,) * a.ndim)
    out = jax.ShapeDtypeStruct((tok_count, DV), jnp.bfloat16)
    return pl.pallas_call(
        mechanism_kernel,
        grid_spec=pltpu.PrefetchScalarGridSpec(
            num_scalar_prefetch=1,
            grid=(1,),
            in_specs=[
                pl.BlockSpec((rank, DK), lambda i, p: (0, p[0])),
                pl.BlockSpec((1, DK), lambda i, p: (0, p[0])),
                pl.BlockSpec((1, DV), lambda i, p: (0, p[0])),
            ]
            + [whole(a) for a in (own, got, *parcels)],
            out_specs=[whole(out)] * HEADS,
            scratch_shapes=[
                pltpu.VMEM((length, DK), jnp.bfloat16),
                pltpu.VMEM((length, DV), jnp.bfloat16),
                pltpu.VMEM((length, DK), jnp.bfloat16),
                pltpu.VMEM((4 * rank, length), jnp.bfloat16),
                pltpu.VMEM((length, DV), jnp.float32),
                pltpu.VMEM((DV, DK), jnp.float32),
                pltpu.VMEM((DV, DK), jnp.float32),
            ],
        ),
        out_shape=[out] * HEADS,
        compiler_params=room(24),
        name="mechanism",
    )(
        place,
        decay_up,
        decay_bias.reshape(1, -1),
        norm_gain.reshape(1, -1),
        own,
        got,
        *parcels,
    )


def join_kernel(place_ref, *refs):
    out_ref = refs[-1]
    for flip, part in enumerate(refs[:-1]):
        at = pl.multiple_of((place_ref[0] ^ flip) * DV, DV)
        out_ref[:, pl.ds(at, DV)] = part[...]


def join_heads(place, parts):
    return pl.pallas_call(
        join_kernel,
        in_specs=[pl.BlockSpec(memory_space=pltpu.SMEM)]
        + [pl.BlockSpec(memory_space=pltpu.VMEM)] * len(parts),
        out_shape=jax.ShapeDtypeStruct((parts[0].shape[0], VAL), jnp.bfloat16),
        compiler_params=room(8),
        name="join",
    )(place, *parts)


def paired_body(
    hidden, queries, values, key_weight, decay_down, decay_up, decay_bias, span_shift, norm_gain
):
    seq_count, tok_count, model_width = hidden.shape
    dp_size = lax.axis_size("dp")
    place = lax.axis_index("sp").reshape(1)
    rank = lax.axis_index("dp").reshape(1)
    token_rows = hidden.reshape(tok_count, model_width)

    peer_rows = exchange(token_rows, "sp", 1)
    own_piece = take_columns(place, key_weight)
    pieces = {0: own_piece}
    for flip in range(2, dp_size, 2):
        pieces[flip] = exchange(own_piece, "dp", flip)
    parcels = make_parcels(
        place,
        token_rows,
        decay_down,
        queries.reshape(tok_count, KEY),
        values.reshape(tok_count, VAL),
        span_shift.reshape(1, tok_count),
    )
    parcels = [parcels[0]] + [exchange(parcels[flip], "sp", flip) for flip in range(1, HEADS)]
    for flip in range(0, dp_size, 2):
        pieces[flip + 1] = exchange(pieces[flip], "dp", 1)
    own, sent = project_keys(rank, token_rows, peer_rows, [pieces[i] for i in range(dp_size)])
    got = exchange(sent, "sp", 2)
    outs = mix_heads(place, decay_up, decay_bias, norm_gain, own, got, parcels)
    parts = [outs[0]] + [exchange(outs[flip], "sp", flip) for flip in range(1, HEADS)]
    return join_heads(place, parts).reshape(seq_count, tok_count, VAL)


def solution(mesh):
    in_specs = (
        P("dp", "sp", None),
        P("dp", "sp", None),
        P("dp", "sp", None),
        P("dp", None),
        P(),
        P(),
        P(),
        P("dp", "sp"),
        P(),
    )
    out_specs = P("dp", "sp", None)
    paired = mesh.shape["sp"] == HEADS and mesh.shape["dp"] % 2 == 0
    body = paired_body if paired else general_body

    return jax.shard_map(body, mesh=mesh, in_specs=in_specs, out_specs=out_specs, check_vma=False)
```

profile of v0, /device:TPU:0, one launch (start us, length us, event | category | flops | bytes accessed | tf_op | source)
XLA Modules:
  0.0 70.1 jit_solution(8438132084272665335)
XLA Ops:
  0.0 0.0 copy-start
  0.0 0.0 copy-start.1
  0.0 1.1 %copy-done.1 = bf16[256,1024]{1,0:T(8,128)(2,1)S(1)} copy-done((bf16[256,1024]{1,0:T(8,128)(2,1)S(1)}, bf16[256,1024]{1,0:T(8,128)(2,1)}, u32[]{:S(2)}) %copy-start.1) | copy-done | bytes 524312
  1.1 0.1 columns.1.refs_0_
  1.2 4.0 %collective-permute-start.6 = (bf16[256,512]{1,0:T(8,128)(2,1)S(1)}, bf16[256,512]{1,0:T(8,128)(2,1)S(1)}, u32[]{:S(2)}, u32[]{:S(2)}) collective-permute-start(bf16[256,512]{1,0:T(8,128)(2,1)S(1)} %columns.1.refs_0_), channel_id=1, source_target_pairs={{0,6},{1,7},{2,4},{3,5},{4,2},{5,3},{6,0},{7,1},{8,14},{9,15},{10,... | collective-permute-start | bytes 786440 | tf_op jit(solution)/shard_map/ppermute | solution.py:161
  5.2 0.5 collective-permute-start.4
  5.7 0.1 collective-permute-start.2
  5.8 0.0 copy-done
  5.8 2.0 %collective-permute-start = (bf16[128,2048]{1,0:T(8,128)(2,1)S(1)}, bf16[128,2048]{1,0:T(8,128)(2,1)S(1)}, u32[]{:S(2)}, u32[]{:S(2)}) collective-permute-start(bf16[128,2048]{1,0:T(8,128)(2,1)S(1)} %bitcast.9), channel_id=1, source_target_pairs={{0,8},{8,0},{16,24},{24,16},{1,9},{9,1},{17,25},{25,17},{2,10},{10... | collective-permute-start | bytes 1572872 | tf_op jit(solution)/shard_map/ppermute | solution.py:161
  7.8 0.0 collective-permute-start.1
  7.8 4.6 %collective-permute-done.6.refs_6_ = bf16[256,512]{1,0:T(8,128)(2,1)S(1)} collective-permute-done((bf16[256,512]{1,0:T(8,128)(2,1)S(1)}, bf16[256,512]{1,0:T(8,128)(2,1)S(1)}, u32[]{:S(2)}, u32[]{:S(2)}) %collective-permute-start.6) | collective-permute-done | bytes 262176 | tf_op jit(solution)/shard_map/ppermute | solution.py:161
  12.4 0.0 collective-permute-start.7
  12.4 4.7 %collective-permute-done.4.refs_4_ = bf16[256,512]{1,0:T(8,128)(2,1)S(1)} collective-permute-done((bf16[256,512]{1,0:T(8,128)(2,1)S(1)}, bf16[256,512]{1,0:T(8,128)(2,1)S(1)}, u32[]{:S(2)}, u32[]{:S(2)}) %collective-permute-start.4) | collective-permute-done | bytes 262176 | tf_op jit(solution)/shard_map/ppermute | solution.py:161
  17.1 0.0 collective-permute-start.5
  17.1 0.3 collective-permute-done.2.refs_2_
  17.4 0.2 collective-permute-start.3
  17.6 0.0 copy-done.3
  17.6 0.7 copy-done.8
  18.3 1.0 %copy-done.2 = bf16[1,128,2048]{2,1,0:T(8,128)(2,1)S(1)} copy-done((bf16[1,128,2048]{2,1,0:T(8,128)(2,1)S(1)}, bf16[1,128,2048]{2,1,0:T(8,128)(2,1)}, u32[]{:S(2)}) %copy-start.2) | copy-done | bytes 524312
  19.3 0.8 %copy-done.4 = bf16[2048,16]{0,1:T(8,128)(2,1)S(1)} copy-done((bf16[2048,16]{0,1:T(8,128)(2,1)S(1)}, bf16[2048,16]{0,1:T(8,128)(2,1)}, u32[]{:S(2)}) %copy-start.4) | copy-done | bytes 65560
  20.1 1.3 %parcels.1 = (bf16[136,768]{1,0:T(8,128)(2,1)S(1)}, bf16[136,768]{1,0:T(8,128)(2,1)}, bf16[136,768]{1,0:T(8,128)(2,1)}, bf16[136,768]{1,0:T(8,128)(2,1)}) custom-call(s32[1]{0:T(128)} %bitcast.place_ref, bf16[128,2048]{1,0:T(8,128)(2,1)S(1)} %bitcast.10, bf16[16,2048]{1,0:T(8,128)(2,1)S(1)} %bitcast.14, bf16[1,128]{1,0:T(2,128)(2,1)S(1)} %copy-done.8, ...), custom_call_target="tpu_custom_call" | custom-call | tf_op jit(solution)/shard_map/parcels/pallas_call | solution.py:242
  21.4 0.0 collective-permute-done.1.refs_1_
  21.4 1.8 %collective-permute-start.9 = (bf16[136,768]{1,0:T(8,128)(2,1)}, bf16[136,768]{1,0:T(8,128)(2,1)}, u32[]{:S(2)}, u32[]{:S(2)}) collective-permute-start(bf16[136,768]{1,0:T(8,128)(2,1)} %get-tuple-element.18), channel_id=1, source_target_pairs={{0,8},{8,0},{16,24},{24,16},{1,9},{9,1},{17,25},{25,17},{2,10},{10... | collective-permute-start | bytes 626696 | tf_op jit(solution)/shard_map/ppermute | solution.py:161
  23.3 0.0 collective-permute-done.7.refs_7_
  23.3 2.6 %collective-permute-start.10 = (bf16[136,768]{1,0:T(8,128)(2,1)}, bf16[136,768]{1,0:T(8,128)(2,1)}, u32[]{:S(2)}, u32[]{:S(2)}) collective-permute-start(bf16[136,768]{1,0:T(8,128)(2,1)} %get-tuple-element.19), channel_id=1, source_target_pairs={{0,16},{8,24},{16,0},{24,8},{1,17},{9,25},{17,1},{25,9},{2,18},{10... | collective-permute-start | bytes 626696 | tf_op jit(solution)/shard_map/ppermute | solution.py:161
  25.9 0.0 collective-permute-done.5.refs_5_
  25.9 0.0 collective-permute-start.11
  25.9 0.0 collective-permute-done.3.refs_3_
  25.9 0.0 collective-permute-done.peer_ref
  25.9 0.0 copy-start.7
  25.9 0.7 %keys.1 = (bf16[256,256]{1,0:T(8,128)(2,1)S(1)}, bf16[256,256]{1,0:T(8,128)(2,1)S(1)}) custom-call(s32[1]{0:T(128)} %bitcast.3.rank_ref, bf16[128,2048]{1,0:T(8,128)(2,1)S(1)} %bitcast.11, bf16[128,2048]{1,0:T(8,128)(2,1)S(1)} %collective-permute-done.peer_ref, bf16[256,512]{1,0:T(8,128)(2,1)S(1)} %columns.1.refs_0_, ...), custom_call_target="tpu_custom_call" | custom-call | tf_op jit(solution)/shard_map/keys/pallas_call | solution.py:272
  26.6 0.0 copy-start.6
  26.6 1.9 %collective-permute-start.8 = (bf16[256,256]{1,0:T(8,128)(2,1)S(1)}, bf16[256,256]{1,0:T(8,128)(2,1)S(1)}, u32[]{:S(2)}, u32[]{:S(2)}) collective-permute-start(bf16[256,256]{1,0:T(8,128)(2,1)S(1)} %get-tuple-element.16), channel_id=1, source_target_pairs={{0,16},{8,24},{16,0},{24,8},{1,17},{9,25},{17,1},{25,9},{2,18},{10... | collective-permute-start | bytes 393224 | tf_op jit(solution)/shard_map/ppermute | solution.py:161
  28.6 4.4 %collective-permute-done.9.p1 = bf16[136,768]{1,0:T(8,128)(2,1)} collective-permute-done((bf16[136,768]{1,0:T(8,128)(2,1)}, bf16[136,768]{1,0:T(8,128)(2,1)}, u32[]{:S(2)}, u32[]{:S(2)}) %collective-permute-start.9) | collective-permute-done | bytes 208928 | tf_op jit(solution)/shard_map/ppermute | solution.py:161
  33.0 11.3 %collective-permute-done.10.p2 = bf16[136,768]{1,0:T(8,128)(2,1)} collective-permute-done((bf16[136,768]{1,0:T(8,128)(2,1)}, bf16[136,768]{1,0:T(8,128)(2,1)}, u32[]{:S(2)}, u32[]{:S(2)}) %collective-permute-start.10) | collective-permute-done | bytes 208928 | tf_op jit(solution)/shard_map/ppermute | solution.py:161
  44.3 0.0 collective-permute-done.11.p3
  44.3 6.1 %collective-permute-done.8.got_ref = bf16[256,256]{1,0:T(8,128)(2,1)S(1)} collective-permute-done((bf16[256,256]{1,0:T(8,128)(2,1)S(1)}, bf16[256,256]{1,0:T(8,128)(2,1)S(1)}, u32[]{:S(2)}, u32[]{:S(2)}) %collective-permute-start.8) | collective-permute-done | bytes 131104 | tf_op jit(solution)/shard_map/ppermute | solution.py:161
  50.4 0.0 copy-done.5
  50.4 0.0 copy-done.7
  50.4 0.0 copy-done.6
  50.4 6.4 %mechanism.1 = (bf16[128,512]{1,0:T(8,128)(2,1)S(1)}, bf16[128,512]{1,0:T(8,128)(2,1)S(1)}, bf16[128,512]{1,0:T(8,128)(2,1)S(1)}, bf16[128,512]{1,0:T(8,128)(2,1)S(1)}) custom-call(s32[1]{0:T(128)} %bitcast.place_ref, f32[16,1024]{1,0:T(8,128)S(1)} %copy-done.5, f32[1,1024]{1,0:T(1,128)S(1)} %bitcast.16, f32[1,2048]{1,0:T(1,128)S(1)} %bitcast.15, ...), custom_call_target="tpu_custom_call" | custom-call | tf_op jit(solution)/shard_map/mechanism/pallas_call | solution.py:381
  56.8 0.1 collective-permute-start.12
  56.9 3.0 %collective-permute-start.13 = (bf16[128,512]{1,0:T(8,128)(2,1)S(1)}, bf16[128,512]{1,0:T(8,128)(2,1)S(1)}, u32[]{:S(2)}, u32[]{:S(2)}) collective-permute-start(bf16[128,512]{1,0:T(8,128)(2,1)S(1)} %get-tuple-element.23), channel_id=1, source_target_pairs={{0,16},{8,24},{16,0},{24,8},{1,17},{9,25},{17,1},{25,9},{2,18},{10... | collective-permute-start | bytes 393224 | tf_op jit(solution)/shard_map/ppermute | solution.py:161
  59.9 1.3 %collective-permute-start.14 = (bf16[128,512]{1,0:T(8,128)(2,1)S(1)}, bf16[128,512]{1,0:T(8,128)(2,1)S(1)}, u32[]{:S(2)}, u32[]{:S(2)}) collective-permute-start(bf16[128,512]{1,0:T(8,128)(2,1)S(1)} %get-tuple-element.24), channel_id=1, source_target_pairs={{0,24},{8,16},{16,8},{24,0},{1,25},{9,17},{17,9},{25,1},{2,26},{10... | collective-permute-start | bytes 393224 | tf_op jit(solution)/shard_map/ppermute | solution.py:161
  61.2 1.8 %collective-permute-done.12.refs_1_ = bf16[128,512]{1,0:T(8,128)(2,1)S(1)} collective-permute-done((bf16[128,512]{1,0:T(8,128)(2,1)S(1)}, bf16[128,512]{1,0:T(8,128)(2,1)S(1)}, u32[]{:S(2)}, u32[]{:S(2)}) %collective-permute-start.12) | collective-permute-done | bytes 131104 | tf_op jit(solution)/shard_map/ppermute | solution.py:161
  63.1 6.2 %collective-permute-done.13.refs_2_ = bf16[128,512]{1,0:T(8,128)(2,1)S(1)} collective-permute-done((bf16[128,512]{1,0:T(8,128)(2,1)S(1)}, bf16[128,512]{1,0:T(8,128)(2,1)S(1)}, u32[]{:S(2)}, u32[]{:S(2)}) %collective-permute-start.13) | collective-permute-done | bytes 131104 | tf_op jit(solution)/shard_map/ppermute | solution.py:161
  69.3 0.0 collective-permute-done.14.refs_3_
  69.3 0.8 %join.1 = bf16[128,2048]{1,0:T(8,128)(2,1)} custom-call(s32[1]{0:T(128)} %bitcast.place_ref, bf16[128,512]{1,0:T(8,128)(2,1)S(1)} %get-tuple-element.21.refs_0_, bf16[128,512]{1,0:T(8,128)(2,1)S(1)} %collective-permute-done.12.refs_1_, bf16[128,512]{1,0:T(8,128)(2,1)S(1)} %collective-permute-done.13.refs_2_, bf16[128,512]{1,0:T(8,128)(2,1)S(1)} %collective-permute-done.14.refs_3_), custom_call_target="tpu_custom_call" | custom-call | tf_op jit(solution)/shard_map/join/pallas_call | solution.py:425
  (5 shorter events, 0.0 us)
Async XLA Ops:
  0.0 5.8 %copy-start = (bf16[1,128,2048]{2,1,0:T(8,128)(2,1)S(1)}, bf16[1,128,2048]{2,1,0:T(8,128)(2,1)}, u32[]{:S(2)}) copy-start(bf16[1,128,2048]{2,1,0:T(8,128)(2,1)} %param.9) | copy-start | bytes 1572868
  0.0 1.1 %copy-start.1 = (bf16[256,1024]{1,0:T(8,128)(2,1)S(1)}, bf16[256,1024]{1,0:T(8,128)(2,1)}, u32[]{:S(2)}) copy-start(bf16[256,1024]{1,0:T(8,128)(2,1)} %weight_ref.1) | copy-start | bytes 1572868
  1.1 16.5 %copy-start.3 = (bf16[1,128,1024]{2,1,0:T(8,128)(2,1)S(1)}, bf16[1,128,1024]{2,1,0:T(8,128)(2,1)}, u32[]{:S(2)}) copy-start(bf16[1,128,1024]{2,1,0:T(8,128)(2,1)} %param.10) | copy-start | bytes 786436
  1.2 11.2 %collective-permute-start.6 = (bf16[256,512]{1,0:T(8,128)(2,1)S(1)}, bf16[256,512]{1,0:T(8,128)(2,1)S(1)}, u32[]{:S(2)}, u32[]{:S(2)}) collective-permute-start(bf16[256,512]{1,0:T(8,128)(2,1)S(1)} %columns.1.refs_0_), channel_id=1, source_target_pairs={{0,6},{1,7},{2,4},{3,5},{4,2},{5,3},{6,0},{7,1},{8,14},{9,15},{10,... | collective-permute-start | bytes 786440 | tf_op jit(solution)/shard_map/ppermute | solution.py:161
  5.2 11.9 %collective-permute-start.4 = (bf16[256,512]{1,0:T(8,128)(2,1)S(1)}, bf16[256,512]{1,0:T(8,128)(2,1)S(1)}, u32[]{:S(2)}, u32[]{:S(2)}) collective-permute-start(bf16[256,512]{1,0:T(8,128)(2,1)S(1)} %columns.1.refs_0_), channel_id=1, source_target_pairs={{0,4},{1,5},{2,6},{3,7},{4,0},{5,1},{6,2},{7,3},{8,12},{9,13},{10,... | collective-permute-start | bytes 786440 | tf_op jit(solution)/shard_map/ppermute | solution.py:161
  5.7 11.7 %collective-permute-start.2 = (bf16[256,512]{1,0:T(8,128)(2,1)S(1)}, bf16[256,512]{1,0:T(8,128)(2,1)S(1)}, u32[]{:S(2)}, u32[]{:S(2)}) collective-permute-start(bf16[256,512]{1,0:T(8,128)(2,1)S(1)} %columns.1.refs_0_), channel_id=1, source_target_pairs={{0,2},{1,3},{2,0},{3,1},{4,6},{5,7},{6,4},{7,5},{8,10},{9,11},{10,... | collective-permute-start | bytes 786440 | tf_op jit(solution)/shard_map/ppermute | solution.py:161
  5.8 20.1 %collective-permute-start = (bf16[128,2048]{1,0:T(8,128)(2,1)S(1)}, bf16[128,2048]{1,0:T(8,128)(2,1)S(1)}, u32[]{:S(2)}, u32[]{:S(2)}) collective-permute-start(bf16[128,2048]{1,0:T(8,128)(2,1)S(1)} %bitcast.9), channel_id=1, source_target_pairs={{0,8},{8,0},{16,24},{24,16},{1,9},{9,1},{17,25},{25,17},{2,10},{10... | collective-permute-start | bytes 1572872 | tf_op jit(solution)/shard_map/ppermute | solution.py:161
  7.8 13.6 %collective-permute-start.1 = (bf16[256,512]{1,0:T(8,128)(2,1)S(1)}, bf16[256,512]{1,0:T(8,128)(2,1)S(1)}, u32[]{:S(2)}, u32[]{:S(2)}) collective-permute-start(bf16[256,512]{1,0:T(8,128)(2,1)S(1)} %columns.1.refs_0_), channel_id=1, source_target_pairs={{0,1},{1,0},{2,3},{3,2},{4,5},{5,4},{6,7},{7,6},{8,9},{9,8},{10,11... | collective-permute-start | bytes 786440 | tf_op jit(solution)/shard_map/ppermute | solution.py:161
  12.4 10.9 %collective-permute-start.7 = (bf16[256,512]{1,0:T(8,128)(2,1)S(1)}, bf16[256,512]{1,0:T(8,128)(2,1)S(1)}, u32[]{:S(2)}, u32[]{:S(2)}) collective-permute-start(bf16[256,512]{1,0:T(8,128)(2,1)S(1)} %collective-permute-done.6.refs_6_), channel_id=1, source_target_pairs={{0,1},{1,0},{2,3},{3,2},{4,5},{5,4},{6,7},{7,6},{8,9},{9,8},{10,11... | collective-permute-start | bytes 786440 | tf_op jit(solution)/shard_map/ppermute | solution.py:161
  17.1 8.8 %collective-permute-start.5 = (bf16[256,512]{1,0:T(8,128)(2,1)S(1)}, bf16[256,512]{1,0:T(8,128)(2,1)S(1)}, u32[]{:S(2)}, u32[]{:S(2)}) collective-permute-start(bf16[256,512]{1,0:T(8,128)(2,1)S(1)} %collective-permute-done.4.refs_4_), channel_id=1, source_target_pairs={{0,1},{1,0},{2,3},{3,2},{4,5},{5,4},{6,7},{7,6},{8,9},{9,8},{10,11... | collective-permute-start | bytes 786440 | tf_op jit(solution)/shard_map/ppermute | solution.py:161
  17.4 8.5 %collective-permute-start.3 = (bf16[256,512]{1,0:T(8,128)(2,1)S(1)}, bf16[256,512]{1,0:T(8,128)(2,1)S(1)}, u32[]{:S(2)}, u32[]{:S(2)}) collective-permute-start(bf16[256,512]{1,0:T(8,128)(2,1)S(1)} %collective-permute-done.2.refs_2_), channel_id=1, source_target_pairs={{0,1},{1,0},{2,3},{3,2},{4,5},{5,4},{6,7},{7,6},{8,9},{9,8},{10,11... | collective-permute-start | bytes 786440 | tf_op jit(solution)/shard_map/ppermute | solution.py:161
  17.6 0.7 copy-start.8
  18.3 1.0 %copy-start.2 = (bf16[1,128,2048]{2,1,0:T(8,128)(2,1)S(1)}, bf16[1,128,2048]{2,1,0:T(8,128)(2,1)}, u32[]{:S(2)}) copy-start(bf16[1,128,2048]{2,1,0:T(8,128)(2,1)} %param.11) | copy-start | bytes 1572868
  19.3 0.8 %copy-start.4 = (bf16[2048,16]{0,1:T(8,128)(2,1)S(1)}, bf16[2048,16]{0,1:T(8,128)(2,1)}, u32[]{:S(2)}) copy-start(bf16[2048,16]{0,1:T(8,128)(2,1)} %param.13) | copy-start | bytes 196612
  21.4 11.6 %collective-permute-start.9 = (bf16[136,768]{1,0:T(8,128)(2,1)}, bf16[136,768]{1,0:T(8,128)(2,1)}, u32[]{:S(2)}, u32[]{:S(2)}) collective-permute-start(bf16[136,768]{1,0:T(8,128)(2,1)} %get-tuple-element.18), channel_id=1, source_target_pairs={{0,8},{8,0},{16,24},{24,16},{1,9},{9,1},{17,25},{25,17},{2,10},{10... | collective-permute-start | bytes 626696 | tf_op jit(solution)/shard_map/ppermute | solution.py:161
  23.3 21.0 %collective-permute-start.10 = (bf16[136,768]{1,0:T(8,128)(2,1)}, bf16[136,768]{1,0:T(8,128)(2,1)}, u32[]{:S(2)}, u32[]{:S(2)}) collective-permute-start(bf16[136,768]{1,0:T(8,128)(2,1)} %get-tuple-element.19), channel_id=1, source_target_pairs={{0,16},{8,24},{16,0},{24,8},{1,17},{9,25},{17,1},{25,9},{2,18},{10... | collective-permute-start | bytes 626696 | tf_op jit(solution)/shard_map/ppermute | solution.py:161
  25.9 18.4 %collective-permute-start.11 = (bf16[136,768]{1,0:T(8,128)(2,1)}, bf16[136,768]{1,0:T(8,128)(2,1)}, u32[]{:S(2)}, u32[]{:S(2)}) collective-permute-start(bf16[136,768]{1,0:T(8,128)(2,1)} %get-tuple-element.20), channel_id=1, source_target_pairs={{0,24},{8,16},{16,8},{24,0},{1,25},{9,17},{17,9},{25,1},{2,26},{10... | collective-permute-start | bytes 626696 | tf_op jit(solution)/shard_map/ppermute | solution.py:161
  25.9 24.5 %copy-start.5 = (f32[16,1024]{1,0:T(8,128)S(1)}, f32[16,1024]{1,0:T(8,128)}, u32[]{:S(2)}) copy-start(f32[16,1024]{1,0:T(8,128)} %up_ref.1) | copy-start | bytes 196612
  25.9 24.5 %copy-start.7 = (f32[1024]{0:T(1024)S(1)}, f32[1024]{0:T(1024)}, u32[]{:S(2)}) copy-start(f32[1024]{0:T(1024)} %param.15) | copy-start | bytes 12292
  26.6 23.7 %copy-start.6 = (f32[2048]{0:T(1024)S(1)}, f32[2048]{0:T(1024)}, u32[]{:S(2)}) copy-start(f32[2048]{0:T(1024)} %param.17) | copy-start | bytes 24580
  26.6 23.7 %collective-permute-start.8 = (bf16[256,256]{1,0:T(8,128)(2,1)S(1)}, bf16[256,256]{1,0:T(8,128)(2,1)S(1)}, u32[]{:S(2)}, u32[]{:S(2)}) collective-permute-start(bf16[256,256]{1,0:T(8,128)(2,1)S(1)} %get-tuple-element.16), channel_id=1, source_target_pairs={{0,16},{8,24},{16,0},{24,8},{1,17},{9,25},{17,1},{25,9},{2,18},{10... | collective-permute-start | bytes 393224 | tf_op jit(solution)/shard_map/ppermute | solution.py:161
  56.8 6.3 %collective-permute-start.12 = (bf16[128,512]{1,0:T(8,128)(2,1)S(1)}, bf16[128,512]{1,0:T(8,128)(2,1)S(1)}, u32[]{:S(2)}, u32[]{:S(2)}) collective-permute-start(bf16[128,512]{1,0:T(8,128)(2,1)S(1)} %get-tuple-element.22), channel_id=1, source_target_pairs={{0,8},{8,0},{16,24},{24,16},{1,9},{9,1},{17,25},{25,17},{2,10},{10... | collective-permute-start | bytes 393224 | tf_op jit(solution)/shard_map/ppermute | solution.py:161
  56.9 12.4 %collective-permute-start.13 = (bf16[128,512]{1,0:T(8,128)(2,1)S(1)}, bf16[128,512]{1,0:T(8,128)(2,1)S(1)}, u32[]{:S(2)}, u32[]{:S(2)}) collective-permute-start(bf16[128,512]{1,0:T(8,128)(2,1)S(1)} %get-tuple-element.23), channel_id=1, source_target_pairs={{0,16},{8,24},{16,0},{24,8},{1,17},{9,25},{17,1},{25,9},{2,18},{10... | collective-permute-start | bytes 393224 | tf_op jit(solution)/shard_map/ppermute | solution.py:161
  59.9 9.4 %collective-permute-start.14 = (bf16[128,512]{1,0:T(8,128)(2,1)S(1)}, bf16[128,512]{1,0:T(8,128)(2,1)S(1)}, u32[]{:S(2)}, u32[]{:S(2)}) collective-permute-start(bf16[128,512]{1,0:T(8,128)(2,1)S(1)} %get-tuple-element.24), channel_id=1, source_target_pairs={{0,24},{8,16},{16,8},{24,0},{1,25},{9,17},{17,9},{25,1},{2,26},{10... | collective-permute-start | bytes 393224 | tf_op jit(solution)/shard_map/ppermute | solution.py:161
where the time goes:
time: 70.4 us; the launch traced here: 70.1 us
  waiting for transfers between devices  39.4 us (56%)
  starting transfers between devices  17.7 us (25%)
  Pallas kernels  9.29 us (13%)
  local copies, waits for them, and re-layouts  3.66 us (5%)
    ppermute x15, waiting for transfers between devices, exchange(): return lax.ppermute(tensor, axis, [(i, i ^ flip) for i in range(size)])  39.4 us
    ppermute x15, starting transfers between devices, exchange(): return lax.ppermute(tensor, axis, [(i, i ^ flip) for i in range(size)])  17.7 us
    pallas_call x1, Pallas kernels, mix_heads(): pl.pallas_call(mechanism_kernel, grid_spec=pltpu.PrefetchScalarGridSpec(n...  6.42 us
    unnamed x18, local copies, waits for them, and re-layouts  3.66 us
  transfers between devices with their start and end apart: 15, of which 8 were waited for; matrix products, arithmetic and copies ran while one was open for 0% of the time, Pallas kernels for 3%

commit v1 on v0

--- a/solution.py
+++ b/solution.py
@@ -148,7 +148,6 @@
     return normed.reshape(seq_count, tok_count, VAL).astype(jnp.bfloat16)
 
 
-GROUP = 4 * BLOCK
 PACK = 8
 
 
@@ -206,7 +205,7 @@
         scratch_shapes=[pltpu.SemaphoreType.DMA((2,))],
         compiler_params=room(8),
         name="columns",
-    )(place, weight)
+    )(place, pltpu.with_memory_space_constraint(weight, pltpu.HBM))
 
 
 def parcels_kernel(place_ref, hidden_ref, down_ref, shift_ref, query_ref, value_ref, *refs):
@@ -249,7 +248,13 @@
         scratch_shapes=[pltpu.SemaphoreType.DMA((HEADS, 2))],
         compiler_params=room(8),
         name="parcels",
-    )(place, token_rows, decay_down.T, shift, queries, values)
+    )(
+        place,
+        token_rows,
+        decay_down.T,
+        shift,
+        *(pltpu.with_memory_space_constraint(a, pltpu.HBM) for a in (queries, values)),
+    )
 
 
 def keys_kernel(rank_ref, hidden_ref, peer_ref, *refs):
@@ -287,131 +292,265 @@
     return first, second, third
 
 
-def mechanism_kernel(
-    place_ref, up_ref, bias_ref, gain_ref, own_ref, got_ref, p0, p1, p2, p3, *refs
-):
-    outs, (query_s, value_s, key_s, low_s, mixed_s, fwd_s, bwd_s) = refs[:HEADS], refs[HEADS:]
-    place = place_ref[0]
-    tok_count = outs[0].shape[0]
-    length = query_s.shape[0]
-    rank = up_ref.shape[0]
-    for flip, parcel in enumerate((p0, p1, p2, p3)):
-        at = pl.ds(pl.multiple_of((place ^ flip) * tok_count, tok_count), tok_count)
-        query_s[at, :] = parcel[:tok_count, :DK]
-        value_s[at, :] = parcel[:tok_count, DK:]
-        keys = own_ref if flip < 2 else got_ref
-        key_s[at, :] = keys[pl.ds((flip % 2) * tok_count, tok_count), :]
-        low = parcel[tok_count:, :tok_count].astype(jnp.float32)
-        high = parcel[tok_count:, tok_count : 2 * tok_count].astype(jnp.float32)
-        shift = parcel[tok_count:, 2 * tok_count : 3 * tok_count].astype(jnp.float32)
+def in_blocks(tensor):
+    return [tensor[at : at + BLOCK] for at in range(0, tensor.shape[0], BLOCK)]
+
+
+def arrange(place, target, near, far, columns):
+    tok_count = target.shape[0] // 2
+    half = place & 1
+    for which, part in ((half, near), (1 - half, far)):
+        at = pl.ds(pl.multiple_of(which * tok_count, tok_count), tok_count)
+        target[at, :] = part[:tok_count, columns]
+
+
+def arrange_low(place, target, near, far):
+    tok_count = target.shape[1] // 2
+    half = place & 1
+    for which, part in ((half, near), (1 - half, far)):
+        low = part[tok_count:, :tok_count].astype(jnp.float32)
+        high = part[tok_count:, tok_count : 2 * tok_count].astype(jnp.float32)
+        shift = part[tok_count:, 2 * tok_count : 3 * tok_count].astype(jnp.float32)
         row = lax.broadcasted_iota(jnp.int32, shift.shape, 0)
         first = jnp.where(row == 0, shift, 0.0)
         stack = jnp.concatenate([low, high] * 3 + [first, jnp.zeros_like(first)], axis=0)
-        low_s[:, at] = stack.astype(jnp.bfloat16)
+        at = pl.ds(pl.multiple_of(which * tok_count, tok_count), tok_count)
+        target[:, at] = stack.astype(jnp.bfloat16)
+
+
+def decay_of(low, up, bias, sum_up_to):
+    pre = dot_tn(low, up) + bias
+    decay = (jnp.minimum(pre, 0.0) - jnp.log1p(jnp.exp(-jnp.abs(pre)))) * (1.0 / decay_tau)
+    inclusive = sum(dot_nn(sum_up_to, part) for part in split3(decay))
+    return decay, inclusive
+
+
+def scores_of(query_fwd, query_bwd, key_fwd, key_bwd, key_end, rates):
+    blocks = len(rates)
+    short = lambda tensors: [tensor.astype(jnp.bfloat16) for tensor in tensors]
+    key_fwd, near_bwd = short(key_fwd), short(key_bwd)
+    width = blocks * BLOCK
+    row = lax.broadcasted_iota(jnp.int32, (BLOCK, width), 0)
+    col = lax.broadcasted_iota(jnp.int32, (BLOCK, width), 1)
+    rows = []
+    for here in range(blocks):
+        left, right = list(key_fwd), list(near_bwd)
+        for past in range(here):
+            faded = key_end[past]
+            for between in range(past + 1, here):
+                faded = faded * rates[between]
+            left[past] = faded.astype(jnp.bfloat16)
+        fade = None
+        for later in range(here + 1, blocks):
+            fade = rates[later - 1] if fade is None else fade * rates[later - 1]
+            right[later] = (key_bwd[later] * fade).astype(jnp.bfloat16)
+        fwd = dot_nt(query_fwd[here], jnp.concatenate(left, axis=0))
+        bwd = dot_nt(query_bwd[here], jnp.concatenate(right, axis=0))
+        rows.append(jnp.where(col <= row + here * BLOCK, fwd, bwd).astype(jnp.bfloat16))
+    return jnp.concatenate(rows, axis=0)
+
+
+def factors(decay, inclusive, facing_right):
+    blocks = zip(in_blocks(decay), in_blocks(inclusive))
+    decay, inclusive = map(list, zip(*blocks))
+    totals = [tensor[BLOCK - 1 :] for tensor in inclusive]
+    none = jnp.zeros_like(totals[0])
+    right = jnp.where(facing_right, 1.0, 0.0)
+    found = []
+    for at in range(len(totals)):
+        exclusive = inclusive[at] - decay[at]
+        before = sum(totals[:at], none)
+        after = sum(totals[at:], none)
+        base = right * after + (1.0 - right) * before
+        sign = 1.0 - 2.0 * right
+        found.append(
+            dict(
+                query_fwd=jnp.exp(inclusive[at]),
+                query_bwd=jnp.exp(-exclusive),
+                key_fwd=jnp.exp(-inclusive[at]),
+                key_bwd=jnp.exp(exclusive),
+                key_end=jnp.exp(totals[at] - inclusive[at]),
+                key_edge=jnp.exp(base + sign * (exclusive + right * decay[at])),
+                query_edge=jnp.exp(base + sign * (inclusive[at] - right * decay[at])),
+                rate=jnp.exp(totals[at]),
+            )
+        )
+    return {name: [one[name] for one in found] for name in found[0]}
+
+
+def early_kernel(place_ref, up_ref, bias_ref, own_ref, p0, p1, p2, p3, *refs):
+    (
+        mixed_a,
+        mixed_b,
+        query_edge_a,
+        query_fwd_b,
+        query_bwd_b,
+        fwd_b,
+        bwd_b,
+        end_b,
+        edge_b,
+        rate_b,
+        query_s,
+        value_s,
+        key_s,
+        low_s,
+        far_query_s,
+        far_low_s,
+    ) = refs
+    place = place_ref[0]
+    rank = up_ref.shape[0]
+    size = mixed_a.shape[0]
+    at = pl.ds(pl.multiple_of(place * DK, DK), DK)
     ones = (lax.broadcasted_iota(jnp.int32, (rank, DK), 0) == 0).astype(jnp.float32)
     up = jnp.concatenate(
-        [part.astype(jnp.float32) for part in split3(up_ref[...])] + [ones], axis=0
+        [part.astype(jnp.float32) for part in split3(up_ref[:, at])] + [ones], axis=0
     ).astype(jnp.bfloat16)
-    pre = dot_tn(low_s[...], up) + bias_ref[...]
-    log_decay = (jnp.minimum(pre, 0.0) - jnp.log1p(jnp.exp(-jnp.abs(pre)))) * (1.0 / decay_tau)
-
-    row = lax.broadcasted_iota(jnp.int32, (GROUP, GROUP), 0)
-    col = lax.broadcasted_iota(jnp.int32, (GROUP, GROUP), 1)
-    same = (row // BLOCK) == (col // BLOCK)
-    lower = same & (col <= row)
-    upper = same & (col > row)
+    bias = bias_ref[:, at]
+    row = lax.broadcasted_iota(jnp.int32, (size, size), 0)
+    col = lax.broadcasted_iota(jnp.int32, (size, size), 1)
+    lower = ((row // BLOCK) == (col // BLOCK)) & (col <= row)
     sum_up_to = jnp.where(lower, 1.0, 0.0).astype(jnp.bfloat16)
-    steps = [[] for _ in range(5)]
-    rates = []
-    for start in range(0, length, GROUP):
-        decay = log_decay[start : start + GROUP]
-        inclusive = sum(dot_nn(sum_up_to, part) for part in split3(decay))
-        exclusive = inclusive - decay
-        by_block = inclusive.reshape(GROUP // BLOCK, BLOCK, DK)
-        total = by_block[:, BLOCK - 1 :, :]
-        scaled = query_s[start : start + GROUP, :].astype(jnp.float32) * DK**-0.5
-        keys = key_s[start : start + GROUP, :].astype(jnp.float32)
-        query_fwd = (scaled * jnp.exp(inclusive)).astype(jnp.bfloat16)
-        key_fwd = (keys * jnp.exp(-inclusive)).astype(jnp.bfloat16)
-        query_bwd = (scaled * jnp.exp(-exclusive)).astype(jnp.bfloat16)
-        key_bwd = (keys * jnp.exp(exclusive)).astype(jnp.bfloat16)
-        key_end = (keys * jnp.exp(total - by_block).reshape(GROUP, DK)).astype(jnp.bfloat16)
-        scores = jnp.where(
-            lower, dot_nt(query_fwd, key_fwd), jnp.where(upper, dot_nt(query_bwd, key_bwd), 0.0)
-        ).astype(jnp.bfloat16)
-        mixed_s[start : start + GROUP, :] = dot_nn(scores, value_s[start : start + GROUP, :])
-        for block in range(GROUP // BLOCK):
-            at = slice(block * BLOCK, (block + 1) * BLOCK)
-            for kept, tensor in zip(steps, (query_fwd, query_bwd, key_bwd, key_end)):
-                kept.append(tensor[at])
-            rates.append(jnp.exp(total[block]))
-    query_fwd, query_bwd, key_bwd, key_end = steps[:4]
-    blocks = length // BLOCK
-
-    def rows(block):
-        return slice(block * BLOCK, (block + 1) * BLOCK)
-
-    for block in range(1, blocks):
-        term = dot_tn(value_s[rows(block - 1), :], key_end[block - 1])
-        if block > 1:
-            term = term + fwd_s[...] * rates[block - 1]
-        fwd_s[...] = term
-        mixed_s[rows(block), :] += dot_nt(query_fwd[block], term.astype(jnp.bfloat16))
-        back = blocks - 1 - block
-        term = dot_tn(value_s[rows(back + 1), :], key_bwd[back + 1])
-        if block > 1:
-            term = term + bwd_s[...]
-        term = term * rates[back]
-        bwd_s[...] = term
-        mixed_s[rows(back), :] += dot_nt(query_bwd[back], term.astype(jnp.bfloat16))
-
-    for flip, out_ref in enumerate(outs):
-        at = pl.ds(pl.multiple_of((place ^ flip) * tok_count, tok_count), tok_count)
-        mixed = mixed_s[at, :].astype(jnp.bfloat16).astype(jnp.float32)
-        mean = jnp.mean(mixed * mixed, axis=-1, keepdims=True)
-        out_ref[...] = (mixed * lax.rsqrt(mean + norm_eps) * gain_ref[...]).astype(jnp.bfloat16)
+    first_pair = place < HEADS // 2
+    join = lambda tensors: jnp.concatenate(tensors, axis=0)
+    times = lambda left, right: [a * b for a, b in zip(left, right)]
+    short = lambda tensors: [tensor.astype(jnp.bfloat16) for tensor in tensors]
+
+    arrange_low(place, low_s, p0, p1)
+    arrange(place, query_s, p0, p1, slice(0, DK))
+    arrange(place, value_s, p0, p1, slice(DK, DK + DV))
+    arrange(place, key_s, own_ref.at[:size // 2], own_ref.at[size // 2 :], slice(0, DK))
+    found = factors(*decay_of(low_s[...], up, bias, sum_up_to), first_pair)
+    scaled = in_blocks(query_s[...].astype(jnp.float32) * DK**-0.5)
+    keys = in_blocks(key_s[...].astype(jnp.float32))
+    scores = scores_of(
+        short(times(scaled, found["query_fwd"])),
+        short(times(scaled, found["query_bwd"])),
+        times(keys, found["key_fwd"]),
+        times(keys, found["key_bwd"]),
+        times(keys, found["key_end"]),
+        found["rate"],
+    )
+    mixed_a[...] = dot_nn(scores, value_s[...])
+    query_edge_a[...] = join(short(times(scaled, found["query_edge"])))
+    key_edge = join(short(times(keys, found["key_edge"])))
+    state = dot_tn(key_edge, value_s[...]).astype(jnp.bfloat16)
+
+    arrange_low(place, far_low_s, p2, p3)
+    arrange(place, far_query_s, p2, p3, slice(0, DK))
+    found = factors(*decay_of(far_low_s[...], up, bias, sum_up_to), jnp.logical_not(first_pair))
+    scaled = in_blocks(far_query_s[...].astype(jnp.float32) * DK**-0.5)
+    query_fwd_b[...] = join(short(times(scaled, found["query_fwd"])))
+    query_bwd_b[...] = join(short(times(scaled, found["query_bwd"])))
+    mixed_b[...] = dot_nn(join(short(times(scaled, found["query_edge"]))), state)
+    fwd_b[...] = join(found["key_fwd"])
+    bwd_b[...] = join(found["key_bwd"])
+    end_b[...] = join(found["key_end"])
+    edge_b[...] = join(found["key_edge"])
+    for at, rate in enumerate(found["rate"]):
+        rate_b[at * PACK : (at + 1) * PACK, :] = jnp.broadcast_to(rate, (PACK, DK))
+
+
+def normed_of(mixed, gain):
+    mixed = mixed.astype(jnp.bfloat16).astype(jnp.float32)
+    mean = jnp.mean(mixed * mixed, axis=-1, keepdims=True)
+    return (mixed * lax.rsqrt(mean + norm_eps) * gain).astype(jnp.bfloat16)
+
+
+def write_halves(place, result_s, near_ref, far_ref):
+    tok_count = near_ref.shape[0]
+    half = place & 1
+    for which, out_ref in ((half, near_ref), (1 - half, far_ref)):
+        at = pl.ds(pl.multiple_of(which * tok_count, tok_count), tok_count)
+        out_ref[...] = result_s[at, :]
+
+
+def far_kernel(
+    place_ref, gain_ref, got_ref, p2, p3, mixed_b, query_fwd_b, query_bwd_b, fwd_b, bwd_b, end_b, rate_b,
+    near_ref, far_ref, value_s, key_s, result_s,
+):
+    place = place_ref[0]
+    size = mixed_b.shape[0]
+    arrange(place, value_s, p2, p3, slice(DK, DK + DV))
+    arrange(place, key_s, got_ref.at[:size // 2], got_ref.at[size // 2 :], slice(0, DK))
+    keys = key_s[...].astype(jnp.float32)
+    rates = [rate_b[at : at + 1, :] for at in range(0, rate_b.shape[0], PACK)]
+    scores = scores_of(
+        in_blocks(query_fwd_b[...]),
+        in_blocks(query_bwd_b[...]),
+        in_blocks(keys * fwd_b[...]),
+        in_blocks(keys * bwd_b[...]),
+        in_blocks(keys * end_b[...]),
+        rates,
+    )
+    mixed = mixed_b[...] + dot_nn(scores, value_s[...])
+    gain = gain_ref[:, pl.ds(pl.multiple_of(place * DV, DV), DV)]
+    result_s[...] = normed_of(mixed, gain)
+    write_halves(place, result_s, near_ref, far_ref)
+
+
+def near_kernel(
+    place_ref, gain_ref, got_ref, p2, p3, mixed_a, query_edge_a, edge_b,
+    near_ref, far_ref, value_s, key_s, result_s,
+):
+    place = place_ref[0]
+    size = mixed_a.shape[0]
+    arrange(place, value_s, p2, p3, slice(DK, DK + DV))
+    arrange(place, key_s, got_ref.at[:size // 2], got_ref.at[size // 2 :], slice(0, DK))
+    key_edge = (key_s[...].astype(jnp.float32) * edge_b[...]).astype(jnp.bfloat16)
+    state = dot_tn(key_edge, value_s[...]).astype(jnp.bfloat16)
+    mixed = mixed_a[...] + dot_nn(query_edge_a[...], state)
+    gain = gain_ref[:, pl.ds(pl.multiple_of(place * DV, DV), DV)]
+    result_s[...] = normed_of(mixed, gain)
+    write_halves(place, result_s, near_ref, far_ref)
+
+
+def on_chip(kernel, place, operands, shapes, scratch):
+    return pl.pallas_call(
+        kernel,
+        in_specs=[pl.BlockSpec(memory_space=pltpu.SMEM)]
+        + [pl.BlockSpec(memory_space=pltpu.VMEM)] * len(operands),
+        out_specs=[pl.BlockSpec(memory_space=pltpu.VMEM)] * len(shapes),
+        out_shape=[jax.ShapeDtypeStruct(*shape) for shape in shapes],
+        scratch_shapes=[pltpu.VMEM(*shape) for shape in scratch],
+        compiler_params=room(16),
+    )(place, *operands)
 
 
 def mix_heads(place, decay_up, decay_bias, norm_gain, own, got, parcels):
     tok_count = parcels[0].shape[0] - PACK
-    length = HEADS * tok_count
+    size = 2 * tok_count
     rank = decay_up.shape[0]
-    whole = lambda a: pl.BlockSpec(a.shape, lambda i, p: (0,) * a.ndim)
-    out = jax.ShapeDtypeStruct((tok_count, DV), jnp.bfloat16)
-    return pl.pallas_call(
-        mechanism_kernel,
-        grid_spec=pltpu.PrefetchScalarGridSpec(
-            num_scalar_prefetch=1,
-            grid=(1,),
-            in_specs=[
-                pl.BlockSpec((rank, DK), lambda i, p: (0, p[0])),
-                pl.BlockSpec((1, DK), lambda i, p: (0, p[0])),
-                pl.BlockSpec((1, DV), lambda i, p: (0, p[0])),
-            ]
-            + [whole(a) for a in (own, got, *parcels)],
-            out_specs=[whole(out)] * HEADS,
-            scratch_shapes=[
-                pltpu.VMEM((length, DK), jnp.bfloat16),
-                pltpu.VMEM((length, DV), jnp.bfloat16),
-                pltpu.VMEM((length, DK), jnp.bfloat16),
-                pltpu.VMEM((4 * rank, length), jnp.bfloat16),
-                pltpu.VMEM((length, DV), jnp.float32),
-                pltpu.VMEM((DV, DK), jnp.float32),
-                pltpu.VMEM((DV, DK), jnp.float32),
-            ],
-        ),
-        out_shape=[out] * HEADS,
-        compiler_params=room(24),
-        name="mechanism",
-    )(
+    short, wide = jnp.bfloat16, jnp.float32
+    query, value, mixed = ((size, DK), short), ((size, DV), short), ((size, DV), wide)
+    factor = ((size, DK), wide)
+    rates = ((size // BLOCK * PACK, DK), wide)
+    half = ((tok_count, DV), short)
+    (
+        mixed_a, mixed_b, query_edge_a, query_fwd_b, query_bwd_b, fwd_b, bwd_b, end_b, edge_b, rate_b,
+    ) = on_chip(
+        early_kernel,
         place,
-        decay_up,
-        decay_bias.reshape(1, -1),
-        norm_gain.reshape(1, -1),
-        own,
-        got,
-        *parcels,
-    )
+        (decay_up, decay_bias.reshape(1, -1), own, *parcels),
+        [mixed, mixed, query, query, query, factor, factor, factor, factor, rates],
+        [query, value, query, ((4 * rank, size), short), query, ((4 * rank, size), short)],
+    )
+    gain = norm_gain.reshape(1, -1)
+    scratch = [value, query, value]
+    far = on_chip(
+        far_kernel,
+        place,
+        (gain, got, *parcels[2:], mixed_b, query_fwd_b, query_bwd_b, fwd_b, bwd_b, end_b, rate_b),
+        [half, half],
+        scratch,
+    )
+    near = on_chip(
+        near_kernel,
+        place,
+        (gain, got, *parcels[2:], mixed_a, query_edge_a, edge_b),
+        [half, half],
+        scratch,
+    )
+    return [*near, *far]
 
 
 def join_kernel(place_ref, *refs):

time: 70.4 us -> 65.1 us (0.925)
  waiting for transfers between devices: 39.4 us -> 34.4 us
  local copies, waits for them, and re-layouts: 3.66 us -> 0.67 us
  starting transfers between devices: 17.7 us -> 19.1 us
  Pallas kernels: 9.29 us -> 10.6 us
    ppermute x15, waiting for transfers between devices: 39.4 us -> 34.4 us  [exchange(): return lax.ppermute(tensor, axis, [(i, i ^ flip) for i in range(size)])]
    unnamed x18 -> x12, local copies, waits for them, and re-layouts: 3.66 us -> 0.67 us
    pallas_call x1 -> x3, Pallas kernels: 6.42 us -> 4.86 us  [on_chip(): pl.pallas_call(kernel, in_specs=[pl.BlockSpec(memory_space=pltpu.SMEM)] +...]
    ppermute x15, starting transfers between devices: 17.7 us -> 19.1 us  [exchange(): return lax.ppermute(tensor, axis, [(i, i ^ flip) for i in range(size)])]
    pallas_call x1, Pallas kernels: 0.06 us -> 1.05 us  [take_columns(): pl.pallas_call(columns_kernel, in_specs=[pl.BlockSpec(memory_space=pltpu....]
    pallas_call x1, Pallas kernels: 0.72 us -> 1.69 us  [project_keys(): pl.pallas_call(keys_kernel, in_specs=[pl.BlockSpec(memory_space=pltpu.SME...]
    pallas_call x1, Pallas kernels: 1.27 us -> 2.16 us  [make_parcels(): pl.pallas_call(parcels_kernel, in_specs=[pl.BlockSpec(memory_space=pltpu....]
  transfers between devices with their start and end apart: 15 -> 15, of which waited for: 8 -> 7; matrix products, arithmetic and copies ran while one was open for 0% -> 0% of each run, Pallas kernels for 3% -> 12%
where the time goes in v1:
time: 65.1 us; the launch traced here: 64.9 us
  waiting for transfers between devices  34.4 us (53%)
  starting transfers between devices  19.1 us (29%)
  Pallas kernels  10.6 us (16%)
  local copies, waits for them, and re-layouts  0.67 us (1%)
    ppermute x15, waiting for transfers between devices, exchange(): return lax.ppermute(tensor, axis, [(i, i ^ flip) for i in range(size)])  34.4 us
    ppermute x15, starting transfers between devices, exchange(): return lax.ppermute(tensor, axis, [(i, i ^ flip) for i in range(size)])  19.1 us
    pallas_call x3, Pallas kernels, on_chip(): pl.pallas_call(kernel, in_specs=[pl.BlockSpec(memory_space=pltpu.SMEM)] +...  4.86 us
    pallas_call x1, Pallas kernels, make_parcels(): pl.pallas_call(parcels_kernel, in_specs=[pl.BlockSpec(memory_space=pltpu....  2.16 us
    pallas_call x1, Pallas kernels, project_keys(): pl.pallas_call(keys_kernel, in_specs=[pl.BlockSpec(memory_space=pltpu.SME...  1.69 us
  transfers between devices with their start and end apart: 15, of which 7 were waited for; matrix products, arithmetic and copies ran while one was open for 0% of the time, Pallas kernels for 12%

profile of v1, /device:TPU:0, one launch (start us, length us, event | category | flops | bytes accessed | tf_op | source)
XLA Modules:
  0.0 64.9 jit_solution(5741086908231411268)
XLA Ops:
  0.0 0.0 copy-start
  0.0 0.0 copy-start.1
  0.0 1.0 %columns.1.refs_0_ = bf16[256,512]{1,0:T(8,128)(2,1)S(1)} custom-call(s32[1]{0:T(128)} %bitcast.place_ref, bf16[256,1024]{1,0:T(8,128)(2,1)} %weight_ref.1), custom_call_target="tpu_custom_call" | custom-call | tf_op jit(solution)/shard_map/columns/pallas_call | solution.py:200
  1.1 4.0 %collective-permute-start.6 = (bf16[256,512]{1,0:T(8,128)(2,1)S(1)}, bf16[256,512]{1,0:T(8,128)(2,1)S(1)}, u32[]{:S(2)}, u32[]{:S(2)}) collective-permute-start(bf16[256,512]{1,0:T(8,128)(2,1)S(1)} %columns.1.refs_0_), channel_id=1, source_target_pairs={{0,6},{1,7},{2,4},{3,5},{4,2},{5,3},{6,0},{7,1},{8,14},{9,15},{10,... | collective-permute-start | bytes 786440 | tf_op jit(solution)/shard_map/ppermute | solution.py:160
  5.0 0.5 collective-permute-start.4
  5.6 0.1 collective-permute-start.2
  5.7 0.0 copy-done
  5.7 2.0 %collective-permute-start = (bf16[128,2048]{1,0:T(8,128)(2,1)S(1)}, bf16[128,2048]{1,0:T(8,128)(2,1)S(1)}, u32[]{:S(2)}, u32[]{:S(2)}) collective-permute-start(bf16[128,2048]{1,0:T(8,128)(2,1)S(1)} %bitcast.9), channel_id=1, source_target_pairs={{0,8},{8,0},{16,24},{24,16},{1,9},{9,1},{17,25},{25,17},{2,10},{10... | collective-permute-start | bytes 1572872 | tf_op jit(solution)/shard_map/ppermute | solution.py:160
  7.7 0.0 collective-permute-start.1
  7.7 4.6 %collective-permute-done.6.refs_6_ = bf16[256,512]{1,0:T(8,128)(2,1)S(1)} collective-permute-done((bf16[256,512]{1,0:T(8,128)(2,1)S(1)}, bf16[256,512]{1,0:T(8,128)(2,1)S(1)}, u32[]{:S(2)}, u32[]{:S(2)}) %collective-permute-start.6) | collective-permute-done | bytes 262176 | tf_op jit(solution)/shard_map/ppermute | solution.py:160
  12.2 0.0 collective-permute-start.7
  12.3 4.7 %collective-permute-done.4.refs_4_ = bf16[256,512]{1,0:T(8,128)(2,1)S(1)} collective-permute-done((bf16[256,512]{1,0:T(8,128)(2,1)S(1)}, bf16[256,512]{1,0:T(8,128)(2,1)S(1)}, u32[]{:S(2)}, u32[]{:S(2)}) %collective-permute-start.4) | collective-permute-done | bytes 262176 | tf_op jit(solution)/shard_map/ppermute | solution.py:160
  17.0 0.0 collective-permute-start.5
  17.0 0.3 collective-permute-done.2.refs_2_
  17.3 0.2 collective-permute-start.3
  17.5 0.0 copy-start.5
  17.5 0.0 copy-done.1
  17.5 0.7 %copy-done.5 = bf16[1,128]{1,0:T(2,128)(2,1)S(1)} copy-done((bf16[1,128]{1,0:T(2,128)(2,1)S(1)}, bf16[1,128]{1,0:T(2,128)(2,1)}, u32[]{:S(2)}) %copy-start.5) | copy-done | bytes 280
  18.1 2.2 %parcels.1 = (bf16[136,768]{1,0:T(8,128)(2,1)S(1)}, bf16[136,768]{1,0:T(8,128)(2,1)}, bf16[136,768]{1,0:T(8,128)(2,1)}, bf16[136,768]{1,0:T(8,128)(2,1)}) custom-call(s32[1]{0:T(128)} %bitcast.place_ref, bf16[128,2048]{1,0:T(8,128)(2,1)S(1)} %bitcast.10, bf16[16,2048]{1,0:T(8,128)(2,1)S(1)} %bitcast.12, bf16[1,128]{1,0:T(2,128)(2,1)S(1)} %copy-done.5, ...), custom_call_target="tpu_custom_call" | custom-call | tf_op jit(solution)/shard_map/parcels/pallas_call | solution.py:241
  20.3 0.0 collective-permute-done.1.refs_1_
  20.3 2.8 %collective-permute-start.9 = (bf16[136,768]{1,0:T(8,128)(2,1)}, bf16[136,768]{1,0:T(8,128)(2,1)S(1)}, u32[]{:S(2)}, u32[]{:S(2)}) collective-permute-start(bf16[136,768]{1,0:T(8,128)(2,1)} %get-tuple-element.26), channel_id=1, source_target_pairs={{0,16},{8,24},{16,0},{24,8},{1,17},{9,25},{17,1},{25,9},{2,18},{10... | collective-permute-start | bytes 626696 | tf_op jit(solution)/shard_map/ppermute | solution.py:160
  23.2 0.0 collective-permute-done.7.refs_7_
  23.2 1.3 %collective-permute-start.10 = (bf16[136,768]{1,0:T(8,128)(2,1)}, bf16[136,768]{1,0:T(8,128)(2,1)S(1)}, u32[]{:S(2)}, u32[]{:S(2)}) collective-permute-start(bf16[136,768]{1,0:T(8,128)(2,1)} %get-tuple-element.27), channel_id=1, source_target_pairs={{0,24},{8,16},{16,8},{24,0},{1,25},{9,17},{17,9},{25,1},{2,26},{10... | collective-permute-start | bytes 626696 | tf_op jit(solution)/shard_map/ppermute | solution.py:160
  24.5 0.0 collective-permute-done.5.refs_5_
  24.5 0.3 collective-permute-start.11
  24.8 0.0 collective-permute-done.3.refs_3_
  24.8 0.0 collective-permute-done.peer_ref
  24.8 0.0 copy-start.2
  24.8 1.7 %keys.1 = (bf16[256,256]{1,0:T(8,128)(2,1)S(1)}, bf16[256,256]{1,0:T(8,128)(2,1)S(1)}) custom-call(s32[1]{0:T(128)} %bitcast.2.rank_ref, bf16[128,2048]{1,0:T(8,128)(2,1)S(1)} %bitcast.11, bf16[128,2048]{1,0:T(8,128)(2,1)S(1)} %collective-permute-done.peer_ref, bf16[256,512]{1,0:T(8,128)(2,1)S(1)} %columns.1.refs_0_, ...), custom_call_target="tpu_custom_call" | custom-call | tf_op jit(solution)/shard_map/keys/pallas_call | solution.py:277
  26.5 0.0 copy-start.4
  26.6 2.8 %collective-permute-start.8 = (bf16[256,256]{1,0:T(8,128)(2,1)S(1)}, bf16[256,256]{1,0:T(8,128)(2,1)S(1)}, u32[]{:S(2)}, u32[]{:S(2)}) collective-permute-start(bf16[256,256]{1,0:T(8,128)(2,1)S(1)} %get-tuple-element.25), channel_id=1, source_target_pairs={{0,16},{8,24},{16,0},{24,8},{1,17},{9,25},{17,1},{25,9},{2,18},{10... | collective-permute-start | bytes 393224 | tf_op jit(solution)/shard_map/ppermute | solution.py:160
  29.4 9.7 %collective-permute-done.9.p2 = bf16[136,768]{1,0:T(8,128)(2,1)S(1)} collective-permute-done((bf16[136,768]{1,0:T(8,128)(2,1)}, bf16[136,768]{1,0:T(8,128)(2,1)S(1)}, u32[]{:S(2)}, u32[]{:S(2)}) %collective-permute-start.9) | collective-permute-done | bytes 208928 | tf_op jit(solution)/shard_map/ppermute | solution.py:160
  39.0 0.0 collective-permute-done.10.p3
  39.0 0.3 collective-permute-done.11.p1
  39.3 0.0 copy-done.2
  39.3 0.0 copy-done.4
  39.3 3.4 %shard_map.91 = (f32[256,512]{1,0:T(8,128)S(1)}, f32[256,512]{1,0:T(8,128)S(1)}, bf16[256,256]{1,0:T(8,128)(2,1)S(1)}, bf16[256,256]{1,0:T(8,128)(2,1)S(1)}, bf1...) custom-call(s32[1]{0:T(128)} %bitcast.place_ref, ...), custom_call_target="tpu_custom_call" | custom-call | tf_op jit(solution)/shard_map/pallas_call | solution.py:508
  42.7 5.2 %collective-permute-done.8.got_ref = bf16[256,256]{1,0:T(8,128)(2,1)S(1)} collective-permute-done((bf16[256,256]{1,0:T(8,128)(2,1)S(1)}, bf16[256,256]{1,0:T(8,128)(2,1)S(1)}, u32[]{:S(2)}, u32[]{:S(2)}) %collective-permute-start.8) | collective-permute-done | bytes 131104 | tf_op jit(solution)/shard_map/ppermute | solution.py:160
  48.0 0.0 copy-done.3
  48.0 0.7 %shard_map.92 = (bf16[128,512]{1,0:T(8,128)(2,1)S(1)}, bf16[128,512]{1,0:T(8,128)(2,1)S(1)}) custom-call(s32[1]{0:T(128)} %bitcast.place_ref, f32[1,2048]{1,0:T(1,128)S(1)} %bitcast.13, bf16[256,256]{1,0:T(8,128)(2,1)S(1)} %collective-permute-done.8.got_ref, bf16[136,768]{1,0:T(8,128)(2,1)S(1)} %collective-permute-done.9.p2, ...), custom_call_target="tpu_custom_call" | custom-call | tf_op jit(solution)/shard_map/pallas_call | solution.py:508
  48.6 1.9 %collective-permute-start.12 = (bf16[128,512]{1,0:T(8,128)(2,1)S(1)}, bf16[128,512]{1,0:T(8,128)(2,1)S(1)}, u32[]{:S(2)}, u32[]{:S(2)}) collective-permute-start(bf16[128,512]{1,0:T(8,128)(2,1)S(1)} %get-tuple-element.35), channel_id=1, source_target_pairs={{0,8},{8,0},{16,24},{24,16},{1,9},{9,1},{17,25},{25,17},{2,10},{10... | collective-permute-start | bytes 393224 | tf_op jit(solution)/shard_map/ppermute | solution.py:160
  50.6 0.8 %shard_map.93 = (bf16[128,512]{1,0:T(8,128)(2,1)S(1)}, bf16[128,512]{1,0:T(8,128)(2,1)S(1)}) custom-call(s32[1]{0:T(128)} %bitcast.place_ref, f32[1,2048]{1,0:T(1,128)S(1)} %bitcast.14, bf16[256,256]{1,0:T(8,128)(2,1)S(1)} %collective-permute-done.8.got_ref, bf16[136,768]{1,0:T(8,128)(2,1)S(1)} %collective-permute-done.9.p2, ...), custom_call_target="tpu_custom_call" | custom-call | tf_op jit(solution)/shard_map/pallas_call | solution.py:508
  51.4 2.2 %collective-permute-start.13 = (bf16[128,512]{1,0:T(8,128)(2,1)S(1)}, bf16[128,512]{1,0:T(8,128)(2,1)S(1)}, u32[]{:S(2)}, u32[]{:S(2)}) collective-permute-start(bf16[128,512]{1,0:T(8,128)(2,1)S(1)} %get-tuple-element.43), channel_id=1, source_target_pairs={{0,16},{8,24},{16,0},{24,8},{1,17},{9,25},{17,1},{25,9},{2,18},{10... | collective-permute-start | bytes 393224 | tf_op jit(solution)/shard_map/ppermute | solution.py:160
  53.6 0.8 %collective-permute-start.14 = (bf16[128,512]{1,0:T(8,128)(2,1)S(1)}, bf16[128,512]{1,0:T(8,128)(2,1)S(1)}, u32[]{:S(2)}, u32[]{:S(2)}) collective-permute-start(bf16[128,512]{1,0:T(8,128)(2,1)S(1)} %get-tuple-element.44), channel_id=1, source_target_pairs={{0,24},{8,16},{16,8},{24,0},{1,25},{9,17},{17,9},{25,1},{2,26},{10... | collective-permute-start | bytes 393224 | tf_op jit(solution)/shard_map/ppermute | solution.py:160
  54.4 0.0 collective-permute-done.12.refs_1_
  54.4 9.7 %collective-permute-done.13.refs_2_ = bf16[128,512]{1,0:T(8,128)(2,1)S(1)} collective-permute-done((bf16[128,512]{1,0:T(8,128)(2,1)S(1)}, bf16[128,512]{1,0:T(8,128)(2,1)S(1)}, u32[]{:S(2)}, u32[]{:S(2)}) %collective-permute-start.13) | collective-permute-done | bytes 131104 | tf_op jit(solution)/shard_map/ppermute | solution.py:160
  64.1 0.0 collective-permute-done.14.refs_3_
  64.1 0.8 %join.1 = bf16[128,2048]{1,0:T(8,128)(2,1)} custom-call(s32[1]{0:T(128)} %bitcast.place_ref, bf16[128,512]{1,0:T(8,128)(2,1)S(1)} %get-tuple-element.34.refs_0_, bf16[128,512]{1,0:T(8,128)(2,1)S(1)} %collective-permute-done.12.refs_1_, bf16[128,512]{1,0:T(8,128)(2,1)S(1)} %collective-permute-done.13.refs_2_, bf16[128,512]{1,0:T(8,128)(2,1)S(1)} %collective-permute-done.14.refs_3_), custom_call_target="tpu_custom_call" | custom-call | tf_op jit(solution)/shard_map/join/pallas_call | solution.py:564
  (1 shorter events, 0.0 us)
Async XLA Ops:
  0.0 5.7 %copy-start = (bf16[1,128,2048]{2,1,0:T(8,128)(2,1)S(1)}, bf16[1,128,2048]{2,1,0:T(8,128)(2,1)}, u32[]{:S(2)}) copy-start(bf16[1,128,2048]{2,1,0:T(8,128)(2,1)} %param.9) | copy-start | bytes 1572868
  0.0 17.5 %copy-start.1 = (bf16[2048,16]{0,1:T(8,128)(2,1)S(1)}, bf16[2048,16]{0,1:T(8,128)(2,1)}, u32[]{:S(2)}) copy-start(bf16[2048,16]{0,1:T(8,128)(2,1)} %param.13) | copy-start | bytes 196612
  1.1 11.2 %collective-permute-start.6 = (bf16[256,512]{1,0:T(8,128)(2,1)S(1)}, bf16[256,512]{1,0:T(8,128)(2,1)S(1)}, u32[]{:S(2)}, u32[]{:S(2)}) collective-permute-start(bf16[256,512]{1,0:T(8,128)(2,1)S(1)} %columns.1.refs_0_), channel_id=1, source_target_pairs={{0,6},{1,7},{2,4},{3,5},{4,2},{5,3},{6,0},{7,1},{8,14},{9,15},{10,... | collective-permute-start | bytes 786440 | tf_op jit(solution)/shard_map/ppermute | solution.py:160
  5.0 11.9 %collective-permute-start.4 = (bf16[256,512]{1,0:T(8,128)(2,1)S(1)}, bf16[256,512]{1,0:T(8,128)(2,1)S(1)}, u32[]{:S(2)}, u32[]{:S(2)}) collective-permute-start(bf16[256,512]{1,0:T(8,128)(2,1)S(1)} %columns.1.refs_0_), channel_id=1, source_target_pairs={{0,4},{1,5},{2,6},{3,7},{4,0},{5,1},{6,2},{7,3},{8,12},{9,13},{10,... | collective-permute-start | bytes 786440 | tf_op jit(solution)/shard_map/ppermute | solution.py:160
  5.6 11.7 %collective-permute-start.2 = (bf16[256,512]{1,0:T(8,128)(2,1)S(1)}, bf16[256,512]{1,0:T(8,128)(2,1)S(1)}, u32[]{:S(2)}, u32[]{:S(2)}) collective-permute-start(bf16[256,512]{1,0:T(8,128)(2,1)S(1)} %columns.1.refs_0_), channel_id=1, source_target_pairs={{0,2},{1,3},{2,0},{3,1},{4,6},{5,7},{6,4},{7,5},{8,10},{9,11},{10,... | collective-permute-start | bytes 786440 | tf_op jit(solution)/shard_map/ppermute | solution.py:160
  5.7 19.1 %collective-permute-start = (bf16[128,2048]{1,0:T(8,128)(2,1)S(1)}, bf16[128,2048]{1,0:T(8,128)(2,1)S(1)}, u32[]{:S(2)}, u32[]{:S(2)}) collective-permute-start(bf16[128,2048]{1,0:T(8,128)(2,1)S(1)} %bitcast.9), channel_id=1, source_target_pairs={{0,8},{8,0},{16,24},{24,16},{1,9},{9,1},{17,25},{25,17},{2,10},{10... | collective-permute-start | bytes 1572872 | tf_op jit(solution)/shard_map/ppermute | solution.py:160
  7.7 12.6 %collective-permute-start.1 = (bf16[256,512]{1,0:T(8,128)(2,1)S(1)}, bf16[256,512]{1,0:T(8,128)(2,1)S(1)}, u32[]{:S(2)}, u32[]{:S(2)}) collective-permute-start(bf16[256,512]{1,0:T(8,128)(2,1)S(1)} %columns.1.refs_0_), channel_id=1, source_target_pairs={{0,1},{1,0},{2,3},{3,2},{4,5},{5,4},{6,7},{7,6},{8,9},{9,8},{10,11... | collective-permute-start | bytes 786440 | tf_op jit(solution)/shard_map/ppermute | solution.py:160
  12.2 10.9 %collective-permute-start.7 = (bf16[256,512]{1,0:T(8,128)(2,1)S(1)}, bf16[256,512]{1,0:T(8,128)(2,1)S(1)}, u32[]{:S(2)}, u32[]{:S(2)}) collective-permute-start(bf16[256,512]{1,0:T(8,128)(2,1)S(1)} %collective-permute-done.6.refs_6_), channel_id=1, source_target_pairs={{0,1},{1,0},{2,3},{3,2},{4,5},{5,4},{6,7},{7,6},{8,9},{9,8},{10,11... | collective-permute-start | bytes 786440 | tf_op jit(solution)/shard_map/ppermute | solution.py:160
  17.0 7.6 %collective-permute-start.5 = (bf16[256,512]{1,0:T(8,128)(2,1)S(1)}, bf16[256,512]{1,0:T(8,128)(2,1)S(1)}, u32[]{:S(2)}, u32[]{:S(2)}) collective-permute-start(bf16[256,512]{1,0:T(8,128)(2,1)S(1)} %collective-permute-done.4.refs_4_), channel_id=1, source_target_pairs={{0,1},{1,0},{2,3},{3,2},{4,5},{5,4},{6,7},{7,6},{8,9},{9,8},{10,11... | collective-permute-start | bytes 786440 | tf_op jit(solution)/shard_map/ppermute | solution.py:160
  17.3 7.6 %collective-permute-start.3 = (bf16[256,512]{1,0:T(8,128)(2,1)S(1)}, bf16[256,512]{1,0:T(8,128)(2,1)}, u32[]{:S(2)}, u32[]{:S(2)}) collective-permute-start(bf16[256,512]{1,0:T(8,128)(2,1)S(1)} %collective-permute-done.2.refs_2_), channel_id=1, source_target_pairs={{0,1},{1,0},{2,3},{3,2},{4,5},{5,4},{6,7},{7,6},{8,9},{9,8},{10,11... | collective-permute-start | bytes 786440 | tf_op jit(solution)/shard_map/ppermute | solution.py:160
  17.5 0.7 %copy-start.5 = (bf16[1,128]{1,0:T(2,128)(2,1)S(1)}, bf16[1,128]{1,0:T(2,128)(2,1)}, u32[]{:S(2)}) copy-start(bf16[1,128]{1,0:T(2,128)(2,1)} %shift_ref.1) | copy-start | bytes 772
  20.3 18.7 %collective-permute-start.9 = (bf16[136,768]{1,0:T(8,128)(2,1)}, bf16[136,768]{1,0:T(8,128)(2,1)S(1)}, u32[]{:S(2)}, u32[]{:S(2)}) collective-permute-start(bf16[136,768]{1,0:T(8,128)(2,1)} %get-tuple-element.26), channel_id=1, source_target_pairs={{0,16},{8,24},{16,0},{24,8},{1,17},{9,25},{17,1},{25,9},{2,18},{10... | collective-permute-start | bytes 626696 | tf_op jit(solution)/shard_map/ppermute | solution.py:160
  23.2 15.9 %collective-permute-start.10 = (bf16[136,768]{1,0:T(8,128)(2,1)}, bf16[136,768]{1,0:T(8,128)(2,1)S(1)}, u32[]{:S(2)}, u32[]{:S(2)}) collective-permute-start(bf16[136,768]{1,0:T(8,128)(2,1)} %get-tuple-element.27), channel_id=1, source_target_pairs={{0,24},{8,16},{16,8},{24,0},{1,25},{9,17},{17,9},{25,1},{2,26},{10... | collective-permute-start | bytes 626696 | tf_op jit(solution)/shard_map/ppermute | solution.py:160
  24.5 14.8 %collective-permute-start.11 = (bf16[136,768]{1,0:T(8,128)(2,1)}, bf16[136,768]{1,0:T(8,128)(2,1)}, u32[]{:S(2)}, u32[]{:S(2)}) collective-permute-start(bf16[136,768]{1,0:T(8,128)(2,1)} %get-tuple-element.30), channel_id=1, source_target_pairs={{0,8},{8,0},{16,24},{24,16},{1,9},{9,1},{17,25},{25,17},{2,10},{10... | collective-permute-start | bytes 626696 | tf_op jit(solution)/shard_map/ppermute | solution.py:160
  24.8 14.5 %copy-start.2 = (f32[16,1024]{1,0:T(8,128)S(1)}, f32[16,1024]{1,0:T(8,128)}, u32[]{:S(2)}) copy-start(f32[16,1024]{1,0:T(8,128)} %up_ref.1) | copy-start | bytes 196612
  26.5 12.8 %copy-start.4 = (f32[1024]{0:T(1024)S(1)}, f32[1024]{0:T(1024)}, u32[]{:S(2)}) copy-start(f32[1024]{0:T(1024)} %param.15) | copy-start | bytes 12292
  26.6 21.4 %collective-permute-start.8 = (bf16[256,256]{1,0:T(8,128)(2,1)S(1)}, bf16[256,256]{1,0:T(8,128)(2,1)S(1)}, u32[]{:S(2)}, u32[]{:S(2)}) collective-permute-start(bf16[256,256]{1,0:T(8,128)(2,1)S(1)} %get-tuple-element.25), channel_id=1, source_target_pairs={{0,16},{8,24},{16,0},{24,8},{1,17},{9,25},{17,1},{25,9},{2,18},{10... | collective-permute-start | bytes 393224 | tf_op jit(solution)/shard_map/ppermute | solution.py:160
  39.3 8.6 %copy-start.3 = (f32[2048]{0:T(1024)S(1)}, f32[2048]{0:T(1024)}, u32[]{:S(2)}) copy-start(f32[2048]{0:T(1024)} %param.17) | copy-start | bytes 24580
  48.6 5.8 %collective-permute-start.12 = (bf16[128,512]{1,0:T(8,128)(2,1)S(1)}, bf16[128,512]{1,0:T(8,128)(2,1)S(1)}, u32[]{:S(2)}, u32[]{:S(2)}) collective-permute-start(bf16[128,512]{1,0:T(8,128)(2,1)S(1)} %get-tuple-element.35), channel_id=1, source_target_pairs={{0,8},{8,0},{16,24},{24,16},{1,9},{9,1},{17,25},{25,17},{2,10},{10... | collective-permute-start | bytes 393224 | tf_op jit(solution)/shard_map/ppermute | solution.py:160
  51.4 12.7 %collective-permute-start.13 = (bf16[128,512]{1,0:T(8,128)(2,1)S(1)}, bf16[128,512]{1,0:T(8,128)(2,1)S(1)}, u32[]{:S(2)}, u32[]{:S(2)}) collective-permute-start(bf16[128,512]{1,0:T(8,128)(2,1)S(1)} %get-tuple-element.43), channel_id=1, source_target_pairs={{0,16},{8,24},{16,0},{24,8},{1,17},{9,25},{17,1},{25,9},{2,18},{10... | collective-permute-start | bytes 393224 | tf_op jit(solution)/shard_map/ppermute | solution.py:160
  53.6 10.4 %collective-permute-start.14 = (bf16[128,512]{1,0:T(8,128)(2,1)S(1)}, bf16[128,512]{1,0:T(8,128)(2,1)S(1)}, u32[]{:S(2)}, u32[]{:S(2)}) collective-permute-start(bf16[128,512]{1,0:T(8,128)(2,1)S(1)} %get-tuple-element.44), channel_id=1, source_target_pairs={{0,24},{8,16},{16,8},{24,0},{1,25},{9,17},{17,9},{25,1},{2,26},{10... | collective-permute-start | bytes 393224 | tf_op jit(solution)/shard_map/ppermute | solution.py:160

commit v2 on v1

--- a/solution.py
+++ b/solution.py
@@ -155,6 +155,10 @@
     return pltpu.CompilerParams(vmem_limit_bytes=mebibytes * 2**20)
 
 
+def inner(tensors):
+    return [pltpu.with_memory_space_constraint(tensor, pltpu.VMEM) for tensor in tensors]
+
+
 def exchange(tensor, axis, flip):
     size = lax.axis_size(axis)
     return lax.ppermute(tensor, axis, [(i, i ^ flip) for i in range(size)])
@@ -178,83 +182,74 @@
     )
 
 
-def columns_kernel(place_ref, weight_ref, out_ref, sems):
-    copies = []
-    for half in range(2):
-        at = pl.multiple_of((place_ref[0] ^ (2 * half)) * DK, DK)
-        copies.append(
-            pltpu.make_async_copy(
-                weight_ref.at[:, pl.ds(at, DK)],
-                out_ref.at[:, pl.ds(half * DK, DK)],
-                sems.at[half],
-            )
-        )
-    for copy in copies:
-        copy.start()
-    for copy in copies:
-        copy.wait()
-
-
-def take_columns(place, weight):
-    rows = weight.shape[0]
-    return pl.pallas_call(
-        columns_kernel,
-        in_specs=[pl.BlockSpec(memory_space=pltpu.SMEM), pl.BlockSpec(memory_space=pl.ANY)],
-        out_specs=pl.BlockSpec(memory_space=pltpu.VMEM),
-        out_shape=jax.ShapeDtypeStruct((rows, 2 * DK), weight.dtype),
-        scratch_shapes=[pltpu.SemaphoreType.DMA((2,))],
-        compiler_params=room(8),
-        name="columns",
-    )(place, pltpu.with_memory_space_constraint(weight, pltpu.HBM))
-
-
-def parcels_kernel(place_ref, hidden_ref, down_ref, shift_ref, query_ref, value_ref, *refs):
-    out_refs, sems = refs[:HEADS], refs[HEADS]
+def prepare_kernel(
+    place_ref, rank_ref, down_ref, shift_ref, up_ref, bias_ref, gain_ref, weight_ref, hidden_ref, query_ref,
+    value_ref, piece_ref, hidden_out, up_out, bias_out, gain_out, p0, p1, p2, p3, down_s, shift_s, sems,
+):
+    parcels = (p0, p1, p2, p3)
+    place = place_ref[0]
     tok_count = query_ref.shape[0]
     copies = []
-    for flip, out_ref in enumerate(out_refs):
-        head = place_ref[0] ^ flip
-        for which, (source, width, at) in enumerate(((query_ref, DK, 0), (value_ref, DV, DK))):
-            copies.append(
-                pltpu.make_async_copy(
-                    source.at[:, pl.ds(pl.multiple_of(head * width, width), width)],
-                    out_ref.at[pl.ds(0, tok_count), pl.ds(at, width)],
-                    sems.at[flip, which],
-                )
-            )
-    for copy in copies:
-        copy.start()
-    low = dot_nt(down_ref[...], hidden_ref[...]).astype(jnp.bfloat16)
-    shift = jnp.broadcast_to(shift_ref[...].astype(jnp.float32), (PACK, tok_count))
+
+    def fetch(source, target, head=None, width=None):
+        if width is not None:
+            source = source.at[:, pl.ds(pl.multiple_of(head * width, width), width)]
+        copies.append(pltpu.make_async_copy(source, target, sems.at[len(copies)]))
+        copies[-1].start()
+
+    fetch(hidden_ref, hidden_out)
+    fetch(down_ref, down_s)
+    fetch(shift_ref, shift_s)
+    for half in range(2):
+        fetch(weight_ref, piece_ref.at[:, pl.ds(half * DK, DK)], place ^ (2 * half), DK)
+    for flip in (2, 3, 1, 0):
+        rows = parcels[flip].at[pl.ds(0, tok_count), :]
+        fetch(query_ref, rows.at[:, pl.ds(0, DK)], place ^ flip, DK)
+        fetch(value_ref, rows.at[:, pl.ds(DK, DV)], place ^ flip, DV)
+    fetch(up_ref, up_out, place, DK)
+    fetch(bias_ref, bias_out, place, DK)
+    fetch(gain_ref, gain_out, place, DV)
+    for copy in copies[:3]:
+        copy.wait()
+    low = dot_nt(down_s[...], hidden_out[...]).astype(jnp.bfloat16).astype(jnp.float32)
+    shift = jnp.broadcast_to(shift_s[...].astype(jnp.float32), (PACK, tok_count))
     empty = jnp.zeros((PACK, DK + DV - 3 * tok_count), jnp.float32)
-    low = low.astype(jnp.float32)
     tail = jnp.concatenate([low[:PACK], low[PACK:], shift, empty], axis=1).astype(jnp.bfloat16)
-    for out_ref in out_refs:
-        out_ref[tok_count:, :] = tail
-    for copy in copies:
+    for parcel in parcels:
+        parcel[tok_count:, :] = tail
+    for copy in copies[3:]:
         copy.wait()
 
 
-def make_parcels(place, token_rows, decay_down, queries, values, shift):
-    tok_count = token_rows.shape[0]
-    shape = jax.ShapeDtypeStruct((tok_count + PACK, DK + DV), jnp.bfloat16)
+def prepare(place, rank, token_rows, small, key_weight, queries, values):
+    tok_count, rows = token_rows.shape[0], key_weight.shape[0]
+    down, shift, up, bias, gain = small
+    outer = [
+        pltpu.with_memory_space_constraint(a, pltpu.HBM)
+        for a in (down, shift, up, bias, gain, key_weight, token_rows, queries, values)
+    ]
+    parcel = jax.ShapeDtypeStruct((tok_count + PACK, DK + DV), jnp.bfloat16)
+    shapes = [
+        jax.ShapeDtypeStruct((rows, 2 * DK), jnp.bfloat16),
+        jax.ShapeDtypeStruct(token_rows.shape, jnp.bfloat16),
+        jax.ShapeDtypeStruct((up.shape[0], DK), jnp.float32),
+        jax.ShapeDtypeStruct((1, DK), jnp.float32),
+        jax.ShapeDtypeStruct((1, DV), jnp.float32),
+    ]
     return pl.pallas_call(
-        parcels_kernel,
-        in_specs=[pl.BlockSpec(memory_space=pltpu.SMEM)]
-        + [pl.BlockSpec(memory_space=pltpu.VMEM)] * 3
-        + [pl.BlockSpec(memory_space=pl.ANY)] * 2,
-        out_specs=[pl.BlockSpec(memory_space=pltpu.VMEM)] * HEADS,
-        out_shape=[shape] * HEADS,
-        scratch_shapes=[pltpu.SemaphoreType.DMA((HEADS, 2))],
+        prepare_kernel,
+        in_specs=[pl.BlockSpec(memory_space=pltpu.SMEM)] * 2
+        + [pl.BlockSpec(memory_space=pl.ANY)] * len(outer),
+        out_specs=[pl.BlockSpec(memory_space=pltpu.VMEM)] * (len(shapes) + HEADS),
+        out_shape=[pltpu.VMEM(a.shape, a.dtype) for a in shapes + [parcel] * HEADS],
+        scratch_shapes=[
+            pltpu.VMEM(down.shape, down.dtype),
+            pltpu.VMEM(shift.shape, shift.dtype),
+            pltpu.SemaphoreType.DMA((8 + 2 * HEADS,)),
+        ],
         compiler_params=room(8),
-        name="parcels",
-    )(
-        place,
-        token_rows,
-        decay_down.T,
-        shift,
-        *(pltpu.with_memory_space_constraint(a, pltpu.HBM) for a in (queries, values)),
-    )
+        name="prepare",
+    )(place, rank, *outer)
 
 
 def keys_kernel(rank_ref, hidden_ref, peer_ref, *refs):
@@ -281,7 +276,7 @@
         out_shape=[shape, shape],
         compiler_params=room(12),
         name="keys",
-    )(rank, token_rows, peer_rows, *pieces)
+    )(rank, *inner((token_rows, peer_rows, *pieces)))
 
 
 def split3(tensor):
@@ -296,26 +291,34 @@
     return [tensor[at : at + BLOCK] for at in range(0, tensor.shape[0], BLOCK)]
 
 
-def arrange(place, target, near, far, columns):
+def arrange(place, target, near, far):
     tok_count = target.shape[0] // 2
     half = place & 1
     for which, part in ((half, near), (1 - half, far)):
         at = pl.ds(pl.multiple_of(which * tok_count, tok_count), tok_count)
-        target[at, :] = part[:tok_count, columns]
-
-
-def arrange_low(place, target, near, far):
-    tok_count = target.shape[1] // 2
-    half = place & 1
-    for which, part in ((half, near), (1 - half, far)):
-        low = part[tok_count:, :tok_count].astype(jnp.float32)
-        high = part[tok_count:, tok_count : 2 * tok_count].astype(jnp.float32)
-        shift = part[tok_count:, 2 * tok_count : 3 * tok_count].astype(jnp.float32)
+        target[at, :] = part[...]
+
+
+def query_of(parcel):
+    return parcel.at[: parcel.shape[0] - PACK, :DK]
+
+
+def value_of(parcel):
+    return parcel.at[: parcel.shape[0] - PACK, DK:]
+
+
+def arrange_low(place, near, far):
+    tok_count = near.shape[0] - PACK
+    near, far = (part[tok_count:, :].astype(jnp.float32) for part in (near, far))
+    odd = (place & 1) == 1
+    halves = []
+    for part in (jnp.where(odd, far, near), jnp.where(odd, near, far)):
+        low = [part[:, :tok_count], part[:, tok_count : 2 * tok_count]]
+        shift = part[:, 2 * tok_count : 3 * tok_count]
         row = lax.broadcasted_iota(jnp.int32, shift.shape, 0)
         first = jnp.where(row == 0, shift, 0.0)
-        stack = jnp.concatenate([low, high] * 3 + [first, jnp.zeros_like(first)], axis=0)
-        at = pl.ds(pl.multiple_of(which * tok_count, tok_count), tok_count)
-        target[:, at] = stack.astype(jnp.bfloat16)
+        halves.append(jnp.concatenate(low * 3 + [first, jnp.zeros_like(first)], axis=0))
+    return jnp.concatenate(halves, axis=1).astype(jnp.bfloat16)
 
 
 def decay_of(low, up, bias, sum_up_to):
@@ -378,48 +381,42 @@
     return {name: [one[name] for one in found] for name in found[0]}
 
 
-def early_kernel(place_ref, up_ref, bias_ref, own_ref, p0, p1, p2, p3, *refs):
-    (
-        mixed_a,
-        mixed_b,
-        query_edge_a,
-        query_fwd_b,
-        query_bwd_b,
-        fwd_b,
-        bwd_b,
-        end_b,
-        edge_b,
-        rate_b,
-        query_s,
-        value_s,
-        key_s,
-        low_s,
-        far_query_s,
-        far_low_s,
-    ) = refs
-    place = place_ref[0]
+def decay_inputs(up_ref, bias_ref, size):
     rank = up_ref.shape[0]
-    size = mixed_a.shape[0]
-    at = pl.ds(pl.multiple_of(place * DK, DK), DK)
     ones = (lax.broadcasted_iota(jnp.int32, (rank, DK), 0) == 0).astype(jnp.float32)
     up = jnp.concatenate(
-        [part.astype(jnp.float32) for part in split3(up_ref[:, at])] + [ones], axis=0
+        [part.astype(jnp.float32) for part in split3(up_ref[...])] + [ones], axis=0
     ).astype(jnp.bfloat16)
-    bias = bias_ref[:, at]
     row = lax.broadcasted_iota(jnp.int32, (size, size), 0)
     col = lax.broadcasted_iota(jnp.int32, (size, size), 1)
     lower = ((row // BLOCK) == (col // BLOCK)) & (col <= row)
-    sum_up_to = jnp.where(lower, 1.0, 0.0).astype(jnp.bfloat16)
-    first_pair = place < HEADS // 2
-    join = lambda tensors: jnp.concatenate(tensors, axis=0)
-    times = lambda left, right: [a * b for a, b in zip(left, right)]
-    short = lambda tensors: [tensor.astype(jnp.bfloat16) for tensor in tensors]
-
-    arrange_low(place, low_s, p0, p1)
-    arrange(place, query_s, p0, p1, slice(0, DK))
-    arrange(place, value_s, p0, p1, slice(DK, DK + DV))
-    arrange(place, key_s, own_ref.at[:size // 2], own_ref.at[size // 2 :], slice(0, DK))
-    found = factors(*decay_of(low_s[...], up, bias, sum_up_to), first_pair)
+    return up, bias_ref[...], jnp.where(lower, 1.0, 0.0).astype(jnp.bfloat16)
+
+
+def joined(tensors):
+    return jnp.concatenate(tensors, axis=0)
+
+
+def times(left, right):
+    return [a * b for a, b in zip(left, right)]
+
+
+def short(tensors):
+    return [tensor.astype(jnp.bfloat16) for tensor in tensors]
+
+
+def own_kernel(
+    place_ref, up_ref, bias_ref, own_ref, p0, p1,
+    mixed_a, query_edge_a, state_a, query_s, value_s, key_s,
+):
+    place = place_ref[0]
+    size = mixed_a.shape[0]
+    arrange(place, query_s, query_of(p0), query_of(p1))
+    arrange(place, value_s, value_of(p0), value_of(p1))
+    arrange(place, key_s, own_ref.at[: size // 2], own_ref.at[size // 2 :])
+    up, bias, sum_up_to = decay_inputs(up_ref, bias_ref, size)
+    low = arrange_low(place, p0, p1)
+    found = factors(*decay_of(low, up, bias, sum_up_to), place < HEADS // 2)
     scaled = in_blocks(query_s[...].astype(jnp.float32) * DK**-0.5)
     keys = in_blocks(key_s[...].astype(jnp.float32))
     scores = scores_of(
@@ -431,21 +428,28 @@
         found["rate"],
     )
     mixed_a[...] = dot_nn(scores, value_s[...])
-    query_edge_a[...] = join(short(times(scaled, found["query_edge"])))
-    key_edge = join(short(times(keys, found["key_edge"])))
-    state = dot_tn(key_edge, value_s[...]).astype(jnp.bfloat16)
-
-    arrange_low(place, far_low_s, p2, p3)
-    arrange(place, far_query_s, p2, p3, slice(0, DK))
-    found = factors(*decay_of(far_low_s[...], up, bias, sum_up_to), jnp.logical_not(first_pair))
-    scaled = in_blocks(far_query_s[...].astype(jnp.float32) * DK**-0.5)
-    query_fwd_b[...] = join(short(times(scaled, found["query_fwd"])))
-    query_bwd_b[...] = join(short(times(scaled, found["query_bwd"])))
-    mixed_b[...] = dot_nn(join(short(times(scaled, found["query_edge"]))), state)
-    fwd_b[...] = join(found["key_fwd"])
-    bwd_b[...] = join(found["key_bwd"])
-    end_b[...] = join(found["key_end"])
-    edge_b[...] = join(found["key_edge"])
+    query_edge_a[...] = joined(short(times(scaled, found["query_edge"])))
+    key_edge = joined(short(times(keys, found["key_edge"])))
+    state_a[...] = dot_tn(key_edge, value_s[...]).astype(jnp.bfloat16)
+
+
+def other_kernel(
+    place_ref, up_ref, bias_ref, state_a, p2, p3,
+    mixed_b, query_fwd_b, query_bwd_b, fwd_b, bwd_b, end_b, edge_b, rate_b, query_s,
+):
+    place = place_ref[0]
+    arrange(place, query_s, query_of(p2), query_of(p3))
+    up, bias, sum_up_to = decay_inputs(up_ref, bias_ref, mixed_b.shape[0])
+    low = arrange_low(place, p2, p3)
+    found = factors(*decay_of(low, up, bias, sum_up_to), place >= HEADS // 2)
+    scaled = in_blocks(query_s[...].astype(jnp.float32) * DK**-0.5)
+    query_fwd_b[...] = joined(short(times(scaled, found["query_fwd"])))
+    query_bwd_b[...] = joined(short(times(scaled, found["query_bwd"])))
+    mixed_b[...] = dot_nn(joined(short(times(scaled, found["query_edge"]))), state_a[...])
+    fwd_b[...] = joined(found["key_fwd"])
+    bwd_b[...] = joined(found["key_bwd"])
+    end_b[...] = joined(found["key_end"])
+    edge_b[...] = joined(found["key_edge"])
     for at, rate in enumerate(found["rate"]):
         rate_b[at * PACK : (at + 1) * PACK, :] = jnp.broadcast_to(rate, (PACK, DK))
 
@@ -470,8 +474,8 @@
 ):
     place = place_ref[0]
     size = mixed_b.shape[0]
-    arrange(place, value_s, p2, p3, slice(DK, DK + DV))
-    arrange(place, key_s, got_ref.at[:size // 2], got_ref.at[size // 2 :], slice(0, DK))
+    arrange(place, value_s, value_of(p2), value_of(p3))
+    arrange(place, key_s, got_ref.at[: size // 2], got_ref.at[size // 2 :])
     keys = key_s[...].astype(jnp.float32)
     rates = [rate_b[at : at + 1, :] for at in range(0, rate_b.shape[0], PACK)]
     scores = scores_of(
@@ -483,8 +487,7 @@
         rates,
     )
     mixed = mixed_b[...] + dot_nn(scores, value_s[...])
-    gain = gain_ref[:, pl.ds(pl.multiple_of(place * DV, DV), DV)]
-    result_s[...] = normed_of(mixed, gain)
+    result_s[...] = normed_of(mixed, gain_ref[...])
     write_halves(place, result_s, near_ref, far_ref)
 
 
@@ -494,13 +497,12 @@
 ):
     place = place_ref[0]
     size = mixed_a.shape[0]
-    arrange(place, value_s, p2, p3, slice(DK, DK + DV))
-    arrange(place, key_s, got_ref.at[:size // 2], got_ref.at[size // 2 :], slice(0, DK))
+    arrange(place, value_s, value_of(p2), value_of(p3))
+    arrange(place, key_s, got_ref.at[: size // 2], got_ref.at[size // 2 :])
     key_edge = (key_s[...].astype(jnp.float32) * edge_b[...]).astype(jnp.bfloat16)
     state = dot_tn(key_edge, value_s[...]).astype(jnp.bfloat16)
     mixed = mixed_a[...] + dot_nn(query_edge_a[...], state)
-    gain = gain_ref[:, pl.ds(pl.multiple_of(place * DV, DV), DV)]
-    result_s[...] = normed_of(mixed, gain)
+    result_s[...] = normed_of(mixed, gain_ref[...])
     write_halves(place, result_s, near_ref, far_ref)
 
 
@@ -513,28 +515,31 @@
         out_shape=[jax.ShapeDtypeStruct(*shape) for shape in shapes],
         scratch_shapes=[pltpu.VMEM(*shape) for shape in scratch],
         compiler_params=room(16),
-    )(place, *operands)
-
-
-def mix_heads(place, decay_up, decay_bias, norm_gain, own, got, parcels):
+    )(place, *inner(operands))
+
+
+def mix_heads(place, up, bias, gain, own, got, parcels):
     tok_count = parcels[0].shape[0] - PACK
     size = 2 * tok_count
-    rank = decay_up.shape[0]
-    short, wide = jnp.bfloat16, jnp.float32
-    query, value, mixed = ((size, DK), short), ((size, DV), short), ((size, DV), wide)
-    factor = ((size, DK), wide)
+    narrow, wide = jnp.bfloat16, jnp.float32
+    query, value, mixed = ((size, DK), narrow), ((size, DV), narrow), ((size, DV), wide)
+    factor, state = ((size, DK), wide), ((DK, DV), narrow)
     rates = ((size // BLOCK * PACK, DK), wide)
-    half = ((tok_count, DV), short)
-    (
-        mixed_a, mixed_b, query_edge_a, query_fwd_b, query_bwd_b, fwd_b, bwd_b, end_b, edge_b, rate_b,
-    ) = on_chip(
-        early_kernel,
+    half = ((tok_count, DV), narrow)
+    mixed_a, query_edge_a, state_a = on_chip(
+        own_kernel,
         place,
-        (decay_up, decay_bias.reshape(1, -1), own, *parcels),
-        [mixed, mixed, query, query, query, factor, factor, factor, factor, rates],
-        [query, value, query, ((4 * rank, size), short), query, ((4 * rank, size), short)],
-    )
-    gain = norm_gain.reshape(1, -1)
+        (up, bias, own, *parcels[:2]),
+        [mixed, query, state],
+        [query, value, query],
+    )
+    mixed_b, query_fwd_b, query_bwd_b, fwd_b, bwd_b, end_b, edge_b, rate_b = on_chip(
+        other_kernel,
+        place,
+        (up, bias, state_a, *parcels[2:]),
+        [mixed, query, query, factor, factor, factor, factor, rates],
+        [query],
+    )
     scratch = [value, query, value]
     far = on_chip(
         far_kernel,
@@ -580,25 +585,32 @@
     rank = lax.axis_index("dp").reshape(1)
     token_rows = hidden.reshape(tok_count, model_width)
 
+    small = (
+        decay_down.T,
+        span_shift.reshape(1, tok_count),
+        decay_up,
+        decay_bias.reshape(1, -1),
+        norm_gain.reshape(1, -1),
+    )
+    own_piece, own_rows, up, bias, gain, *parcels = prepare(
+        place,
+        rank,
+        token_rows,
+        small,
+        key_weight,
+        queries.reshape(tok_count, KEY),
+        values.reshape(tok_count, VAL),
+    )
     peer_rows = exchange(token_rows, "sp", 1)
-    own_piece = take_columns(place, key_weight)
     pieces = {0: own_piece}
     for flip in range(2, dp_size, 2):
         pieces[flip] = exchange(own_piece, "dp", flip)
-    parcels = make_parcels(
-        place,
-        token_rows,
-        decay_down,
-        queries.reshape(tok_count, KEY),
-        values.reshape(tok_count, VAL),
-        span_shift.reshape(1, tok_count),
-    )
     parcels = [parcels[0]] + [exchange(parcels[flip], "sp", flip) for flip in range(1, HEADS)]
     for flip in range(0, dp_size, 2):
         pieces[flip + 1] = exchange(pieces[flip], "dp", 1)
-    own, sent = project_keys(rank, token_rows, peer_rows, [pieces[i] for i in range(dp_size)])
+    own, sent = project_keys(rank, own_rows, peer_rows, [pieces[i] for i in range(dp_size)])
     got = exchange(sent, "sp", 2)
-    outs = mix_heads(place, decay_up, decay_bias, norm_gain, own, got, parcels)
+    outs = mix_heads(place, up, bias, gain, own, got, parcels)
     parts = [outs[0]] + [exchange(outs[flip], "sp", flip) for flip in range(1, HEADS)]
     return join_heads(place, parts).reshape(seq_count, tok_count, VAL)
 

time: 65.1 us -> 62.5 us (0.960)
  Pallas kernels: 10.6 us -> 7.14 us
  waiting for transfers between devices: 34.4 us -> 37.5 us
  starting transfers between devices: 19.1 us -> 17.7 us
  local copies, waits for them, and re-layouts: 0.67 us -> 0 us
    ppermute x15, waiting for transfers between devices: 34.4 us -> 37.5 us  [exchange(): return lax.ppermute(tensor, axis, [(i, i ^ flip) for i in range(size)])]
    pallas_call x2 -> x1, Pallas kernels: 3.21 us -> 1.53 us  [prepare(): pl.pallas_call(prepare_kernel, in_specs=[pl.BlockSpec(memory_space=pltpu....]
    ppermute x15, starting transfers between devices: 19.1 us -> 17.7 us  [exchange(): return lax.ppermute(tensor, axis, [(i, i ^ flip) for i in range(size)])]
    pallas_call x1, Pallas kernels: 1.69 us -> 0.71 us  [project_keys(): pl.pallas_call(keys_kernel, in_specs=[pl.BlockSpec(memory_space=pltpu.SME...]
    pallas_call x3 -> x4, Pallas kernels: 4.86 us -> 4.07 us  [on_chip(): pl.pallas_call(kernel, in_specs=[pl.BlockSpec(memory_space=pltpu.SMEM)] +...]
    unnamed x12 -> x0, local copies, waits for them, and re-layouts: 0.67 us -> none
  transfers between devices with their start and end apart: 15 -> 15, of which waited for: 7 -> 8; matrix products, arithmetic and copies ran while one was open for 0% -> 0% of each run, Pallas kernels for 12% -> 9%
where the time goes in v2:
time: 62.5 us; the launch traced here: 62.4 us
  waiting for transfers between devices  37.5 us (60%)
  starting transfers between devices  17.7 us (28%)
  Pallas kernels  7.14 us (11%)
    ppermute x15, waiting for transfers between devices, exchange(): return lax.ppermute(tensor, axis, [(i, i ^ flip) for i in range(size)])  37.5 us
    ppermute x15, starting transfers between devices, exchange(): return lax.ppermute(tensor, axis, [(i, i ^ flip) for i in range(size)])  17.7 us
    pallas_call x4, Pallas kernels, on_chip(): pl.pallas_call(kernel, in_specs=[pl.BlockSpec(memory_space=pltpu.SMEM)] +...  4.07 us
    pallas_call x1, Pallas kernels, prepare(): pl.pallas_call(prepare_kernel, in_specs=[pl.BlockSpec(memory_space=pltpu....  1.53 us
  transfers between devices with their start and end apart: 15, of which 8 were waited for; matrix products, arithmetic and copies ran while one was open for 0% of the time, Pallas kernels for 9%

profile of v2, /device:TPU:0, one launch (start us, length us, event | category | flops | bytes accessed | tf_op | source)
XLA Modules:
  0.0 62.4 jit_solution(12171801792229089746)
XLA Ops:
  0.0 3.1 %collective-permute-start = (bf16[128,2048]{1,0:T(8,128)(2,1)}, bf16[128,2048]{1,0:T(8,128)(2,1)S(1)}, u32[]{:S(2)}, u32[]{:S(2)}) collective-permute-start(bf16[128,2048]{1,0:T(8,128)(2,1)} %bitcast.10), channel_id=1, source_target_pairs={{0,8},{8,0},{16,24},{24,16},{1,9},{9,1},{17,25},{25,17},{2,10},{10... | collective-permute-start | bytes 1572872 | tf_op jit(solution)/shard_map/ppermute | solution.py:164
  3.1 1.5 %prepare.1 = (bf16[256,512]{1,0:T(8,128)(2,1)S(1)}, bf16[128,2048]{1,0:T(8,128)(2,1)S(1)}, f32[16,256]{1,0:T(8,128)S(1)}, f32[1,256]{1,0:T(1,128)S(1)}, f32[1,51...) custom-call(s32[1]{0:T(128)} %bitcast.place_ref, ...), custom_call_target="tpu_custom_call" | custom-call | tf_op jit(solution)/shard_map/prepare/pallas_call | solution.py:239
  4.6 2.5 %collective-permute-start.6 = (bf16[256,512]{1,0:T(8,128)(2,1)S(1)}, bf16[256,512]{1,0:T(8,128)(2,1)S(1)}, u32[]{:S(2)}, u32[]{:S(2)}) collective-permute-start(bf16[256,512]{1,0:T(8,128)(2,1)S(1)} %get-tuple-element.33.refs_0_), channel_id=1, source_target_pairs={{0,6},{1,7},{2,4},{3,5},{4,2},{5,3},{6,0},{7,1},{8,14},{9,15},{10,... | collective-permute-start | bytes 786440 | tf_op jit(solution)/shard_map/ppermute | solution.py:164
  7.1 0.5 collective-permute-start.4
  7.6 0.5 collective-permute-start.2
  8.1 0.0 collective-permute-start.1
  8.1 6.6 %collective-permute-done.6.refs_6_ = bf16[256,512]{1,0:T(8,128)(2,1)S(1)} collective-permute-done((bf16[256,512]{1,0:T(8,128)(2,1)S(1)}, bf16[256,512]{1,0:T(8,128)(2,1)S(1)}, u32[]{:S(2)}, u32[]{:S(2)}) %collective-permute-start.6) | collective-permute-done | bytes 262176 | tf_op jit(solution)/shard_map/ppermute | solution.py:164
  14.8 0.0 collective-permute-start.7
  14.8 4.2 %collective-permute-done.4.refs_4_ = bf16[256,512]{1,0:T(8,128)(2,1)S(1)} collective-permute-done((bf16[256,512]{1,0:T(8,128)(2,1)S(1)}, bf16[256,512]{1,0:T(8,128)(2,1)S(1)}, u32[]{:S(2)}, u32[]{:S(2)}) %collective-permute-start.4) | collective-permute-done | bytes 262176 | tf_op jit(solution)/shard_map/ppermute | solution.py:164
  18.9 0.0 collective-permute-start.5
  19.0 0.1 collective-permute-done.2.refs_2_
  19.0 0.4 collective-permute-start.3
  19.5 0.0 collective-permute-done.1.refs_1_
  19.5 0.3 collective-permute-start.11
  19.7 0.0 collective-permute-done.peer_ref
  19.7 2.8 %collective-permute-start.9 = (bf16[136,768]{1,0:T(8,128)(2,1)S(1)}, bf16[136,768]{1,0:T(8,128)(2,1)S(1)}, u32[]{:S(2)}, u32[]{:S(2)}) collective-permute-start(bf16[136,768]{1,0:T(8,128)(2,1)S(1)} %get-tuple-element.35), channel_id=1, source_target_pairs={{0,16},{8,24},{16,0},{24,8},{1,17},{9,25},{17,1},{25,9},{2,18},{10... | collective-permute-start | bytes 626696 | tf_op jit(solution)/shard_map/ppermute | solution.py:164
  22.5 0.0 collective-permute-done.7.refs_7_
  22.5 1.3 %collective-permute-start.10 = (bf16[136,768]{1,0:T(8,128)(2,1)S(1)}, bf16[136,768]{1,0:T(8,128)(2,1)S(1)}, u32[]{:S(2)}, u32[]{:S(2)}) collective-permute-start(bf16[136,768]{1,0:T(8,128)(2,1)S(1)} %get-tuple-element.36), channel_id=1, source_target_pairs={{0,24},{8,16},{16,8},{24,0},{1,25},{9,17},{17,9},{25,1},{2,26},{10... | collective-permute-start | bytes 626696 | tf_op jit(solution)/shard_map/ppermute | solution.py:164
  23.9 0.0 collective-permute-done.5.refs_5_
  23.9 0.0 collective-permute-done.3.refs_3_
  23.9 0.7 %keys.1 = (bf16[256,256]{1,0:T(8,128)(2,1)S(1)}, bf16[256,256]{1,0:T(8,128)(2,1)S(1)}) custom-call(s32[1]{0:T(128)} %bitcast.1.rank_ref, bf16[128,2048]{1,0:T(8,128)(2,1)S(1)} %get-tuple-element.32.hidden_ref, bf16[128,2048]{1,0:T(8,128)(2,1)S(1)} %collective-permute-done.peer_ref, bf16[256,512]{1,0:T(8,128)(2,1)S(1)} %get-tuple-element.33.refs_0_, ...), custom_call_target="tpu_custom_call" | custom-call | tf_op jit(solution)/shard_map/keys/pallas_call | solution.py:272
  24.6 1.8 %collective-permute-start.8 = (bf16[256,256]{1,0:T(8,128)(2,1)S(1)}, bf16[256,256]{1,0:T(8,128)(2,1)S(1)}, u32[]{:S(2)}, u32[]{:S(2)}) collective-permute-start(bf16[256,256]{1,0:T(8,128)(2,1)S(1)} %get-tuple-element.34), channel_id=1, source_target_pairs={{0,16},{8,24},{16,0},{24,8},{1,17},{9,25},{17,1},{25,9},{2,18},{10... | collective-permute-start | bytes 393224 | tf_op jit(solution)/shard_map/ppermute | solution.py:164
  26.3 4.8 %collective-permute-done.11.p1 = bf16[136,768]{1,0:T(8,128)(2,1)S(1)} collective-permute-done((bf16[136,768]{1,0:T(8,128)(2,1)S(1)}, bf16[136,768]{1,0:T(8,128)(2,1)S(1)}, u32[]{:S(2)}, u32[]{:S(2)}) %collective-permute-start.11) | collective-permute-done | bytes 208928 | tf_op jit(solution)/shard_map/ppermute | solution.py:164
  31.1 1.5 %shard_map.91 = (f32[256,512]{1,0:T(8,128)S(1)}, bf16[256,256]{1,0:T(8,128)(2,1)S(1)}, bf16[256,512]{1,0:T(8,128)(2,1)S(1)}) custom-call(s32[1]{0:T(128)} %bitcast.place_ref, f32[16,256]{1,0:T(8,128)S(1)} %get-tuple-element.37.up_ref, f32[1,256]{1,0:T(1,128)S(1)} %get-tuple-element.38.bias_ref, bf16[256,256]{1,0:T(8,128)(2,1)S(1)} %get-tuple-element.39.own_ref, ...), custom_call_target="tpu_custom_call" | custom-call | tf_op jit(solution)/shard_map/pallas_call | solution.py:510
  32.6 0.0 collective-permute-done.9.p2
  32.6 6.0 %collective-permute-done.10.p3 = bf16[136,768]{1,0:T(8,128)(2,1)S(1)} collective-permute-done((bf16[136,768]{1,0:T(8,128)(2,1)S(1)}, bf16[136,768]{1,0:T(8,128)(2,1)S(1)}, u32[]{:S(2)}, u32[]{:S(2)}) %collective-permute-start.10) | collective-permute-done | bytes 208928 | tf_op jit(solution)/shard_map/ppermute | solution.py:164
  38.6 1.1 %shard_map.92 = (f32[256,512]{1,0:T(8,128)S(1)}, bf16[256,256]{1,0:T(8,128)(2,1)S(1)}, bf16[256,256]{1,0:T(8,128)(2,1)S(1)}, f32[256,256]{1,0:T(8,128)S(1)}, f32...) custom-call(s32[1]{0:T(128)} %bitcast.place_ref, ...), custom_call_target="tpu_custom_call" | custom-call | tf_op jit(solution)/shard_map/pallas_call | solution.py:510
  39.7 7.1 %collective-permute-done.8.got_ref = bf16[256,256]{1,0:T(8,128)(2,1)S(1)} collective-permute-done((bf16[256,256]{1,0:T(8,128)(2,1)S(1)}, bf16[256,256]{1,0:T(8,128)(2,1)S(1)}, u32[]{:S(2)}, u32[]{:S(2)}) %collective-permute-start.8) | collective-permute-done | bytes 131104 | tf_op jit(solution)/shard_map/ppermute | solution.py:164
  46.8 0.7 %shard_map.93 = (bf16[128,512]{1,0:T(8,128)(2,1)S(1)}, bf16[128,512]{1,0:T(8,128)(2,1)S(1)}) custom-call(s32[1]{0:T(128)} %bitcast.place_ref, f32[1,512]{1,0:T(1,128)S(1)} %get-tuple-element.31.gain_ref, bf16[256,256]{1,0:T(8,128)(2,1)S(1)} %collective-permute-done.8.got_ref, bf16[136,768]{1,0:T(8,128)(2,1)S(1)} %collective-permute-done.9.p2, ...), custom_call_target="tpu_custom_call" | custom-call | tf_op jit(solution)/shard_map/pallas_call | solution.py:510
  47.5 0.8 %collective-permute-start.12 = (bf16[128,512]{1,0:T(8,128)(2,1)S(1)}, bf16[128,512]{1,0:T(8,128)(2,1)S(1)}, u32[]{:S(2)}, u32[]{:S(2)}) collective-permute-start(bf16[128,512]{1,0:T(8,128)(2,1)S(1)} %get-tuple-element.47), channel_id=1, source_target_pairs={{0,8},{8,0},{16,24},{24,16},{1,9},{9,1},{17,25},{25,17},{2,10},{10... | collective-permute-start | bytes 393224 | tf_op jit(solution)/shard_map/ppermute | solution.py:164
  48.3 0.8 %shard_map.94 = (bf16[128,512]{1,0:T(8,128)(2,1)S(1)}, bf16[128,512]{1,0:T(8,128)(2,1)S(1)}) custom-call(s32[1]{0:T(128)} %bitcast.place_ref, f32[1,512]{1,0:T(1,128)S(1)} %get-tuple-element.31.gain_ref, bf16[256,256]{1,0:T(8,128)(2,1)S(1)} %collective-permute-done.8.got_ref, bf16[136,768]{1,0:T(8,128)(2,1)S(1)} %collective-permute-done.9.p2, ...), custom_call_target="tpu_custom_call" | custom-call | tf_op jit(solution)/shard_map/pallas_call | solution.py:510
  49.1 3.4 %collective-permute-start.13 = (bf16[128,512]{1,0:T(8,128)(2,1)S(1)}, bf16[128,512]{1,0:T(8,128)(2,1)S(1)}, u32[]{:S(2)}, u32[]{:S(2)}) collective-permute-start(bf16[128,512]{1,0:T(8,128)(2,1)S(1)} %get-tuple-element.55), channel_id=1, source_target_pairs={{0,16},{8,24},{16,0},{24,8},{1,17},{9,25},{17,1},{25,9},{2,18},{10... | collective-permute-start | bytes 393224 | tf_op jit(solution)/shard_map/ppermute | solution.py:164
  52.5 0.2 collective-permute-start.14
  52.8 0.1 collective-permute-done.12.refs_1_
  52.9 8.6 %collective-permute-done.13.refs_2_ = bf16[128,512]{1,0:T(8,128)(2,1)S(1)} collective-permute-done((bf16[128,512]{1,0:T(8,128)(2,1)S(1)}, bf16[128,512]{1,0:T(8,128)(2,1)S(1)}, u32[]{:S(2)}, u32[]{:S(2)}) %collective-permute-start.13) | collective-permute-done | bytes 131104 | tf_op jit(solution)/shard_map/ppermute | solution.py:164
  61.5 0.0 collective-permute-done.14.refs_3_
  61.5 0.8 %join.1 = bf16[128,2048]{1,0:T(8,128)(2,1)} custom-call(s32[1]{0:T(128)} %bitcast.place_ref, bf16[128,512]{1,0:T(8,128)(2,1)S(1)} %get-tuple-element.46.refs_0_, bf16[128,512]{1,0:T(8,128)(2,1)S(1)} %collective-permute-done.12.refs_1_, bf16[128,512]{1,0:T(8,128)(2,1)S(1)} %collective-permute-done.13.refs_2_, bf16[128,512]{1,0:T(8,128)(2,1)S(1)} %collective-permute-done.14.refs_3_), custom_call_target="tpu_custom_call" | custom-call | tf_op jit(solution)/shard_map/join/pallas_call | solution.py:569
Async XLA Ops:
  0.0 19.7 %collective-permute-start = (bf16[128,2048]{1,0:T(8,128)(2,1)}, bf16[128,2048]{1,0:T(8,128)(2,1)S(1)}, u32[]{:S(2)}, u32[]{:S(2)}) collective-permute-start(bf16[128,2048]{1,0:T(8,128)(2,1)} %bitcast.10), channel_id=1, source_target_pairs={{0,8},{8,0},{16,24},{24,16},{1,9},{9,1},{17,25},{25,17},{2,10},{10... | collective-permute-start | bytes 1572872 | tf_op jit(solution)/shard_map/ppermute | solution.py:164
  4.6 10.2 %collective-permute-start.6 = (bf16[256,512]{1,0:T(8,128)(2,1)S(1)}, bf16[256,512]{1,0:T(8,128)(2,1)S(1)}, u32[]{:S(2)}, u32[]{:S(2)}) collective-permute-start(bf16[256,512]{1,0:T(8,128)(2,1)S(1)} %get-tuple-element.33.refs_0_), channel_id=1, source_target_pairs={{0,6},{1,7},{2,4},{3,5},{4,2},{5,3},{6,0},{7,1},{8,14},{9,15},{10,... | collective-permute-start | bytes 786440 | tf_op jit(solution)/shard_map/ppermute | solution.py:164
  7.1 11.8 %collective-permute-start.4 = (bf16[256,512]{1,0:T(8,128)(2,1)S(1)}, bf16[256,512]{1,0:T(8,128)(2,1)S(1)}, u32[]{:S(2)}, u32[]{:S(2)}) collective-permute-start(bf16[256,512]{1,0:T(8,128)(2,1)S(1)} %get-tuple-element.33.refs_0_), channel_id=1, source_target_pairs={{0,4},{1,5},{2,6},{3,7},{4,0},{5,1},{6,2},{7,3},{8,12},{9,13},{10,... | collective-permute-start | bytes 786440 | tf_op jit(solution)/shard_map/ppermute | solution.py:164
  7.6 11.4 %collective-permute-start.2 = (bf16[256,512]{1,0:T(8,128)(2,1)S(1)}, bf16[256,512]{1,0:T(8,128)(2,1)S(1)}, u32[]{:S(2)}, u32[]{:S(2)}) collective-permute-start(bf16[256,512]{1,0:T(8,128)(2,1)S(1)} %get-tuple-element.33.refs_0_), channel_id=1, source_target_pairs={{0,2},{1,3},{2,0},{3,1},{4,6},{5,7},{6,4},{7,5},{8,10},{9,11},{10,... | collective-permute-start | bytes 786440 | tf_op jit(solution)/shard_map/ppermute | solution.py:164
  8.1 11.3 %collective-permute-start.1 = (bf16[256,512]{1,0:T(8,128)(2,1)S(1)}, bf16[256,512]{1,0:T(8,128)(2,1)S(1)}, u32[]{:S(2)}, u32[]{:S(2)}) collective-permute-start(bf16[256,512]{1,0:T(8,128)(2,1)S(1)} %get-tuple-element.33.refs_0_), channel_id=1, source_target_pairs={{0,1},{1,0},{2,3},{3,2},{4,5},{5,4},{6,7},{7,6},{8,9},{9,8},{10,11... | collective-permute-start | bytes 786440 | tf_op jit(solution)/shard_map/ppermute | solution.py:164
  14.8 7.7 %collective-permute-start.7 = (bf16[256,512]{1,0:T(8,128)(2,1)S(1)}, bf16[256,512]{1,0:T(8,128)(2,1)S(1)}, u32[]{:S(2)}, u32[]{:S(2)}) collective-permute-start(bf16[256,512]{1,0:T(8,128)(2,1)S(1)} %collective-permute-done.6.refs_6_), channel_id=1, source_target_pairs={{0,1},{1,0},{2,3},{3,2},{4,5},{5,4},{6,7},{7,6},{8,9},{9,8},{10,11... | collective-permute-start | bytes 786440 | tf_op jit(solution)/shard_map/ppermute | solution.py:164
  18.9 4.9 %collective-permute-start.5 = (bf16[256,512]{1,0:T(8,128)(2,1)S(1)}, bf16[256,512]{1,0:T(8,128)(2,1)S(1)}, u32[]{:S(2)}, u32[]{:S(2)}) collective-permute-start(bf16[256,512]{1,0:T(8,128)(2,1)S(1)} %collective-permute-done.4.refs_4_), channel_id=1, source_target_pairs={{0,1},{1,0},{2,3},{3,2},{4,5},{5,4},{6,7},{7,6},{8,9},{9,8},{10,11... | collective-permute-start | bytes 786440 | tf_op jit(solution)/shard_map/ppermute | solution.py:164
  19.0 4.8 %collective-permute-start.3 = (bf16[256,512]{1,0:T(8,128)(2,1)S(1)}, bf16[256,512]{1,0:T(8,128)(2,1)S(1)}, u32[]{:S(2)}, u32[]{:S(2)}) collective-permute-start(bf16[256,512]{1,0:T(8,128)(2,1)S(1)} %collective-permute-done.2.refs_2_), channel_id=1, source_target_pairs={{0,1},{1,0},{2,3},{3,2},{4,5},{5,4},{6,7},{7,6},{8,9},{9,8},{10,11... | collective-permute-start | bytes 786440 | tf_op jit(solution)/shard_map/ppermute | solution.py:164
  19.5 11.6 %collective-permute-start.11 = (bf16[136,768]{1,0:T(8,128)(2,1)S(1)}, bf16[136,768]{1,0:T(8,128)(2,1)S(1)}, u32[]{:S(2)}, u32[]{:S(2)}) collective-permute-start(bf16[136,768]{1,0:T(8,128)(2,1)S(1)} %get-tuple-element.41), channel_id=1, source_target_pairs={{0,8},{8,0},{16,24},{24,16},{1,9},{9,1},{17,25},{25,17},{2,10},{10... | collective-permute-start | bytes 626696 | tf_op jit(solution)/shard_map/ppermute | solution.py:164
  19.7 12.9 %collective-permute-start.9 = (bf16[136,768]{1,0:T(8,128)(2,1)S(1)}, bf16[136,768]{1,0:T(8,128)(2,1)S(1)}, u32[]{:S(2)}, u32[]{:S(2)}) collective-permute-start(bf16[136,768]{1,0:T(8,128)(2,1)S(1)} %get-tuple-element.35), channel_id=1, source_target_pairs={{0,16},{8,24},{16,0},{24,8},{1,17},{9,25},{17,1},{25,9},{2,18},{10... | collective-permute-start | bytes 626696 | tf_op jit(solution)/shard_map/ppermute | solution.py:164
  22.5 16.1 %collective-permute-start.10 = (bf16[136,768]{1,0:T(8,128)(2,1)S(1)}, bf16[136,768]{1,0:T(8,128)(2,1)S(1)}, u32[]{:S(2)}, u32[]{:S(2)}) collective-permute-start(bf16[136,768]{1,0:T(8,128)(2,1)S(1)} %get-tuple-element.36), channel_id=1, source_target_pairs={{0,24},{8,16},{16,8},{24,0},{1,25},{9,17},{17,9},{25,1},{2,26},{10... | collective-permute-start | bytes 626696 | tf_op jit(solution)/shard_map/ppermute | solution.py:164
  24.6 22.2 %collective-permute-start.8 = (bf16[256,256]{1,0:T(8,128)(2,1)S(1)}, bf16[256,256]{1,0:T(8,128)(2,1)S(1)}, u32[]{:S(2)}, u32[]{:S(2)}) collective-permute-start(bf16[256,256]{1,0:T(8,128)(2,1)S(1)} %get-tuple-element.34), channel_id=1, source_target_pairs={{0,16},{8,24},{16,0},{24,8},{1,17},{9,25},{17,1},{25,9},{2,18},{10... | collective-permute-start | bytes 393224 | tf_op jit(solution)/shard_map/ppermute | solution.py:164
  47.5 5.4 %collective-permute-start.12 = (bf16[128,512]{1,0:T(8,128)(2,1)S(1)}, bf16[128,512]{1,0:T(8,128)(2,1)S(1)}, u32[]{:S(2)}, u32[]{:S(2)}) collective-permute-start(bf16[128,512]{1,0:T(8,128)(2,1)S(1)} %get-tuple-element.47), channel_id=1, source_target_pairs={{0,8},{8,0},{16,24},{24,16},{1,9},{9,1},{17,25},{25,17},{2,10},{10... | collective-permute-start | bytes 393224 | tf_op jit(solution)/shard_map/ppermute | solution.py:164
  49.1 12.4 %collective-permute-start.13 = (bf16[128,512]{1,0:T(8,128)(2,1)S(1)}, bf16[128,512]{1,0:T(8,128)(2,1)S(1)}, u32[]{:S(2)}, u32[]{:S(2)}) collective-permute-start(bf16[128,512]{1,0:T(8,128)(2,1)S(1)} %get-tuple-element.55), channel_id=1, source_target_pairs={{0,16},{8,24},{16,0},{24,8},{1,17},{9,25},{17,1},{25,9},{2,18},{10... | collective-permute-start | bytes 393224 | tf_op jit(solution)/shard_map/ppermute | solution.py:164
  52.5 9.0 %collective-permute-start.14 = (bf16[128,512]{1,0:T(8,128)(2,1)S(1)}, bf16[128,512]{1,0:T(8,128)(2,1)S(1)}, u32[]{:S(2)}, u32[]{:S(2)}) collective-permute-start(bf16[128,512]{1,0:T(8,128)(2,1)S(1)} %get-tuple-element.56), channel_id=1, source_target_pairs={{0,24},{8,16},{16,8},{24,0},{1,25},{9,17},{17,9},{25,1},{2,26},{10... | collective-permute-start | bytes 393224 | tf_op jit(solution)/shard_map/ppermute | solution.py:164

commit v3 on v2

--- a/solution.py
+++ b/solution.py
@@ -184,7 +184,7 @@
 
 def prepare_kernel(
     place_ref, rank_ref, down_ref, shift_ref, up_ref, bias_ref, gain_ref, weight_ref, hidden_ref, query_ref,
-    value_ref, piece_ref, hidden_out, up_out, bias_out, gain_out, p0, p1, p2, p3, down_s, shift_s, sems,
+    value_ref, own_piece, sent_piece, hidden_out, up_out, bias_out, gain_out, p0, p1, p2, p3, down_s, shift_s, sems,
 ):
     parcels = (p0, p1, p2, p3)
     place = place_ref[0]
@@ -200,12 +200,14 @@
     fetch(hidden_ref, hidden_out)
     fetch(down_ref, down_s)
     fetch(shift_ref, shift_s)
-    for half in range(2):
-        fetch(weight_ref, piece_ref.at[:, pl.ds(half * DK, DK)], place ^ (2 * half), DK)
+    fetch(weight_ref, sent_piece, place ^ 2, DK)
+    fetch(weight_ref, own_piece, place, DK)
     for flip in (2, 3, 1, 0):
-        rows = parcels[flip].at[pl.ds(0, tok_count), :]
-        fetch(query_ref, rows.at[:, pl.ds(0, DK)], place ^ flip, DK)
-        fetch(value_ref, rows.at[:, pl.ds(DK, DV)], place ^ flip, DV)
+        head = place ^ flip
+        sources = ((query_ref, head), (value_ref, 2 * head), (value_ref, 2 * head + 1))
+        for slot, (source, column) in enumerate(sources):
+            rows = parcels[flip].at[pl.ds(slot * tok_count, tok_count), :]
+            fetch(source, rows, column, DK)
     fetch(up_ref, up_out, place, DK)
     fetch(bias_ref, bias_out, place, DK)
     fetch(gain_ref, gain_out, place, DV)
@@ -213,10 +215,11 @@
         copy.wait()
     low = dot_nt(down_s[...], hidden_out[...]).astype(jnp.bfloat16).astype(jnp.float32)
     shift = jnp.broadcast_to(shift_s[...].astype(jnp.float32), (PACK, tok_count))
-    empty = jnp.zeros((PACK, DK + DV - 3 * tok_count), jnp.float32)
-    tail = jnp.concatenate([low[:PACK], low[PACK:], shift, empty], axis=1).astype(jnp.bfloat16)
+    low = jnp.concatenate([low[:PACK], low[PACK:]], axis=1)
+    shift = jnp.concatenate([shift, shift], axis=1)
+    tail = jnp.concatenate([low, shift], axis=0).astype(jnp.bfloat16)
     for parcel in parcels:
-        parcel[tok_count:, :] = tail
+        parcel[3 * tok_count :, :] = tail
     for copy in copies[3:]:
         copy.wait()
 
@@ -228,9 +231,10 @@
         pltpu.with_memory_space_constraint(a, pltpu.HBM)
         for a in (down, shift, up, bias, gain, key_weight, token_rows, queries, values)
     ]
-    parcel = jax.ShapeDtypeStruct((tok_count + PACK, DK + DV), jnp.bfloat16)
+    parcel = jax.ShapeDtypeStruct((3 * tok_count + 2 * PACK, DK), jnp.bfloat16)
     shapes = [
-        jax.ShapeDtypeStruct((rows, 2 * DK), jnp.bfloat16),
+        jax.ShapeDtypeStruct((rows, DK), jnp.bfloat16),
+        jax.ShapeDtypeStruct((rows, DK), jnp.bfloat16),
         jax.ShapeDtypeStruct(token_rows.shape, jnp.bfloat16),
         jax.ShapeDtypeStruct((up.shape[0], DK), jnp.float32),
         jax.ShapeDtypeStruct((1, DK), jnp.float32),
@@ -245,38 +249,36 @@
         scratch_shapes=[
             pltpu.VMEM(down.shape, down.dtype),
             pltpu.VMEM(shift.shape, shift.dtype),
-            pltpu.SemaphoreType.DMA((8 + 2 * HEADS,)),
+            pltpu.SemaphoreType.DMA((8 + 3 * HEADS,)),
         ],
         compiler_params=room(8),
         name="prepare",
     )(place, rank, *outer)
 
 
-def keys_kernel(rank_ref, hidden_ref, peer_ref, *refs):
-    pieces, (own_ref, send_ref) = refs[:-2], refs[-2:]
-    tok_count = hidden_ref.shape[0]
-    sums = jnp.zeros((2 * tok_count, 2 * DK), jnp.float32)
-    for flip, piece in enumerate(pieces):
-        rows = piece.shape[0]
-        at = pl.multiple_of((rank_ref[0] ^ flip) * rows, rows)
-        both = jnp.concatenate([hidden_ref[:, pl.ds(at, rows)], peer_ref[:, pl.ds(at, rows)]], axis=0)
-        sums = sums + dot_nn(both, piece[...])
-    keys = sums.astype(jnp.bfloat16)
-    own_ref[...] = keys[:, :DK]
-    send_ref[...] = keys[:, DK:]
-
-
-def project_keys(rank, token_rows, peer_rows, pieces):
-    tok_count = token_rows.shape[0]
-    shape = jax.ShapeDtypeStruct((2 * tok_count, DK), jnp.bfloat16)
+def keys_kernel(rank_ref, *refs):
+    count = lax.axis_size("dp")
+    sets = (len(refs) - count) // 2
+    pieces = refs[sets : sets + count]
+    for tokens, keys in zip(refs[:sets], refs[sets + count :]):
+        sums = jnp.zeros(keys.shape, jnp.float32)
+        for flip, piece in enumerate(pieces):
+            rows = piece.shape[0]
+            at = pl.multiple_of((rank_ref[0] ^ flip) * rows, rows)
+            sums = sums + dot_nn(tokens[:, pl.ds(at, rows)], piece[...])
+        keys[...] = sums.astype(jnp.bfloat16)
+
+
+def project_keys(rank, tokens, pieces):
+    operands = (*tokens, *pieces)
     return pl.pallas_call(
         keys_kernel,
         in_specs=[pl.BlockSpec(memory_space=pltpu.SMEM)]
-        + [pl.BlockSpec(memory_space=pltpu.VMEM)] * (2 + len(pieces)),
-        out_shape=[shape, shape],
+        + [pl.BlockSpec(memory_space=pltpu.VMEM)] * len(operands),
+        out_shape=[jax.ShapeDtypeStruct((rows.shape[0], DK), jnp.bfloat16) for rows in tokens],
         compiler_params=room(12),
         name="keys",
-    )(rank, *inner((token_rows, peer_rows, *pieces)))
+    )(rank, *inner(operands))
 
 
 def split3(tensor):
@@ -299,22 +301,31 @@
         target[at, :] = part[...]
 
 
+def tokens_of(parcel):
+    return (parcel.shape[0] - 2 * PACK) // 3
+
+
 def query_of(parcel):
-    return parcel.at[: parcel.shape[0] - PACK, :DK]
-
-
-def value_of(parcel):
-    return parcel.at[: parcel.shape[0] - PACK, DK:]
+    return parcel.at[: tokens_of(parcel), :]
+
+
+def arrange_values(place, target, near, far):
+    tok_count = target.shape[0] // 2
+    half = place & 1
+    for which, part in ((half, near), (1 - half, far)):
+        at = pl.ds(pl.multiple_of(which * tok_count, tok_count), tok_count)
+        target[at, :DK] = part[tok_count : 2 * tok_count, :]
+        target[at, DK:] = part[2 * tok_count : 3 * tok_count, :]
 
 
 def arrange_low(place, near, far):
-    tok_count = near.shape[0] - PACK
-    near, far = (part[tok_count:, :].astype(jnp.float32) for part in (near, far))
+    tok_count = tokens_of(near)
+    near, far = (part[3 * tok_count :, :].astype(jnp.float32) for part in (near, far))
     odd = (place & 1) == 1
     halves = []
     for part in (jnp.where(odd, far, near), jnp.where(odd, near, far)):
-        low = [part[:, :tok_count], part[:, tok_count : 2 * tok_count]]
-        shift = part[:, 2 * tok_count : 3 * tok_count]
+        low = [part[:PACK, :tok_count], part[:PACK, tok_count:]]
+        shift = part[PACK:, :tok_count]
         row = lax.broadcasted_iota(jnp.int32, shift.shape, 0)
         first = jnp.where(row == 0, shift, 0.0)
         halves.append(jnp.concatenate(low * 3 + [first, jnp.zeros_like(first)], axis=0))
@@ -406,14 +417,14 @@
 
 
 def own_kernel(
-    place_ref, up_ref, bias_ref, own_ref, p0, p1,
+    place_ref, up_ref, bias_ref, near_keys, far_keys, p0, p1,
     mixed_a, query_edge_a, state_a, query_s, value_s, key_s,
 ):
     place = place_ref[0]
     size = mixed_a.shape[0]
     arrange(place, query_s, query_of(p0), query_of(p1))
-    arrange(place, value_s, value_of(p0), value_of(p1))
-    arrange(place, key_s, own_ref.at[: size // 2], own_ref.at[size // 2 :])
+    arrange_values(place, value_s, p0, p1)
+    arrange(place, key_s, near_keys, far_keys)
     up, bias, sum_up_to = decay_inputs(up_ref, bias_ref, size)
     low = arrange_low(place, p0, p1)
     found = factors(*decay_of(low, up, bias, sum_up_to), place < HEADS // 2)
@@ -439,7 +450,7 @@
 ):
     place = place_ref[0]
     arrange(place, query_s, query_of(p2), query_of(p3))
-    up, bias, sum_up_to = decay_inputs(up_ref, bias_ref, mixed_b.shape[0])
+    up, bias, sum_up_to = decay_inputs(up_ref, bias_ref, query_s.shape[0])
     low = arrange_low(place, p2, p3)
     found = factors(*decay_of(low, up, bias, sum_up_to), place >= HEADS // 2)
     scaled = in_blocks(query_s[...].astype(jnp.float32) * DK**-0.5)
@@ -469,13 +480,12 @@
 
 
 def far_kernel(
-    place_ref, gain_ref, got_ref, p2, p3, mixed_b, query_fwd_b, query_bwd_b, fwd_b, bwd_b, end_b, rate_b,
+    place_ref, gain_ref, near_keys, far_keys, p2, p3, mixed_b, query_fwd_b, query_bwd_b, fwd_b, bwd_b, end_b, rate_b,
     near_ref, far_ref, value_s, key_s, result_s,
 ):
     place = place_ref[0]
-    size = mixed_b.shape[0]
-    arrange(place, value_s, value_of(p2), value_of(p3))
-    arrange(place, key_s, got_ref.at[: size // 2], got_ref.at[size // 2 :])
+    arrange_values(place, value_s, p2, p3)
+    arrange(place, key_s, near_keys, far_keys)
     keys = key_s[...].astype(jnp.float32)
     rates = [rate_b[at : at + 1, :] for at in range(0, rate_b.shape[0], PACK)]
     scores = scores_of(
@@ -492,13 +502,12 @@
 
 
 def near_kernel(
-    place_ref, gain_ref, got_ref, p2, p3, mixed_a, query_edge_a, edge_b,
+    place_ref, gain_ref, near_keys, far_keys, p2, p3, mixed_a, query_edge_a, edge_b,
     near_ref, far_ref, value_s, key_s, result_s,
 ):
     place = place_ref[0]
-    size = mixed_a.shape[0]
-    arrange(place, value_s, value_of(p2), value_of(p3))
-    arrange(place, key_s, got_ref.at[: size // 2], got_ref.at[size // 2 :])
+    arrange_values(place, value_s, p2, p3)
+    arrange(place, key_s, near_keys, far_keys)
     key_edge = (key_s[...].astype(jnp.float32) * edge_b[...]).astype(jnp.bfloat16)
     state = dot_tn(key_edge, value_s[...]).astype(jnp.bfloat16)
     mixed = mixed_a[...] + dot_nn(query_edge_a[...], state)
@@ -519,18 +528,18 @@
 
 
 def mix_heads(place, up, bias, gain, own, got, parcels):
-    tok_count = parcels[0].shape[0] - PACK
+    tok_count = tokens_of(parcels[0])
     size = 2 * tok_count
     narrow, wide = jnp.bfloat16, jnp.float32
     query, value, mixed = ((size, DK), narrow), ((size, DV), narrow), ((size, DV), wide)
-    factor, state = ((size, DK), wide), ((DK, DV), narrow)
+    factor = ((size, DK), wide)
     rates = ((size // BLOCK * PACK, DK), wide)
     half = ((tok_count, DV), narrow)
     mixed_a, query_edge_a, state_a = on_chip(
         own_kernel,
         place,
-        (up, bias, own, *parcels[:2]),
-        [mixed, query, state],
+        (up, bias, *own, *parcels[:2]),
+        [mixed, query, ((DK, DV), narrow)],
         [query, value, query],
     )
     mixed_b, query_fwd_b, query_bwd_b, fwd_b, bwd_b, end_b, edge_b, rate_b = on_chip(
@@ -544,14 +553,14 @@
     far = on_chip(
         far_kernel,
         place,
-        (gain, got, *parcels[2:], mixed_b, query_fwd_b, query_bwd_b, fwd_b, bwd_b, end_b, rate_b),
+        (gain, *got, *parcels[2:], mixed_b, query_fwd_b, query_bwd_b, fwd_b, bwd_b, end_b, rate_b),
         [half, half],
         scratch,
     )
     near = on_chip(
         near_kernel,
         place,
-        (gain, got, *parcels[2:], mixed_a, query_edge_a, edge_b),
+        (gain, *got, *parcels[2:], mixed_a, query_edge_a, edge_b),
         [half, half],
         scratch,
     )
@@ -592,7 +601,7 @@
         decay_bias.reshape(1, -1),
         norm_gain.reshape(1, -1),
     )
-    own_piece, own_rows, up, bias, gain, *parcels = prepare(
+    own_piece, sent_piece, own_rows, up, bias, gain, *parcels = prepare(
         place,
         rank,
         token_rows,
@@ -602,14 +611,22 @@
         values.reshape(tok_count, VAL),
     )
     peer_rows = exchange(token_rows, "sp", 1)
-    pieces = {0: own_piece}
-    for flip in range(2, dp_size, 2):
-        pieces[flip] = exchange(own_piece, "dp", flip)
     parcels = [parcels[0]] + [exchange(parcels[flip], "sp", flip) for flip in range(1, HEADS)]
-    for flip in range(0, dp_size, 2):
-        pieces[flip + 1] = exchange(pieces[flip], "dp", 1)
-    own, sent = project_keys(rank, own_rows, peer_rows, [pieces[i] for i in range(dp_size)])
-    got = exchange(sent, "sp", 2)
+
+    def gathered(piece):
+        pieces = [piece] * dp_size
+        for flip in range(2, dp_size, 2):
+            pieces[flip] = exchange(piece, "dp", flip)
+        for flip in range(0, dp_size, 2):
+            pieces[flip + 1] = exchange(pieces[flip], "dp", 1)
+        return pieces
+
+    pieces = gathered(sent_piece)
+    got = []
+    for rows in (own_rows, peer_rows):
+        (sent,) = project_keys(rank, (rows,), pieces)
+        got.append(exchange(sent, "sp", 2))
+    own = project_keys(rank, (own_rows, peer_rows), gathered(own_piece))
     outs = mix_heads(place, up, bias, gain, own, got, parcels)
     parts = [outs[0]] + [exchange(outs[flip], "sp", flip) for flip in range(1, HEADS)]
     return join_heads(place, parts).reshape(seq_count, tok_count, VAL)

time: 62.5 us -> 63.9 us (1.022)
  starting transfers between devices: 17.7 us -> 24.2 us
  waiting for transfers between devices: 37.5 us -> 32 us
    ppermute x15 -> x23, starting transfers between devices: 17.7 us -> 24.2 us  [exchange(): return lax.ppermute(tensor, axis, [(i, i ^ flip) for i in range(size)])]
    ppermute x15 -> x23, waiting for transfers between devices: 37.5 us -> 32 us  [exchange(): return lax.ppermute(tensor, axis, [(i, i ^ flip) for i in range(size)])]
  transfers between devices with their start and end apart: 15 -> 23, of which waited for: 8 -> 11; matrix products, arithmetic and copies ran while one was open for 0% -> 0% of each run, Pallas kernels for 9% -> 9%
where the time goes in v3:
time: 63.9 us; the launch traced here: 63.8 us
  waiting for transfers between devices  32 us (50%)
  starting transfers between devices  24.2 us (38%)
  Pallas kernels  7.54 us (12%)
    ppermute x23, waiting for transfers between devices, exchange(): return lax.ppermute(tensor, axis, [(i, i ^ flip) for i in range(size)])  32 us
    ppermute x23, starting transfers between devices, exchange(): return lax.ppermute(tensor, axis, [(i, i ^ flip) for i in range(size)])  24.2 us
    pallas_call x4, Pallas kernels, on_chip(): pl.pallas_call(kernel, in_specs=[pl.BlockSpec(memory_space=pltpu.SMEM)] +...  4.08 us
    pallas_call x1, Pallas kernels, prepare(): pl.pallas_call(prepare_kernel, in_specs=[pl.BlockSpec(memory_space=pltpu....  1.54 us
  transfers between devices with their start and end apart: 23, of which 11 were waited for; matrix products, arithmetic and copies ran while one was open for 0% of the time, Pallas kernels for 9%

profile of v3, /device:TPU:0, one launch (start us, length us, event | category | flops | bytes accessed | tf_op | source)
XLA Modules:
  0.0 63.8 jit_solution(6676677933509136467)
XLA Ops:
  0.0 3.1 %collective-permute-start.8 = (bf16[128,2048]{1,0:T(8,128)(2,1)}, bf16[128,2048]{1,0:T(8,128)(2,1)S(1)}, u32[]{:S(2)}, u32[]{:S(2)}) collective-permute-start(bf16[128,2048]{1,0:T(8,128)(2,1)} %bitcast.10), channel_id=1, source_target_pairs={{0,8},{8,0},{16,24},{24,16},{1,9},{9,1},{17,25},{25,17},{2,10},{10... | collective-permute-start | bytes 1572872 | tf_op jit(solution)/shard_map/ppermute | solution.py:164
  3.1 1.5 %prepare.1 = (bf16[256,256]{1,0:T(8,128)(2,1)S(1)}, bf16[256,256]{1,0:T(8,128)(2,1)S(1)}, bf16[128,2048]{1,0:T(8,128)(2,1)S(1)}, f32[16,256]{1,0:T(8,128)S(1)}, ...) custom-call(s32[1]{0:T(128)} %bitcast.place_ref, ...), custom_call_target="tpu_custom_call" | custom-call | tf_op jit(solution)/shard_map/prepare/pallas_call | solution.py:243
  4.6 2.5 %collective-permute-start.17 = (bf16[256,256]{1,0:T(8,128)(2,1)S(1)}, bf16[256,256]{1,0:T(8,128)(2,1)S(1)}, u32[]{:S(2)}, u32[]{:S(2)}) collective-permute-start(bf16[256,256]{1,0:T(8,128)(2,1)S(1)} %get-tuple-element.39.refs_2_), channel_id=1, source_target_pairs={{0,6},{1,7},{2,4},{3,5},{4,2},{5,3},{6,0},{7,1},{8,14},{9,15},{10,... | collective-permute-start | bytes 393224 | tf_op jit(solution)/shard_map/ppermute | solution.py:164
  7.1 0.5 collective-permute-start.15
  7.6 0.5 collective-permute-start.13
  8.2 0.0 collective-permute-start.12
  8.2 2.8 %collective-permute-done.17.refs_8_ = bf16[256,256]{1,0:T(8,128)(2,1)S(1)} collective-permute-done((bf16[256,256]{1,0:T(8,128)(2,1)S(1)}, bf16[256,256]{1,0:T(8,128)(2,1)S(1)}, u32[]{:S(2)}, u32[]{:S(2)}) %collective-permute-start.17) | collective-permute-done | bytes 131104 | tf_op jit(solution)/shard_map/ppermute | solution.py:164
  11.0 3.4 %collective-permute-start.5 = (bf16[256,256]{1,0:T(8,128)(2,1)S(1)}, bf16[256,256]{1,0:T(8,128)(2,1)S(1)}, u32[]{:S(2)}, u32[]{:S(2)}) collective-permute-start(bf16[256,256]{1,0:T(8,128)(2,1)S(1)} %get-tuple-element.34.refs_1_), channel_id=1, source_target_pairs={{0,6},{1,7},{2,4},{3,5},{4,2},{5,3},{6,0},{7,1},{8,14},{9,15},{10,... | collective-permute-start | bytes 393224 | tf_op jit(solution)/shard_map/ppermute | solution.py:164
  14.4 0.0 collective-permute-done.15.refs_6_
  14.4 1.3 %collective-permute-start.3 = (bf16[256,256]{1,0:T(8,128)(2,1)S(1)}, bf16[256,256]{1,0:T(8,128)(2,1)S(1)}, u32[]{:S(2)}, u32[]{:S(2)}) collective-permute-start(bf16[256,256]{1,0:T(8,128)(2,1)S(1)} %get-tuple-element.34.refs_1_), channel_id=1, source_target_pairs={{0,4},{1,5},{2,6},{3,7},{4,0},{5,1},{6,2},{7,3},{8,12},{9,13},{10,... | collective-permute-start | bytes 393224 | tf_op jit(solution)/shard_map/ppermute | solution.py:164
  15.7 0.1 collective-permute-start
  15.7 2.4 %collective-permute-done.5.refs_7_ = bf16[256,256]{1,0:T(8,128)(2,1)S(1)} collective-permute-done((bf16[256,256]{1,0:T(8,128)(2,1)S(1)}, bf16[256,256]{1,0:T(8,128)(2,1)S(1)}, u32[]{:S(2)}, u32[]{:S(2)}) %collective-permute-start.5) | collective-permute-done | bytes 131104 | tf_op jit(solution)/shard_map/ppermute | solution.py:164
  18.2 0.0 collective-permute-start.18
  18.2 2.0 %collective-permute-done.3.refs_5_ = bf16[256,256]{1,0:T(8,128)(2,1)S(1)} collective-permute-done((bf16[256,256]{1,0:T(8,128)(2,1)S(1)}, bf16[256,256]{1,0:T(8,128)(2,1)S(1)}, u32[]{:S(2)}, u32[]{:S(2)}) %collective-permute-start.3) | collective-permute-done | bytes 131104 | tf_op jit(solution)/shard_map/ppermute | solution.py:164
  20.1 0.6 collective-permute-done.1.refs_3_
  20.7 0.0 collective-permute-start.4
  20.7 0.0 collective-permute-done.refs_2_
  20.7 0.5 collective-permute-start.2
  21.2 0.5 collective-permute-start.19
  21.7 0.0 collective-permute-done.6.refs_8_
  21.7 2.6 %collective-permute-start.10 = (bf16[400,256]{1,0:T(8,128)(2,1)S(1)}, bf16[400,256]{1,0:T(8,128)(2,1)S(1)}, u32[]{:S(2)}, u32[]{:S(2)}) collective-permute-start(bf16[400,256]{1,0:T(8,128)(2,1)S(1)} %get-tuple-element.35), channel_id=1, source_target_pairs={{0,16},{8,24},{16,0},{24,8},{1,17},{9,25},{17,1},{25,9},{2,18},{10... | collective-permute-start | bytes 614408 | tf_op jit(solution)/shard_map/ppermute | solution.py:164
  24.3 0.0 collective-permute-done.4.refs_6_
  24.3 1.3 %collective-permute-start.11 = (bf16[400,256]{1,0:T(8,128)(2,1)S(1)}, bf16[400,256]{1,0:T(8,128)(2,1)S(1)}, u32[]{:S(2)}, u32[]{:S(2)}) collective-permute-start(bf16[400,256]{1,0:T(8,128)(2,1)S(1)} %get-tuple-element.36), channel_id=1, source_target_pairs={{0,24},{8,16},{16,8},{24,0},{1,25},{9,17},{17,9},{25,1},{2,26},{10... | collective-permute-start | bytes 614408 | tf_op jit(solution)/shard_map/ppermute | solution.py:164
  25.6 0.0 collective-permute-start.16
  25.6 0.0 collective-permute-done.8.refs_0_.refs_1_
  25.6 0.5 collective-permute-start.14
  26.1 0.3 keys.3
  26.4 0.3 keys.4
  26.8 0.2 collective-permute-done.16.refs_7_
  27.0 1.7 %collective-permute-start.7 = (bf16[128,256]{1,0:T(8,128)(2,1)S(1)}, bf16[128,256]{1,0:T(8,128)(2,1)S(1)}, u32[]{:S(2)}, u32[]{:S(2)}) collective-permute-start(bf16[128,256]{1,0:T(8,128)(2,1)S(1)} %keys.3), channel_id=1, source_target_pairs={{0,16},{8,24},{16,0},{24,8},{1,17},{9,25},{17,1},{25,9},{2,18},{10... | collective-permute-start | bytes 196616 | tf_op jit(solution)/shard_map/ppermute | solution.py:164
  28.7 0.0 collective-permute-done.14.refs_5_
  28.7 1.2 %collective-permute-start.9 = (bf16[128,256]{1,0:T(8,128)(2,1)S(1)}, bf16[128,256]{1,0:T(8,128)(2,1)S(1)}, u32[]{:S(2)}, u32[]{:S(2)}) collective-permute-start(bf16[128,256]{1,0:T(8,128)(2,1)S(1)} %keys.4), channel_id=1, source_target_pairs={{0,16},{8,24},{16,0},{24,8},{1,17},{9,25},{17,1},{25,9},{2,18},{10... | collective-permute-start | bytes 196616 | tf_op jit(solution)/shard_map/ppermute | solution.py:164
  29.9 0.5 keys.5
  30.4 2.2 %collective-permute-done.19.p1 = bf16[400,256]{1,0:T(8,128)(2,1)S(1)} collective-permute-done((bf16[400,256]{1,0:T(8,128)(2,1)S(1)}, bf16[400,256]{1,0:T(8,128)(2,1)S(1)}, u32[]{:S(2)}, u32[]{:S(2)}) %collective-permute-start.19) | collective-permute-done | bytes 204832 | tf_op jit(solution)/shard_map/ppermute | solution.py:164
  32.6 1.5 %shard_map.91 = (f32[256,512]{1,0:T(8,128)S(1)}, bf16[256,256]{1,0:T(8,128)(2,1)S(1)}, bf16[256,512]{1,0:T(8,128)(2,1)S(1)}) custom-call(s32[1]{0:T(128)} %bitcast.place_ref, f32[16,256]{1,0:T(8,128)S(1)} %get-tuple-element.37.up_ref, f32[1,256]{1,0:T(1,128)S(1)} %get-tuple-element.38.bias_ref, bf16[128,256]{1,0:T(8,128)(2,1)S(1)} %get-tuple-element.40.near_keys, ...), custom_call_target="tpu_custom_call" | custom-call | tf_op jit(solution)/shard_map/pallas_call | solution.py:519
  34.1 8.0 %collective-permute-done.10.p2 = bf16[400,256]{1,0:T(8,128)(2,1)S(1)} collective-permute-done((bf16[400,256]{1,0:T(8,128)(2,1)S(1)}, bf16[400,256]{1,0:T(8,128)(2,1)S(1)}, u32[]{:S(2)}, u32[]{:S(2)}) %collective-permute-start.10) | collective-permute-done | bytes 204832 | tf_op jit(solution)/shard_map/ppermute | solution.py:164
  42.1 0.0 collective-permute-done.11.p3
  42.1 1.1 %shard_map.92 = (f32[256,512]{1,0:T(8,128)S(1)}, bf16[256,256]{1,0:T(8,128)(2,1)S(1)}, bf16[256,256]{1,0:T(8,128)(2,1)S(1)}, f32[256,256]{1,0:T(8,128)S(1)}, f32...) custom-call(s32[1]{0:T(128)} %bitcast.place_ref, ...), custom_call_target="tpu_custom_call" | custom-call | tf_op jit(solution)/shard_map/pallas_call | solution.py:519
  43.2 4.4 %collective-permute-done.7.near_keys = bf16[128,256]{1,0:T(8,128)(2,1)S(1)} collective-permute-done((bf16[128,256]{1,0:T(8,128)(2,1)S(1)}, bf16[128,256]{1,0:T(8,128)(2,1)S(1)}, u32[]{:S(2)}, u32[]{:S(2)}) %collective-permute-start.7) | collective-permute-done | bytes 65568 | tf_op jit(solution)/shard_map/ppermute | solution.py:164
  47.6 0.7 %collective-permute-done.9.far_keys = bf16[128,256]{1,0:T(8,128)(2,1)S(1)} collective-permute-done((bf16[128,256]{1,0:T(8,128)(2,1)S(1)}, bf16[128,256]{1,0:T(8,128)(2,1)S(1)}, u32[]{:S(2)}, u32[]{:S(2)}) %collective-permute-start.9) | collective-permute-done | bytes 65568 | tf_op jit(solution)/shard_map/ppermute | solution.py:164
  48.3 0.7 %shard_map.93 = (bf16[128,512]{1,0:T(8,128)(2,1)S(1)}, bf16[128,512]{1,0:T(8,128)(2,1)S(1)}) custom-call(s32[1]{0:T(128)} %bitcast.place_ref, f32[1,512]{1,0:T(1,128)S(1)} %get-tuple-element.32.gain_ref, bf16[128,256]{1,0:T(8,128)(2,1)S(1)} %collective-permute-done.7.near_keys, bf16[128,256]{1,0:T(8,128)(2,1)S(1)} %collective-permute-done.9.far_keys, ...), custom_call_target="tpu_custom_call" | custom-call | tf_op jit(solution)/shard_map/pallas_call | solution.py:519
  49.0 0.7 %collective-permute-start.20 = (bf16[128,512]{1,0:T(8,128)(2,1)S(1)}, bf16[128,512]{1,0:T(8,128)(2,1)S(1)}, u32[]{:S(2)}, u32[]{:S(2)}) collective-permute-start(bf16[128,512]{1,0:T(8,128)(2,1)S(1)} %get-tuple-element.49), channel_id=1, source_target_pairs={{0,8},{8,0},{16,24},{24,16},{1,9},{9,1},{17,25},{25,17},{2,10},{10... | collective-permute-start | bytes 393224 | tf_op jit(solution)/shard_map/ppermute | solution.py:164
  49.7 0.8 %shard_map.94 = (bf16[128,512]{1,0:T(8,128)(2,1)S(1)}, bf16[128,512]{1,0:T(8,128)(2,1)S(1)}) custom-call(s32[1]{0:T(128)} %bitcast.place_ref, f32[1,512]{1,0:T(1,128)S(1)} %get-tuple-element.32.gain_ref, bf16[128,256]{1,0:T(8,128)(2,1)S(1)} %collective-permute-done.7.near_keys, bf16[128,256]{1,0:T(8,128)(2,1)S(1)} %collective-permute-done.9.far_keys, ...), custom_call_target="tpu_custom_call" | custom-call | tf_op jit(solution)/shard_map/pallas_call | solution.py:519
  50.5 3.4 %collective-permute-start.21 = (bf16[128,512]{1,0:T(8,128)(2,1)S(1)}, bf16[128,512]{1,0:T(8,128)(2,1)S(1)}, u32[]{:S(2)}, u32[]{:S(2)}) collective-permute-start(bf16[128,512]{1,0:T(8,128)(2,1)S(1)} %get-tuple-element.57), channel_id=1, source_target_pairs={{0,16},{8,24},{16,0},{24,8},{1,17},{9,25},{17,1},{25,9},{2,18},{10... | collective-permute-start | bytes 393224 | tf_op jit(solution)/shard_map/ppermute | solution.py:164
  53.9 0.4 collective-permute-start.22
  54.3 0.3 collective-permute-done.20.refs_1_
  54.6 8.3 %collective-permute-done.21.refs_2_ = bf16[128,512]{1,0:T(8,128)(2,1)S(1)} collective-permute-done((bf16[128,512]{1,0:T(8,128)(2,1)S(1)}, bf16[128,512]{1,0:T(8,128)(2,1)S(1)}, u32[]{:S(2)}, u32[]{:S(2)}) %collective-permute-start.21) | collective-permute-done | bytes 131104 | tf_op jit(solution)/shard_map/ppermute | solution.py:164
  62.9 0.8 %join.1 = bf16[128,2048]{1,0:T(8,128)(2,1)} custom-call(s32[1]{0:T(128)} %bitcast.place_ref, bf16[128,512]{1,0:T(8,128)(2,1)S(1)} %get-tuple-element.48.refs_0_, bf16[128,512]{1,0:T(8,128)(2,1)S(1)} %collective-permute-done.20.refs_1_, bf16[128,512]{1,0:T(8,128)(2,1)S(1)} %collective-permute-done.21.refs_2_, bf16[128,512]{1,0:T(8,128)(2,1)S(1)} %collective-permute-done.22.refs_3_), custom_call_target="tpu_custom_call" | custom-call | tf_op jit(solution)/shard_map/join/pallas_call | solution.py:578
  (7 shorter events, 0.0 us)
Async XLA Ops:
  0.0 25.6 %collective-permute-start.8 = (bf16[128,2048]{1,0:T(8,128)(2,1)}, bf16[128,2048]{1,0:T(8,128)(2,1)S(1)}, u32[]{:S(2)}, u32[]{:S(2)}) collective-permute-start(bf16[128,2048]{1,0:T(8,128)(2,1)} %bitcast.10), channel_id=1, source_target_pairs={{0,8},{8,0},{16,24},{24,16},{1,9},{9,1},{17,25},{25,17},{2,10},{10... | collective-permute-start | bytes 1572872 | tf_op jit(solution)/shard_map/ppermute | solution.py:164
  4.6 6.4 %collective-permute-start.17 = (bf16[256,256]{1,0:T(8,128)(2,1)S(1)}, bf16[256,256]{1,0:T(8,128)(2,1)S(1)}, u32[]{:S(2)}, u32[]{:S(2)}) collective-permute-start(bf16[256,256]{1,0:T(8,128)(2,1)S(1)} %get-tuple-element.39.refs_2_), channel_id=1, source_target_pairs={{0,6},{1,7},{2,4},{3,5},{4,2},{5,3},{6,0},{7,1},{8,14},{9,15},{10,... | collective-permute-start | bytes 393224 | tf_op jit(solution)/shard_map/ppermute | solution.py:164
  7.1 7.3 %collective-permute-start.15 = (bf16[256,256]{1,0:T(8,128)(2,1)S(1)}, bf16[256,256]{1,0:T(8,128)(2,1)S(1)}, u32[]{:S(2)}, u32[]{:S(2)}) collective-permute-start(bf16[256,256]{1,0:T(8,128)(2,1)S(1)} %get-tuple-element.39.refs_2_), channel_id=1, source_target_pairs={{0,4},{1,5},{2,6},{3,7},{4,0},{5,1},{6,2},{7,3},{8,12},{9,13},{10,... | collective-permute-start | bytes 393224 | tf_op jit(solution)/shard_map/ppermute | solution.py:164
  7.6 8.0 %collective-permute-start.13 = (bf16[256,256]{1,0:T(8,128)(2,1)S(1)}, bf16[256,256]{1,0:T(8,128)(2,1)S(1)}, u32[]{:S(2)}, u32[]{:S(2)}) collective-permute-start(bf16[256,256]{1,0:T(8,128)(2,1)S(1)} %get-tuple-element.39.refs_2_), channel_id=1, source_target_pairs={{0,2},{1,3},{2,0},{3,1},{4,6},{5,7},{6,4},{7,5},{8,10},{9,11},{10,... | collective-permute-start | bytes 393224 | tf_op jit(solution)/shard_map/ppermute | solution.py:164
  8.2 7.5 %collective-permute-start.12 = (bf16[256,256]{1,0:T(8,128)(2,1)S(1)}, bf16[256,256]{1,0:T(8,128)(2,1)S(1)}, u32[]{:S(2)}, u32[]{:S(2)}) collective-permute-start(bf16[256,256]{1,0:T(8,128)(2,1)S(1)} %get-tuple-element.39.refs_2_), channel_id=1, source_target_pairs={{0,1},{1,0},{2,3},{3,2},{4,5},{5,4},{6,7},{7,6},{8,9},{9,8},{10,11... | collective-permute-start | bytes 393224 | tf_op jit(solution)/shard_map/ppermute | solution.py:164
  11.0 7.2 %collective-permute-start.5 = (bf16[256,256]{1,0:T(8,128)(2,1)S(1)}, bf16[256,256]{1,0:T(8,128)(2,1)S(1)}, u32[]{:S(2)}, u32[]{:S(2)}) collective-permute-start(bf16[256,256]{1,0:T(8,128)(2,1)S(1)} %get-tuple-element.34.refs_1_), channel_id=1, source_target_pairs={{0,6},{1,7},{2,4},{3,5},{4,2},{5,3},{6,0},{7,1},{8,14},{9,15},{10,... | collective-permute-start | bytes 393224 | tf_op jit(solution)/shard_map/ppermute | solution.py:164
  14.4 5.8 %collective-permute-start.3 = (bf16[256,256]{1,0:T(8,128)(2,1)S(1)}, bf16[256,256]{1,0:T(8,128)(2,1)S(1)}, u32[]{:S(2)}, u32[]{:S(2)}) collective-permute-start(bf16[256,256]{1,0:T(8,128)(2,1)S(1)} %get-tuple-element.34.refs_1_), channel_id=1, source_target_pairs={{0,4},{1,5},{2,6},{3,7},{4,0},{5,1},{6,2},{7,3},{8,12},{9,13},{10,... | collective-permute-start | bytes 393224 | tf_op jit(solution)/shard_map/ppermute | solution.py:164
  15.7 5.0 %collective-permute-start.1 = (bf16[256,256]{1,0:T(8,128)(2,1)S(1)}, bf16[256,256]{1,0:T(8,128)(2,1)S(1)}, u32[]{:S(2)}, u32[]{:S(2)}) collective-permute-start(bf16[256,256]{1,0:T(8,128)(2,1)S(1)} %get-tuple-element.34.refs_1_), channel_id=1, source_target_pairs={{0,2},{1,3},{2,0},{3,1},{4,6},{5,7},{6,4},{7,5},{8,10},{9,11},{10,... | collective-permute-start | bytes 393224 | tf_op jit(solution)/shard_map/ppermute | solution.py:164
  15.7 5.0 %collective-permute-start = (bf16[256,256]{1,0:T(8,128)(2,1)S(1)}, bf16[256,256]{1,0:T(8,128)(2,1)S(1)}, u32[]{:S(2)}, u32[]{:S(2)}) collective-permute-start(bf16[256,256]{1,0:T(8,128)(2,1)S(1)} %get-tuple-element.34.refs_1_), channel_id=1, source_target_pairs={{0,1},{1,0},{2,3},{3,2},{4,5},{5,4},{6,7},{7,6},{8,9},{9,8},{10,11... | collective-permute-start | bytes 393224 | tf_op jit(solution)/shard_map/ppermute | solution.py:164
  18.2 3.1 %collective-permute-start.18 = (bf16[256,256]{1,0:T(8,128)(2,1)S(1)}, bf16[256,256]{1,0:T(8,128)(2,1)S(1)}, u32[]{:S(2)}, u32[]{:S(2)}) collective-permute-start(bf16[256,256]{1,0:T(8,128)(2,1)S(1)} %collective-permute-done.17.refs_8_), channel_id=1, source_target_pairs={{0,1},{1,0},{2,3},{3,2},{4,5},{5,4},{6,7},{7,6},{8,9},{9,8},{10,11... | collective-permute-start | bytes 393224 | tf_op jit(solution)/shard_map/ppermute | solution.py:164
  20.1 1.5 %collective-permute-start.6 = (bf16[256,256]{1,0:T(8,128)(2,1)S(1)}, bf16[256,256]{1,0:T(8,128)(2,1)S(1)}, u32[]{:S(2)}, u32[]{:S(2)}) collective-permute-start(bf16[256,256]{1,0:T(8,128)(2,1)S(1)} %collective-permute-done.5.refs_7_), channel_id=1, source_target_pairs={{0,1},{1,0},{2,3},{3,2},{4,5},{5,4},{6,7},{7,6},{8,9},{9,8},{10,11... | collective-permute-start | bytes 393224 | tf_op jit(solution)/shard_map/ppermute | solution.py:164
  20.7 3.6 %collective-permute-start.4 = (bf16[256,256]{1,0:T(8,128)(2,1)S(1)}, bf16[256,256]{1,0:T(8,128)(2,1)S(1)}, u32[]{:S(2)}, u32[]{:S(2)}) collective-permute-start(bf16[256,256]{1,0:T(8,128)(2,1)S(1)} %collective-permute-done.3.refs_5_), channel_id=1, source_target_pairs={{0,1},{1,0},{2,3},{3,2},{4,5},{5,4},{6,7},{7,6},{8,9},{9,8},{10,11... | collective-permute-start | bytes 393224 | tf_op jit(solution)/shard_map/ppermute | solution.py:164
  20.7 4.9 %collective-permute-start.2 = (bf16[256,256]{1,0:T(8,128)(2,1)S(1)}, bf16[256,256]{1,0:T(8,128)(2,1)S(1)}, u32[]{:S(2)}, u32[]{:S(2)}) collective-permute-start(bf16[256,256]{1,0:T(8,128)(2,1)S(1)} %collective-permute-done.1.refs_3_), channel_id=1, source_target_pairs={{0,1},{1,0},{2,3},{3,2},{4,5},{5,4},{6,7},{7,6},{8,9},{9,8},{10,11... | collective-permute-start | bytes 393224 | tf_op jit(solution)/shard_map/ppermute | solution.py:164
  21.2 11.4 %collective-permute-start.19 = (bf16[400,256]{1,0:T(8,128)(2,1)S(1)}, bf16[400,256]{1,0:T(8,128)(2,1)S(1)}, u32[]{:S(2)}, u32[]{:S(2)}) collective-permute-start(bf16[400,256]{1,0:T(8,128)(2,1)S(1)} %get-tuple-element.43), channel_id=1, source_target_pairs={{0,8},{8,0},{16,24},{24,16},{1,9},{9,1},{17,25},{25,17},{2,10},{10... | collective-permute-start | bytes 614408 | tf_op jit(solution)/shard_map/ppermute | solution.py:164
  21.7 20.4 %collective-permute-start.10 = (bf16[400,256]{1,0:T(8,128)(2,1)S(1)}, bf16[400,256]{1,0:T(8,128)(2,1)S(1)}, u32[]{:S(2)}, u32[]{:S(2)}) collective-permute-start(bf16[400,256]{1,0:T(8,128)(2,1)S(1)} %get-tuple-element.35), channel_id=1, source_target_pairs={{0,16},{8,24},{16,0},{24,8},{1,17},{9,25},{17,1},{25,9},{2,18},{10... | collective-permute-start | bytes 614408 | tf_op jit(solution)/shard_map/ppermute | solution.py:164
  24.3 17.9 %collective-permute-start.11 = (bf16[400,256]{1,0:T(8,128)(2,1)S(1)}, bf16[400,256]{1,0:T(8,128)(2,1)S(1)}, u32[]{:S(2)}, u32[]{:S(2)}) collective-permute-start(bf16[400,256]{1,0:T(8,128)(2,1)S(1)} %get-tuple-element.36), channel_id=1, source_target_pairs={{0,24},{8,16},{16,8},{24,0},{1,25},{9,17},{17,9},{25,1},{2,26},{10... | collective-permute-start | bytes 614408 | tf_op jit(solution)/shard_map/ppermute | solution.py:164
  25.6 1.3 %collective-permute-start.16 = (bf16[256,256]{1,0:T(8,128)(2,1)S(1)}, bf16[256,256]{1,0:T(8,128)(2,1)S(1)}, u32[]{:S(2)}, u32[]{:S(2)}) collective-permute-start(bf16[256,256]{1,0:T(8,128)(2,1)S(1)} %collective-permute-done.15.refs_6_), channel_id=1, source_target_pairs={{0,1},{1,0},{2,3},{3,2},{4,5},{5,4},{6,7},{7,6},{8,9},{9,8},{10,11... | collective-permute-start | bytes 393224 | tf_op jit(solution)/shard_map/ppermute | solution.py:164
  25.6 3.0 %collective-permute-start.14 = (bf16[256,256]{1,0:T(8,128)(2,1)S(1)}, bf16[256,256]{1,0:T(8,128)(2,1)S(1)}, u32[]{:S(2)}, u32[]{:S(2)}) collective-permute-start(bf16[256,256]{1,0:T(8,128)(2,1)S(1)} %collective-permute-done.13.refs_4_), channel_id=1, source_target_pairs={{0,1},{1,0},{2,3},{3,2},{4,5},{5,4},{6,7},{7,6},{8,9},{9,8},{10,11... | collective-permute-start | bytes 393224 | tf_op jit(solution)/shard_map/ppermute | solution.py:164
  27.0 20.7 %collective-permute-start.7 = (bf16[128,256]{1,0:T(8,128)(2,1)S(1)}, bf16[128,256]{1,0:T(8,128)(2,1)S(1)}, u32[]{:S(2)}, u32[]{:S(2)}) collective-permute-start(bf16[128,256]{1,0:T(8,128)(2,1)S(1)} %keys.3), channel_id=1, source_target_pairs={{0,16},{8,24},{16,0},{24,8},{1,17},{9,25},{17,1},{25,9},{2,18},{10... | collective-permute-start | bytes 196616 | tf_op jit(solution)/shard_map/ppermute | solution.py:164
  28.7 19.7 %collective-permute-start.9 = (bf16[128,256]{1,0:T(8,128)(2,1)S(1)}, bf16[128,256]{1,0:T(8,128)(2,1)S(1)}, u32[]{:S(2)}, u32[]{:S(2)}) collective-permute-start(bf16[128,256]{1,0:T(8,128)(2,1)S(1)} %keys.4), channel_id=1, source_target_pairs={{0,16},{8,24},{16,0},{24,8},{1,17},{9,25},{17,1},{25,9},{2,18},{10... | collective-permute-start | bytes 196616 | tf_op jit(solution)/shard_map/ppermute | solution.py:164
  49.0 5.6 %collective-permute-start.20 = (bf16[128,512]{1,0:T(8,128)(2,1)S(1)}, bf16[128,512]{1,0:T(8,128)(2,1)S(1)}, u32[]{:S(2)}, u32[]{:S(2)}) collective-permute-start(bf16[128,512]{1,0:T(8,128)(2,1)S(1)} %get-tuple-element.49), channel_id=1, source_target_pairs={{0,8},{8,0},{16,24},{24,16},{1,9},{9,1},{17,25},{25,17},{2,10},{10... | collective-permute-start | bytes 393224 | tf_op jit(solution)/shard_map/ppermute | solution.py:164
  50.5 12.5 %collective-permute-start.21 = (bf16[128,512]{1,0:T(8,128)(2,1)S(1)}, bf16[128,512]{1,0:T(8,128)(2,1)S(1)}, u32[]{:S(2)}, u32[]{:S(2)}) collective-permute-start(bf16[128,512]{1,0:T(8,128)(2,1)S(1)} %get-tuple-element.57), channel_id=1, source_target_pairs={{0,16},{8,24},{16,0},{24,8},{1,17},{9,25},{17,1},{25,9},{2,18},{10... | collective-permute-start | bytes 393224 | tf_op jit(solution)/shard_map/ppermute | solution.py:164
  53.9 9.0 %collective-permute-start.22 = (bf16[128,512]{1,0:T(8,128)(2,1)S(1)}, bf16[128,512]{1,0:T(8,128)(2,1)S(1)}, u32[]{:S(2)}, u32[]{:S(2)}) collective-permute-start(bf16[128,512]{1,0:T(8,128)(2,1)S(1)} %get-tuple-element.58), channel_id=1, source_target_pairs={{0,24},{8,16},{16,8},{24,0},{1,25},{9,17},{17,9},{25,1},{2,26},{10... | collective-permute-start | bytes 393224 | tf_op jit(solution)/shard_map/ppermute | solution.py:164

commit v4 on v3

--- a/solution.py
+++ b/solution.py
@@ -417,8 +417,8 @@
 
 
 def own_kernel(
-    place_ref, up_ref, bias_ref, near_keys, far_keys, p0, p1,
-    mixed_a, query_edge_a, state_a, query_s, value_s, key_s,
+    place_ref, up_ref, bias_ref, near_keys, far_keys, p0, p1, query_edge_b,
+    mixed_a, mixed_b, query_edge_a, query_s, value_s, key_s,
 ):
     place = place_ref[0]
     size = mixed_a.shape[0]
@@ -441,22 +441,24 @@
     mixed_a[...] = dot_nn(scores, value_s[...])
     query_edge_a[...] = joined(short(times(scaled, found["query_edge"])))
     key_edge = joined(short(times(keys, found["key_edge"])))
-    state_a[...] = dot_tn(key_edge, value_s[...]).astype(jnp.bfloat16)
+    state = dot_tn(key_edge, value_s[...]).astype(jnp.bfloat16)
+    mixed_b[...] = dot_nn(query_edge_b[...], state)
 
 
 def other_kernel(
-    place_ref, up_ref, bias_ref, state_a, p2, p3,
-    mixed_b, query_fwd_b, query_bwd_b, fwd_b, bwd_b, end_b, edge_b, rate_b, query_s,
+    place_ref, up_ref, bias_ref, own_keys, p2, p3,
+    query_edge_b, value_b, query_fwd_b, query_bwd_b, fwd_b, bwd_b, end_b, edge_b, rate_b, query_s,
 ):
     place = place_ref[0]
     arrange(place, query_s, query_of(p2), query_of(p3))
+    arrange_values(place, value_b, p2, p3)
     up, bias, sum_up_to = decay_inputs(up_ref, bias_ref, query_s.shape[0])
     low = arrange_low(place, p2, p3)
     found = factors(*decay_of(low, up, bias, sum_up_to), place >= HEADS // 2)
     scaled = in_blocks(query_s[...].astype(jnp.float32) * DK**-0.5)
     query_fwd_b[...] = joined(short(times(scaled, found["query_fwd"])))
     query_bwd_b[...] = joined(short(times(scaled, found["query_bwd"])))
-    mixed_b[...] = dot_nn(joined(short(times(scaled, found["query_edge"]))), state_a[...])
+    query_edge_b[...] = joined(short(times(scaled, found["query_edge"])))
     fwd_b[...] = joined(found["key_fwd"])
     bwd_b[...] = joined(found["key_bwd"])
     end_b[...] = joined(found["key_end"])
@@ -468,25 +470,32 @@
 def normed_of(mixed, gain):
     mixed = mixed.astype(jnp.bfloat16).astype(jnp.float32)
     mean = jnp.mean(mixed * mixed, axis=-1, keepdims=True)
-    return (mixed * lax.rsqrt(mean + norm_eps) * gain).astype(jnp.bfloat16)
-
-
-def write_halves(place, result_s, near_ref, far_ref):
+    return mixed * lax.rsqrt(mean + norm_eps) * gain
+
+
+def in_order(place, near, far):
+    odd = (place & 1) == 1
+    return jnp.where(odd, far, near), jnp.where(odd, near, far)
+
+
+def ordered_keys(place, near_keys, far_keys):
+    halves = (keys[...].astype(jnp.float32) for keys in (near_keys, far_keys))
+    return joined(in_order(place, *halves))
+
+
+def write_halves(place, result, near_ref, far_ref):
     tok_count = near_ref.shape[0]
-    half = place & 1
-    for which, out_ref in ((half, near_ref), (1 - half, far_ref)):
-        at = pl.ds(pl.multiple_of(which * tok_count, tok_count), tok_count)
-        out_ref[...] = result_s[at, :]
+    near, far = in_order(place, result[:tok_count], result[tok_count:])
+    near_ref[...] = near.astype(jnp.bfloat16)
+    far_ref[...] = far.astype(jnp.bfloat16)
 
 
 def far_kernel(
-    place_ref, gain_ref, near_keys, far_keys, p2, p3, mixed_b, query_fwd_b, query_bwd_b, fwd_b, bwd_b, end_b, rate_b,
-    near_ref, far_ref, value_s, key_s, result_s,
+    place_ref, gain_ref, near_keys, far_keys, value_b, mixed_b, query_fwd_b, query_bwd_b, fwd_b, bwd_b,
+    end_b, rate_b, near_ref, far_ref,
 ):
     place = place_ref[0]
-    arrange_values(place, value_s, p2, p3)
-    arrange(place, key_s, near_keys, far_keys)
-    keys = key_s[...].astype(jnp.float32)
+    keys = ordered_keys(place, near_keys, far_keys)
     rates = [rate_b[at : at + 1, :] for at in range(0, rate_b.shape[0], PACK)]
     scores = scores_of(
         in_blocks(query_fwd_b[...]),
@@ -496,23 +505,18 @@
         in_blocks(keys * end_b[...]),
         rates,
     )
-    mixed = mixed_b[...] + dot_nn(scores, value_s[...])
-    result_s[...] = normed_of(mixed, gain_ref[...])
-    write_halves(place, result_s, near_ref, far_ref)
+    mixed = mixed_b[...] + dot_nn(scores, value_b[...])
+    write_halves(place, normed_of(mixed, gain_ref[...]), near_ref, far_ref)
 
 
 def near_kernel(
-    place_ref, gain_ref, near_keys, far_keys, p2, p3, mixed_a, query_edge_a, edge_b,
-    near_ref, far_ref, value_s, key_s, result_s,
+    place_ref, gain_ref, near_keys, far_keys, value_b, mixed_a, query_edge_a, edge_b, near_ref, far_ref
 ):
     place = place_ref[0]
-    arrange_values(place, value_s, p2, p3)
-    arrange(place, key_s, near_keys, far_keys)
-    key_edge = (key_s[...].astype(jnp.float32) * edge_b[...]).astype(jnp.bfloat16)
-    state = dot_tn(key_edge, value_s[...]).astype(jnp.bfloat16)
+    keys = ordered_keys(place, near_keys, far_keys)
+    state = dot_tn((keys * edge_b[...]).astype(jnp.bfloat16), value_b[...]).astype(jnp.bfloat16)
     mixed = mixed_a[...] + dot_nn(query_edge_a[...], state)
-    result_s[...] = normed_of(mixed, gain_ref[...])
-    write_halves(place, result_s, near_ref, far_ref)
+    write_halves(place, normed_of(mixed, gain_ref[...]), near_ref, far_ref)
 
 
 def on_chip(kernel, place, operands, shapes, scratch):
@@ -535,34 +539,29 @@
     factor = ((size, DK), wide)
     rates = ((size // BLOCK * PACK, DK), wide)
     half = ((tok_count, DV), narrow)
-    mixed_a, query_edge_a, state_a = on_chip(
+    query_edge_b, value_b, query_fwd_b, query_bwd_b, fwd_b, bwd_b, end_b, edge_b, rate_b = on_chip(
+        other_kernel,
+        place,
+        (up, bias, own[0], *parcels[2:]),
+        [query, value, query, query, factor, factor, factor, factor, rates],
+        [query],
+    )
+    mixed_a, mixed_b, query_edge_a = on_chip(
         own_kernel,
         place,
-        (up, bias, *own, *parcels[:2]),
-        [mixed, query, ((DK, DV), narrow)],
+        (up, bias, *own, *parcels[:2], query_edge_b),
+        [mixed, mixed, query],
         [query, value, query],
     )
-    mixed_b, query_fwd_b, query_bwd_b, fwd_b, bwd_b, end_b, edge_b, rate_b = on_chip(
-        other_kernel,
-        place,
-        (up, bias, state_a, *parcels[2:]),
-        [mixed, query, query, factor, factor, factor, factor, rates],
-        [query],
-    )
-    scratch = [value, query, value]
     far = on_chip(
         far_kernel,
         place,
-        (gain, *got, *parcels[2:], mixed_b, query_fwd_b, query_bwd_b, fwd_b, bwd_b, end_b, rate_b),
+        (gain, *got, value_b, mixed_b, query_fwd_b, query_bwd_b, fwd_b, bwd_b, end_b, rate_b),
         [half, half],
-        scratch,
+        [],
     )
     near = on_chip(
-        near_kernel,
-        place,
-        (gain, *got, *parcels[2:], mixed_a, query_edge_a, edge_b),
-        [half, half],
-        scratch,
+        near_kernel, place, (gain, *got, value_b, mixed_a, query_edge_a, edge_b), [half, half], []
     )
     return [*near, *far]
 

time: 63.9 us -> 63.6 us (level)
  transfers between devices with their start and end apart: 23 -> 23, of which waited for: 11 -> 10; matrix products, arithmetic and copies ran while one was open for 0% -> 0% of each run, Pallas kernels for 9% -> 9%
where the time goes in v4:
time: 63.6 us; the launch traced here: 63.5 us
  waiting for transfers between devices  31.9 us (50%)
  starting transfers between devices  24 us (38%)
  Pallas kernels  7.43 us (12%)
    ppermute x23, waiting for transfers between devices, exchange(): return lax.ppermute(tensor, axis, [(i, i ^ flip) for i in range(size)])  31.9 us
    ppermute x23, starting transfers between devices, exchange(): return lax.ppermute(tensor, axis, [(i, i ^ flip) for i in range(size)])  24 us
    pallas_call x4, Pallas kernels, on_chip(): pl.pallas_call(kernel, in_specs=[pl.BlockSpec(memory_space=pltpu.SMEM)] +...  3.98 us
    pallas_call x1, Pallas kernels, prepare(): pl.pallas_call(prepare_kernel, in_specs=[pl.BlockSpec(memory_space=pltpu....  1.54 us
  transfers between devices with their start and end apart: 23, of which 10 were waited for; matrix products, arithmetic and copies ran while one was open for 0% of the time, Pallas kernels for 9%

profile of v4, /device:TPU:0, one launch (start us, length us, event | category | flops | bytes accessed | tf_op | source)
XLA Modules:
  0.0 63.5 jit_solution(5253281322703683282)
XLA Ops:
  0.0 3.1 %collective-permute-start.8 = (bf16[128,2048]{1,0:T(8,128)(2,1)}, bf16[128,2048]{1,0:T(8,128)(2,1)S(1)}, u32[]{:S(2)}, u32[]{:S(2)}) collective-permute-start(bf16[128,2048]{1,0:T(8,128)(2,1)} %bitcast.10), channel_id=1, source_target_pairs={{0,8},{8,0},{16,24},{24,16},{1,9},{9,1},{17,25},{25,17},{2,10},{10... | collective-permute-start | bytes 1572872 | tf_op jit(solution)/shard_map/ppermute | solution.py:164
  3.1 1.5 %prepare.1 = (bf16[256,256]{1,0:T(8,128)(2,1)S(1)}, bf16[256,256]{1,0:T(8,128)(2,1)S(1)}, bf16[128,2048]{1,0:T(8,128)(2,1)S(1)}, f32[16,256]{1,0:T(8,128)S(1)}, ...) custom-call(s32[1]{0:T(128)} %bitcast.place_ref, ...), custom_call_target="tpu_custom_call" | custom-call | tf_op jit(solution)/shard_map/prepare/pallas_call | solution.py:243
  4.6 2.5 %collective-permute-start.15 = (bf16[256,256]{1,0:T(8,128)(2,1)S(1)}, bf16[256,256]{1,0:T(8,128)(2,1)S(1)}, u32[]{:S(2)}, u32[]{:S(2)}) collective-permute-start(bf16[256,256]{1,0:T(8,128)(2,1)S(1)} %get-tuple-element.38.refs_2_), channel_id=1, source_target_pairs={{0,6},{1,7},{2,4},{3,5},{4,2},{5,3},{6,0},{7,1},{8,14},{9,15},{10,... | collective-permute-start | bytes 393224 | tf_op jit(solution)/shard_map/ppermute | solution.py:164
  7.1 0.5 collective-permute-start.13
  7.6 0.5 collective-permute-start.11
  8.2 0.0 collective-permute-start.10
  8.2 2.8 %collective-permute-done.15.refs_8_ = bf16[256,256]{1,0:T(8,128)(2,1)S(1)} collective-permute-done((bf16[256,256]{1,0:T(8,128)(2,1)S(1)}, bf16[256,256]{1,0:T(8,128)(2,1)S(1)}, u32[]{:S(2)}, u32[]{:S(2)}) %collective-permute-start.15) | collective-permute-done | bytes 131104 | tf_op jit(solution)/shard_map/ppermute | solution.py:164
  11.0 3.4 %collective-permute-start.5 = (bf16[256,256]{1,0:T(8,128)(2,1)S(1)}, bf16[256,256]{1,0:T(8,128)(2,1)S(1)}, u32[]{:S(2)}, u32[]{:S(2)}) collective-permute-start(bf16[256,256]{1,0:T(8,128)(2,1)S(1)} %get-tuple-element.35.refs_1_), channel_id=1, source_target_pairs={{0,6},{1,7},{2,4},{3,5},{4,2},{5,3},{6,0},{7,1},{8,14},{9,15},{10,... | collective-permute-start | bytes 393224 | tf_op jit(solution)/shard_map/ppermute | solution.py:164
  14.4 0.0 collective-permute-done.13.refs_6_
  14.4 1.3 %collective-permute-start.3 = (bf16[256,256]{1,0:T(8,128)(2,1)S(1)}, bf16[256,256]{1,0:T(8,128)(2,1)S(1)}, u32[]{:S(2)}, u32[]{:S(2)}) collective-permute-start(bf16[256,256]{1,0:T(8,128)(2,1)S(1)} %get-tuple-element.35.refs_1_), channel_id=1, source_target_pairs={{0,4},{1,5},{2,6},{3,7},{4,0},{5,1},{6,2},{7,3},{8,12},{9,13},{10,... | collective-permute-start | bytes 393224 | tf_op jit(solution)/shard_map/ppermute | solution.py:164
  15.7 0.0 collective-permute-done.11.refs_4_
  15.7 0.1 collective-permute-start
  15.7 2.4 %collective-permute-done.5.refs_7_ = bf16[256,256]{1,0:T(8,128)(2,1)S(1)} collective-permute-done((bf16[256,256]{1,0:T(8,128)(2,1)S(1)}, bf16[256,256]{1,0:T(8,128)(2,1)S(1)}, u32[]{:S(2)}, u32[]{:S(2)}) %collective-permute-start.5) | collective-permute-done | bytes 131104 | tf_op jit(solution)/shard_map/ppermute | solution.py:164
  18.2 0.0 collective-permute-start.16
  18.2 2.0 %collective-permute-done.3.refs_5_ = bf16[256,256]{1,0:T(8,128)(2,1)S(1)} collective-permute-done((bf16[256,256]{1,0:T(8,128)(2,1)S(1)}, bf16[256,256]{1,0:T(8,128)(2,1)S(1)}, u32[]{:S(2)}, u32[]{:S(2)}) %collective-permute-start.3) | collective-permute-done | bytes 131104 | tf_op jit(solution)/shard_map/ppermute | solution.py:164
  20.1 0.6 collective-permute-done.1.refs_3_
  20.7 0.0 collective-permute-start.4
  20.7 0.0 collective-permute-done.refs_2_
  20.7 0.5 collective-permute-start.2
  21.2 2.6 %collective-permute-start.17 = (bf16[400,256]{1,0:T(8,128)(2,1)S(1)}, bf16[400,256]{1,0:T(8,128)(2,1)S(1)}, u32[]{:S(2)}, u32[]{:S(2)}) collective-permute-start(bf16[400,256]{1,0:T(8,128)(2,1)S(1)} %get-tuple-element.40), channel_id=1, source_target_pairs={{0,16},{8,24},{16,0},{24,8},{1,17},{9,25},{17,1},{25,9},{2,18},{10... | collective-permute-start | bytes 614408 | tf_op jit(solution)/shard_map/ppermute | solution.py:164
  23.8 0.2 collective-permute-start.18
  24.0 0.0 collective-permute-done.4.refs_6_
  24.0 0.7 %collective-permute-start.19 = (bf16[400,256]{1,0:T(8,128)(2,1)S(1)}, bf16[400,256]{1,0:T(8,128)(2,1)S(1)}, u32[]{:S(2)}, u32[]{:S(2)}) collective-permute-start(bf16[400,256]{1,0:T(8,128)(2,1)S(1)} %get-tuple-element.45), channel_id=1, source_target_pairs={{0,8},{8,0},{16,24},{24,16},{1,9},{9,1},{17,25},{25,17},{2,10},{10... | collective-permute-start | bytes 614408 | tf_op jit(solution)/shard_map/ppermute | solution.py:164
  24.7 0.0 collective-permute-start.14
  24.7 0.0 collective-permute-done.8.refs_0_.refs_1_
  24.7 0.5 collective-permute-start.12
  25.2 0.3 keys.3
  25.5 0.3 keys.4
  25.9 0.2 collective-permute-done.14.refs_7_
  26.1 3.5 %collective-permute-start.7 = (bf16[128,256]{1,0:T(8,128)(2,1)S(1)}, bf16[128,256]{1,0:T(8,128)(2,1)S(1)}, u32[]{:S(2)}, u32[]{:S(2)}) collective-permute-start(bf16[128,256]{1,0:T(8,128)(2,1)S(1)} %keys.3), channel_id=1, source_target_pairs={{0,16},{8,24},{16,0},{24,8},{1,17},{9,25},{17,1},{25,9},{2,18},{10... | collective-permute-start | bytes 196616 | tf_op jit(solution)/shard_map/ppermute | solution.py:164
  29.6 0.0 collective-permute-done.12.refs_5_
  29.6 0.2 collective-permute-start.9
  29.7 0.5 keys.5
  30.2 8.7 %collective-permute-done.17.p2 = bf16[400,256]{1,0:T(8,128)(2,1)S(1)} collective-permute-done((bf16[400,256]{1,0:T(8,128)(2,1)S(1)}, bf16[400,256]{1,0:T(8,128)(2,1)S(1)}, u32[]{:S(2)}, u32[]{:S(2)}) %collective-permute-start.17) | collective-permute-done | bytes 204832 | tf_op jit(solution)/shard_map/ppermute | solution.py:164
  38.9 0.0 collective-permute-done.18.p3
  38.9 0.9 %shard_map.91 = (bf16[256,256]{1,0:T(8,128)(2,1)S(1)}, bf16[256,512]{1,0:T(8,128)(2,1)S(1)}, bf16[256,256]{1,0:T(8,128)(2,1)S(1)}, bf16[256,256]{1,0:T(8,128)(2,...) custom-call(s32[1]{0:T(128)} %bitcast.place_ref, ...), custom_call_target="tpu_custom_call" | custom-call | tf_op jit(solution)/shard_map/pallas_call | solution.py:523
  39.8 1.7 %shard_map.92 = (f32[256,512]{1,0:T(8,128)S(1)}, f32[256,512]{1,0:T(8,128)S(1)}, bf16[256,256]{1,0:T(8,128)(2,1)S(1)}) custom-call(s32[1]{0:T(128)} %bitcast.place_ref, f32[16,256]{1,0:T(8,128)S(1)} %get-tuple-element.36.up_ref, f32[1,256]{1,0:T(1,128)S(1)} %get-tuple-element.37.bias_ref, bf16[128,256]{1,0:T(8,128)(2,1)S(1)} %get-tuple-element.39.own_keys.near_keys, ...), custom_call_target="tpu_custom_call" | custom-call | tf_op jit(solution)/shard_map/pallas_call | solution.py:523
  41.5 5.0 %collective-permute-done.7.near_keys = bf16[128,256]{1,0:T(8,128)(2,1)S(1)} collective-permute-done((bf16[128,256]{1,0:T(8,128)(2,1)S(1)}, bf16[128,256]{1,0:T(8,128)(2,1)S(1)}, u32[]{:S(2)}, u32[]{:S(2)}) %collective-permute-start.7) | collective-permute-done | bytes 65568 | tf_op jit(solution)/shard_map/ppermute | solution.py:164
  46.6 1.3 %collective-permute-done.9.far_keys = bf16[128,256]{1,0:T(8,128)(2,1)S(1)} collective-permute-done((bf16[128,256]{1,0:T(8,128)(2,1)S(1)}, bf16[128,256]{1,0:T(8,128)(2,1)S(1)}, u32[]{:S(2)}, u32[]{:S(2)}) %collective-permute-start.9) | collective-permute-done | bytes 65568 | tf_op jit(solution)/shard_map/ppermute | solution.py:164
  47.9 0.6 shard_map.93
  48.5 0.6 collective-permute-start.20
  49.1 0.7 %shard_map.94 = (bf16[128,512]{1,0:T(8,128)(2,1)S(1)}, bf16[128,512]{1,0:T(8,128)(2,1)S(1)}) custom-call(s32[1]{0:T(128)} %bitcast.place_ref, f32[1,512]{1,0:T(1,128)S(1)} %get-tuple-element.33.gain_ref, bf16[128,256]{1,0:T(8,128)(2,1)S(1)} %collective-permute-done.7.near_keys, bf16[128,256]{1,0:T(8,128)(2,1)S(1)} %collective-permute-done.9.far_keys, ...), custom_call_target="tpu_custom_call" | custom-call | tf_op jit(solution)/shard_map/pallas_call | solution.py:523
  49.8 2.7 %collective-permute-start.21 = (bf16[128,512]{1,0:T(8,128)(2,1)S(1)}, bf16[128,512]{1,0:T(8,128)(2,1)S(1)}, u32[]{:S(2)}, u32[]{:S(2)}) collective-permute-start(bf16[128,512]{1,0:T(8,128)(2,1)S(1)} %get-tuple-element.59), channel_id=1, source_target_pairs={{0,16},{8,24},{16,0},{24,8},{1,17},{9,25},{17,1},{25,9},{2,18},{10... | collective-permute-start | bytes 393224 | tf_op jit(solution)/shard_map/ppermute | solution.py:164
  52.5 1.2 %collective-permute-start.22 = (bf16[128,512]{1,0:T(8,128)(2,1)S(1)}, bf16[128,512]{1,0:T(8,128)(2,1)S(1)}, u32[]{:S(2)}, u32[]{:S(2)}) collective-permute-start(bf16[128,512]{1,0:T(8,128)(2,1)S(1)} %get-tuple-element.60), channel_id=1, source_target_pairs={{0,24},{8,16},{16,8},{24,0},{1,25},{9,17},{17,9},{25,1},{2,26},{10... | collective-permute-start | bytes 393224 | tf_op jit(solution)/shard_map/ppermute | solution.py:164
  53.8 2.0 %collective-permute-done.20.refs_1_ = bf16[128,512]{1,0:T(8,128)(2,1)S(1)} collective-permute-done((bf16[128,512]{1,0:T(8,128)(2,1)S(1)}, bf16[128,512]{1,0:T(8,128)(2,1)S(1)}, u32[]{:S(2)}, u32[]{:S(2)}) %collective-permute-start.20) | collective-permute-done | bytes 131104 | tf_op jit(solution)/shard_map/ppermute | solution.py:164
  55.7 6.9 %collective-permute-done.21.refs_2_ = bf16[128,512]{1,0:T(8,128)(2,1)S(1)} collective-permute-done((bf16[128,512]{1,0:T(8,128)(2,1)S(1)}, bf16[128,512]{1,0:T(8,128)(2,1)S(1)}, u32[]{:S(2)}, u32[]{:S(2)}) %collective-permute-start.21) | collective-permute-done | bytes 131104 | tf_op jit(solution)/shard_map/ppermute | solution.py:164
  62.7 0.0 collective-permute-done.22.refs_3_
  62.7 0.8 %join.1 = bf16[128,2048]{1,0:T(8,128)(2,1)} custom-call(s32[1]{0:T(128)} %bitcast.place_ref, bf16[128,512]{1,0:T(8,128)(2,1)S(1)} %get-tuple-element.50.refs_0_, bf16[128,512]{1,0:T(8,128)(2,1)S(1)} %collective-permute-done.20.refs_1_, bf16[128,512]{1,0:T(8,128)(2,1)S(1)} %collective-permute-done.21.refs_2_, bf16[128,512]{1,0:T(8,128)(2,1)S(1)} %collective-permute-done.22.refs_3_), custom_call_target="tpu_custom_call" | custom-call | tf_op jit(solution)/shard_map/join/pallas_call | solution.py:577
  (7 shorter events, 0.0 us)
Async XLA Ops:
  0.0 24.7 %collective-permute-start.8 = (bf16[128,2048]{1,0:T(8,128)(2,1)}, bf16[128,2048]{1,0:T(8,128)(2,1)S(1)}, u32[]{:S(2)}, u32[]{:S(2)}) collective-permute-start(bf16[128,2048]{1,0:T(8,128)(2,1)} %bitcast.10), channel_id=1, source_target_pairs={{0,8},{8,0},{16,24},{24,16},{1,9},{9,1},{17,25},{25,17},{2,10},{10... | collective-permute-start | bytes 1572872 | tf_op jit(solution)/shard_map/ppermute | solution.py:164
  4.6 6.4 %collective-permute-start.15 = (bf16[256,256]{1,0:T(8,128)(2,1)S(1)}, bf16[256,256]{1,0:T(8,128)(2,1)S(1)}, u32[]{:S(2)}, u32[]{:S(2)}) collective-permute-start(bf16[256,256]{1,0:T(8,128)(2,1)S(1)} %get-tuple-element.38.refs_2_), channel_id=1, source_target_pairs={{0,6},{1,7},{2,4},{3,5},{4,2},{5,3},{6,0},{7,1},{8,14},{9,15},{10,... | collective-permute-start | bytes 393224 | tf_op jit(solution)/shard_map/ppermute | solution.py:164
  7.1 7.3 %collective-permute-start.13 = (bf16[256,256]{1,0:T(8,128)(2,1)S(1)}, bf16[256,256]{1,0:T(8,128)(2,1)S(1)}, u32[]{:S(2)}, u32[]{:S(2)}) collective-permute-start(bf16[256,256]{1,0:T(8,128)(2,1)S(1)} %get-tuple-element.38.refs_2_), channel_id=1, source_target_pairs={{0,4},{1,5},{2,6},{3,7},{4,0},{5,1},{6,2},{7,3},{8,12},{9,13},{10,... | collective-permute-start | bytes 393224 | tf_op jit(solution)/shard_map/ppermute | solution.py:164
  7.6 8.0 %collective-permute-start.11 = (bf16[256,256]{1,0:T(8,128)(2,1)S(1)}, bf16[256,256]{1,0:T(8,128)(2,1)S(1)}, u32[]{:S(2)}, u32[]{:S(2)}) collective-permute-start(bf16[256,256]{1,0:T(8,128)(2,1)S(1)} %get-tuple-element.38.refs_2_), channel_id=1, source_target_pairs={{0,2},{1,3},{2,0},{3,1},{4,6},{5,7},{6,4},{7,5},{8,10},{9,11},{10,... | collective-permute-start | bytes 393224 | tf_op jit(solution)/shard_map/ppermute | solution.py:164
  8.2 7.5 %collective-permute-start.10 = (bf16[256,256]{1,0:T(8,128)(2,1)S(1)}, bf16[256,256]{1,0:T(8,128)(2,1)S(1)}, u32[]{:S(2)}, u32[]{:S(2)}) collective-permute-start(bf16[256,256]{1,0:T(8,128)(2,1)S(1)} %get-tuple-element.38.refs_2_), channel_id=1, source_target_pairs={{0,1},{1,0},{2,3},{3,2},{4,5},{5,4},{6,7},{7,6},{8,9},{9,8},{10,11... | collective-permute-start | bytes 393224 | tf_op jit(solution)/shard_map/ppermute | solution.py:164
  11.0 7.2 %collective-permute-start.5 = (bf16[256,256]{1,0:T(8,128)(2,1)S(1)}, bf16[256,256]{1,0:T(8,128)(2,1)S(1)}, u32[]{:S(2)}, u32[]{:S(2)}) collective-permute-start(bf16[256,256]{1,0:T(8,128)(2,1)S(1)} %get-tuple-element.35.refs_1_), channel_id=1, source_target_pairs={{0,6},{1,7},{2,4},{3,5},{4,2},{5,3},{6,0},{7,1},{8,14},{9,15},{10,... | collective-permute-start | bytes 393224 | tf_op jit(solution)/shard_map/ppermute | solution.py:164
  14.4 5.8 %collective-permute-start.3 = (bf16[256,256]{1,0:T(8,128)(2,1)S(1)}, bf16[256,256]{1,0:T(8,128)(2,1)S(1)}, u32[]{:S(2)}, u32[]{:S(2)}) collective-permute-start(bf16[256,256]{1,0:T(8,128)(2,1)S(1)} %get-tuple-element.35.refs_1_), channel_id=1, source_target_pairs={{0,4},{1,5},{2,6},{3,7},{4,0},{5,1},{6,2},{7,3},{8,12},{9,13},{10,... | collective-permute-start | bytes 393224 | tf_op jit(solution)/shard_map/ppermute | solution.py:164
  15.7 5.0 %collective-permute-start.1 = (bf16[256,256]{1,0:T(8,128)(2,1)S(1)}, bf16[256,256]{1,0:T(8,128)(2,1)S(1)}, u32[]{:S(2)}, u32[]{:S(2)}) collective-permute-start(bf16[256,256]{1,0:T(8,128)(2,1)S(1)} %get-tuple-element.35.refs_1_), channel_id=1, source_target_pairs={{0,2},{1,3},{2,0},{3,1},{4,6},{5,7},{6,4},{7,5},{8,10},{9,11},{10,... | collective-permute-start | bytes 393224 | tf_op jit(solution)/shard_map/ppermute | solution.py:164
  15.7 5.0 %collective-permute-start = (bf16[256,256]{1,0:T(8,128)(2,1)S(1)}, bf16[256,256]{1,0:T(8,128)(2,1)S(1)}, u32[]{:S(2)}, u32[]{:S(2)}) collective-permute-start(bf16[256,256]{1,0:T(8,128)(2,1)S(1)} %get-tuple-element.35.refs_1_), channel_id=1, source_target_pairs={{0,1},{1,0},{2,3},{3,2},{4,5},{5,4},{6,7},{7,6},{8,9},{9,8},{10,11... | collective-permute-start | bytes 393224 | tf_op jit(solution)/shard_map/ppermute | solution.py:164
  18.2 3.1 %collective-permute-start.16 = (bf16[256,256]{1,0:T(8,128)(2,1)S(1)}, bf16[256,256]{1,0:T(8,128)(2,1)S(1)}, u32[]{:S(2)}, u32[]{:S(2)}) collective-permute-start(bf16[256,256]{1,0:T(8,128)(2,1)S(1)} %collective-permute-done.15.refs_8_), channel_id=1, source_target_pairs={{0,1},{1,0},{2,3},{3,2},{4,5},{5,4},{6,7},{7,6},{8,9},{9,8},{10,11... | collective-permute-start | bytes 393224 | tf_op jit(solution)/shard_map/ppermute | solution.py:164
  20.1 3.7 %collective-permute-start.6 = (bf16[256,256]{1,0:T(8,128)(2,1)S(1)}, bf16[256,256]{1,0:T(8,128)(2,1)S(1)}, u32[]{:S(2)}, u32[]{:S(2)}) collective-permute-start(bf16[256,256]{1,0:T(8,128)(2,1)S(1)} %collective-permute-done.5.refs_7_), channel_id=1, source_target_pairs={{0,1},{1,0},{2,3},{3,2},{4,5},{5,4},{6,7},{7,6},{8,9},{9,8},{10,11... | collective-permute-start | bytes 393224 | tf_op jit(solution)/shard_map/ppermute | solution.py:164
  20.7 3.3 %collective-permute-start.4 = (bf16[256,256]{1,0:T(8,128)(2,1)S(1)}, bf16[256,256]{1,0:T(8,128)(2,1)S(1)}, u32[]{:S(2)}, u32[]{:S(2)}) collective-permute-start(bf16[256,256]{1,0:T(8,128)(2,1)S(1)} %collective-permute-done.3.refs_5_), channel_id=1, source_target_pairs={{0,1},{1,0},{2,3},{3,2},{4,5},{5,4},{6,7},{7,6},{8,9},{9,8},{10,11... | collective-permute-start | bytes 393224 | tf_op jit(solution)/shard_map/ppermute | solution.py:164
  20.7 4.0 %collective-permute-start.2 = (bf16[256,256]{1,0:T(8,128)(2,1)S(1)}, bf16[256,256]{1,0:T(8,128)(2,1)S(1)}, u32[]{:S(2)}, u32[]{:S(2)}) collective-permute-start(bf16[256,256]{1,0:T(8,128)(2,1)S(1)} %collective-permute-done.1.refs_3_), channel_id=1, source_target_pairs={{0,1},{1,0},{2,3},{3,2},{4,5},{5,4},{6,7},{7,6},{8,9},{9,8},{10,11... | collective-permute-start | bytes 393224 | tf_op jit(solution)/shard_map/ppermute | solution.py:164
  21.2 17.7 %collective-permute-start.17 = (bf16[400,256]{1,0:T(8,128)(2,1)S(1)}, bf16[400,256]{1,0:T(8,128)(2,1)S(1)}, u32[]{:S(2)}, u32[]{:S(2)}) collective-permute-start(bf16[400,256]{1,0:T(8,128)(2,1)S(1)} %get-tuple-element.40), channel_id=1, source_target_pairs={{0,16},{8,24},{16,0},{24,8},{1,17},{9,25},{17,1},{25,9},{2,18},{10... | collective-permute-start | bytes 614408 | tf_op jit(solution)/shard_map/ppermute | solution.py:164
  23.8 15.1 %collective-permute-start.18 = (bf16[400,256]{1,0:T(8,128)(2,1)S(1)}, bf16[400,256]{1,0:T(8,128)(2,1)S(1)}, u32[]{:S(2)}, u32[]{:S(2)}) collective-permute-start(bf16[400,256]{1,0:T(8,128)(2,1)S(1)} %get-tuple-element.41), channel_id=1, source_target_pairs={{0,24},{8,16},{16,8},{24,0},{1,25},{9,17},{17,9},{25,1},{2,26},{10... | collective-permute-start | bytes 614408 | tf_op jit(solution)/shard_map/ppermute | solution.py:164
  24.0 15.8 %collective-permute-start.19 = (bf16[400,256]{1,0:T(8,128)(2,1)S(1)}, bf16[400,256]{1,0:T(8,128)(2,1)S(1)}, u32[]{:S(2)}, u32[]{:S(2)}) collective-permute-start(bf16[400,256]{1,0:T(8,128)(2,1)S(1)} %get-tuple-element.45), channel_id=1, source_target_pairs={{0,8},{8,0},{16,24},{24,16},{1,9},{9,1},{17,25},{25,17},{2,10},{10... | collective-permute-start | bytes 614408 | tf_op jit(solution)/shard_map/ppermute | solution.py:164
  24.7 1.3 %collective-permute-start.14 = (bf16[256,256]{1,0:T(8,128)(2,1)S(1)}, bf16[256,256]{1,0:T(8,128)(2,1)S(1)}, u32[]{:S(2)}, u32[]{:S(2)}) collective-permute-start(bf16[256,256]{1,0:T(8,128)(2,1)S(1)} %collective-permute-done.13.refs_6_), channel_id=1, source_target_pairs={{0,1},{1,0},{2,3},{3,2},{4,5},{5,4},{6,7},{7,6},{8,9},{9,8},{10,11... | collective-permute-start | bytes 393224 | tf_op jit(solution)/shard_map/ppermute | solution.py:164
  24.7 4.8 %collective-permute-start.12 = (bf16[256,256]{1,0:T(8,128)(2,1)S(1)}, bf16[256,256]{1,0:T(8,128)(2,1)S(1)}, u32[]{:S(2)}, u32[]{:S(2)}) collective-permute-start(bf16[256,256]{1,0:T(8,128)(2,1)S(1)} %collective-permute-done.11.refs_4_), channel_id=1, source_target_pairs={{0,1},{1,0},{2,3},{3,2},{4,5},{5,4},{6,7},{7,6},{8,9},{9,8},{10,11... | collective-permute-start | bytes 393224 | tf_op jit(solution)/shard_map/ppermute | solution.py:164
  26.1 20.5 %collective-permute-start.7 = (bf16[128,256]{1,0:T(8,128)(2,1)S(1)}, bf16[128,256]{1,0:T(8,128)(2,1)S(1)}, u32[]{:S(2)}, u32[]{:S(2)}) collective-permute-start(bf16[128,256]{1,0:T(8,128)(2,1)S(1)} %keys.3), channel_id=1, source_target_pairs={{0,16},{8,24},{16,0},{24,8},{1,17},{9,25},{17,1},{25,9},{2,18},{10... | collective-permute-start | bytes 196616 | tf_op jit(solution)/shard_map/ppermute | solution.py:164
  29.6 18.3 %collective-permute-start.9 = (bf16[128,256]{1,0:T(8,128)(2,1)S(1)}, bf16[128,256]{1,0:T(8,128)(2,1)S(1)}, u32[]{:S(2)}, u32[]{:S(2)}) collective-permute-start(bf16[128,256]{1,0:T(8,128)(2,1)S(1)} %keys.4), channel_id=1, source_target_pairs={{0,16},{8,24},{16,0},{24,8},{1,17},{9,25},{17,1},{25,9},{2,18},{10... | collective-permute-start | bytes 196616 | tf_op jit(solution)/shard_map/ppermute | solution.py:164
  48.5 7.2 %collective-permute-start.20 = (bf16[128,512]{1,0:T(8,128)(2,1)S(1)}, bf16[128,512]{1,0:T(8,128)(2,1)S(1)}, u32[]{:S(2)}, u32[]{:S(2)}) collective-permute-start(bf16[128,512]{1,0:T(8,128)(2,1)S(1)} %get-tuple-element.51), channel_id=1, source_target_pairs={{0,8},{8,0},{16,24},{24,16},{1,9},{9,1},{17,25},{25,17},{2,10},{10... | collective-permute-start | bytes 393224 | tf_op jit(solution)/shard_map/ppermute | solution.py:164
  49.8 12.8 %collective-permute-start.21 = (bf16[128,512]{1,0:T(8,128)(2,1)S(1)}, bf16[128,512]{1,0:T(8,128)(2,1)S(1)}, u32[]{:S(2)}, u32[]{:S(2)}) collective-permute-start(bf16[128,512]{1,0:T(8,128)(2,1)S(1)} %get-tuple-element.59), channel_id=1, source_target_pairs={{0,16},{8,24},{16,0},{24,8},{1,17},{9,25},{17,1},{25,9},{2,18},{10... | collective-permute-start | bytes 393224 | tf_op jit(solution)/shard_map/ppermute | solution.py:164
  52.5 10.1 %collective-permute-start.22 = (bf16[128,512]{1,0:T(8,128)(2,1)S(1)}, bf16[128,512]{1,0:T(8,128)(2,1)S(1)}, u32[]{:S(2)}, u32[]{:S(2)}) collective-permute-start(bf16[128,512]{1,0:T(8,128)(2,1)S(1)} %get-tuple-element.60), channel_id=1, source_target_pairs={{0,24},{8,16},{16,8},{24,0},{1,25},{9,17},{17,9},{25,1},{2,26},{10... | collective-permute-start | bytes 393224 | tf_op jit(solution)/shard_map/ppermute | solution.py:164
